TPU v7x, 32 devices: a whole 2x2x4 slice. The times are simulated.
32 devices in a mesh: sp: 8 (over z, x), tp: 4 (over y, core).
Axes of the slice: x: 2, y: 2, z: 4, core: 2. Of those that a mesh axis runs over, the one named last changes fastest.
Arguments:
- rows_in: bfloat16 [1024, 2048], P(('sp', 'tp')), may hold values from -8 to 8
- in_gain: float32 [2048], replicated, may hold values from 0.1 to 1.9
- query_down: bfloat16 [2048, 256], replicated, may hold values from -0.125 to 0.125
- query_gain: float32 [256], replicated, may hold values from 0.1 to 1.9
- kv_down: bfloat16 [2048, 128], replicated, may hold values from -0.125 to 0.125
- kv_gain: float32 [128], replicated, may hold values from 0.1 to 1.9
- rope_down: bfloat16 [2048, 64], replicated, may hold values from -0.125 to 0.125
- query_nope_up: bfloat16 [256, 512], P(None, 'tp'), may hold values from -0.375 to 0.375
- query_rope_up: bfloat16 [256, 256], P(None, 'tp'), may hold values from -0.375 to 0.375
- key_up: bfloat16 [128, 512], P(None, 'tp'), may hold values from -2.9811459 to 2.9811459
- value_up: bfloat16 [128, 512], P(None, 'tp'), may hold values from -0.5 to 0.5
- rec_query: bfloat16 [2048, 256], P(None, 'tp'), may hold values from -0.125 to 0.125
- rec_key: bfloat16 [2048, 256], P(None, 'tp'), may hold values from -0.125 to 0.125
- rec_value: bfloat16 [2048, 512], P(None, 'tp'), may hold values from -0.125 to 0.125
- gate_weight: bfloat16 [2048, 4, 4], P(None, None, 'tp'), may hold values from -0.125 to 0.125
- forget_level: float32 [1024, 2, 4], P('sp', None, 'tp'), may hold values from 0 to 14
- head_gain: float32 [512], P('tp'), may hold values from 0.1 to 1.9
- init_state: float32 [2, 4, 64, 128], P(None, 'tp'), may hold values from -96 to 96
- init_norm: float32 [2, 4, 64], P(None, 'tp'), may hold values from -96 to 96
- out_attn: bfloat16 [512, 2048], P('tp'), may hold values from -0.25 to 0.25
- out_rec: bfloat16 [512, 2048], P('tp'), may hold values from -0.25 to 0.25
Outputs:
- mixed_out: bfloat16 [1024, 2048], P(('sp', 'tp'))
All inputs are finite; a program needn't handle non-finite values.
Results may differ from a plain program's by a relative error of at most 0.023.
Values may be sent and summed in bfloat16 or wider, within the bound.
No kernel may reach another device: no remote copies, remote signals or barrier semaphores. Data moves between devices by JAX's collectives and lax.ppermute only.
A program may use at most 64 MiB of HBM per device.

v0:
```python
import functools

import jax
import jax.numpy as jnp
import numpy as np
from jax import lax
from jax.experimental import pallas as pl
from jax.experimental.pallas import tpu as pltpu
from jax.sharding import PartitionSpec as P

EPS = 1e-06
NEG = -(2.0**100)
AUX = 8
F32 = jnp.float32
BF16 = jnp.bfloat16
NT = (((1,), (1,)), ((), ()))


def radices_of(peers):
    first = 2 if peers % 2 == 0 else 1
    rest = peers // first
    radices = [first]
    while rest > 1:
        step = 4 if rest % 4 == 0 else next(p for p in range(2, rest + 1) if rest % p == 0)
        radices.append(step)
        rest //= step
    if len(radices) == 1:
        radices.append(1)
    return radices


def peer_digit(digit, radix, k, sending):
    if radix & (radix - 1) == 0:
        return digit ^ k
    return (digit + k if sending else digit - k + radix) % radix


def digit_pairs(peers, stride, radix, k):
    pairs = []
    for i in range(peers):
        digit = (i // stride) % radix
        pairs.append((i, i + (peer_digit(digit, radix, k, True) - digit) * stride))
    return pairs


def dot(a, b):
    return jnp.dot(a, b, preferred_element_type=F32)


def dot_nt(a, b):
    return lax.dot_general(a, b, NT, preferred_element_type=F32)


def dot_split(a, b):
    high = a.astype(BF16)
    low = (a - high.astype(F32)).astype(BF16)
    return dot(high, b) + dot(low, b)


def rms(values, gain):
    return values * lax.rsqrt(jnp.mean(values * values, axis=-1, keepdims=True) + EPS) * gain


def iota2(rows, cols, dim):
    return lax.broadcasted_iota(jnp.int32, (rows, cols), dim)


def turned_rows(weight_t):
    half = weight_t.shape[0] // 2
    return jnp.concatenate([weight_t, -weight_t[half:], weight_t[:half]], axis=0)


def angle_table(ids_ref, cos_base, sin_base, cos_row, sin_row):
    block = ids_ref[1]
    cb, sb = cos_base[pl.ds(block, 1), :], sin_base[pl.ds(block, 1), :]
    cr, sr = cos_row[...], sin_row[...]
    cos, sin = cb * cr - sb * sr, sb * cr + cb * sr
    half = cr.shape[1] // 2
    return jnp.where(iota2(cr.shape[0], cr.shape[1], 1) < half, cos, sin)


def rotated(product, table):
    mixed = product * table
    return mixed + pltpu.roll(mixed, product.shape[1] // 2, 1)


def aux_rows(n_row, peak_row, keep_row):
    high = keep_row.astype(BF16).astype(F32)
    mid = (keep_row - high).astype(BF16).astype(F32)
    low = keep_row - high - mid
    pad = jnp.zeros((AUX - 5, n_row.shape[1]), F32)
    return jnp.concatenate([n_row, peak_row, high, mid, low, pad], axis=0)


def read_state(block):
    c_rows = block.shape[0] - AUX
    block = block.astype(F32)
    aux = block[c_rows:]
    return block[:c_rows], aux[0:1], aux[1:2], aux[2:3] + aux[3:4] + aux[4:5]


def placed(state, place, use=None):
    c_part, n_part, peak, keep = state
    if use is not None:
        peak, keep = jnp.where(use, peak, NEG), jnp.where(use, keep, 0.0)
    return c_part, n_part, peak, keep, place


def chain(states):
    logs = []
    total = functools.reduce(jnp.add, [state[3] for state in states])
    for index, (_, _, peak, _, place) in enumerate(states):
        log = peak
        for other, (_, _, _, keep, at) in enumerate(states):
            if other != index:
                log = log + jnp.where(at > place, keep, 0.0)
        logs.append(log)
    return logs, functools.reduce(jnp.maximum, logs), total


def weighted(states, logs, top):
    c_sum = n_sum = None
    for state, log in zip(states, logs):
        weight = jnp.exp(log - top)
        c_part, n_part = weight * state[0], weight * state[1]
        c_sum = c_part if c_sum is None else c_sum + c_part
        n_sum = n_part if n_sum is None else n_sum + n_part
    return c_sum, n_sum


def joined(states):
    logs, top, keep = chain(states)
    top = top.astype(BF16).astype(F32)
    c_sum, n_sum = weighted(states, logs, top)
    return jnp.concatenate([c_sum, aux_rows(n_sum, top, keep)], axis=0)


def log_sigmoid(x):
    return jnp.minimum(x, 0.0) - jnp.log(1.0 + jnp.exp(-jnp.abs(x)))


def head_kernel(
    ids,
    *refs,
    pieces,
    key_width,
):
    piece_refs = refs[: 2 * pieces]
    (
        in_gain,
        kv_down,
        kv_gain,
        rope_t,
        key_t,
        rec_value,
        gate_t,
        level,
        cos_base,
        sin_base,
        cos_row,
        sin_row,
        message,
        normed_out,
        keys_out,
        values_out,
        rows_out,
        table_out,
        rows,
    ) = refs[2 * pieces :]
    mine = ids[0]
    pair, core = mine // 2, mine % 2
    step = piece_refs[0].shape[0]
    seq = rows.shape[0]
    for k in range(pieces):
        source = lax.rem(pair - k + pieces, pieces) * 2
        rows[pl.ds(pl.multiple_of((source + core) * step, step), step), :] = piece_refs[2 * k][...]
        rows[pl.ds(pl.multiple_of((source + 1 - core) * step, step), step), :] = piece_refs[
            2 * k + 1
        ][...]
    normed = rms(rows[...].astype(F32), in_gain[...]).astype(BF16)
    normed_out[...] = normed
    table = angle_table(ids, cos_base, sin_base, cos_row, sin_row)
    table_out[...] = table
    latent = kv_down.shape[1]
    straight = dot(normed, jnp.concatenate([kv_down[...], rec_value[...]], axis=1))
    turned = turned_rows(rope_t[...])
    gate_rows = gate_t.shape[0]
    fill = jnp.zeros((turned.shape[0] - key_width - gate_rows, turned.shape[1]), BF16)
    crossed = dot_nt(
        normed, jnp.concatenate([turned, key_t[...], gate_t[...], fill], axis=0)
    )
    rope_lanes = turned.shape[0]
    lat = rms(straight[:, :latent], kv_gain[...]).astype(BF16)
    rope = rotated(crossed[:, :rope_lanes], table)
    half = seq // 2
    quarter = half // 2
    lat = jnp.where(core == 0, lat[:half], lat[half:])
    rope = jnp.where(core == 0, rope[:half], rope[half:])
    lanes = iota2(quarter, rope.shape[1], 1)
    packed = jnp.where(lanes < rope_t.shape[0], rope[:quarter], rope[quarter:])
    message[0:half, :] = lat
    message[half : half + quarter, :] = packed.astype(BF16)

    mixed = crossed[:, rope_lanes:]
    keys = mixed.astype(BF16).astype(F32) * key_width ** (-0.5)
    keys = jnp.where(iota2(seq, keys.shape[1], 1) < key_width, keys, 0.0)
    keys_out[...] = keys.astype(BF16)
    values = straight[:, latent:].astype(BF16)
    values_out[...] = values
    mixed_t = jnp.transpose(mixed)
    gates = mixed_t[key_width : key_width + 8]

    in_f, in_b = gates[0:1], gates[2:3]
    keep_f = log_sigmoid(gates[1:2] + level[0:1])
    keep_b = log_sigmoid(gates[3:4] + level[1:2])
    row_id, col_id = iota2(seq, seq, 0), iota2(seq, seq, 1)
    upper = jnp.where(row_id <= col_id, 1.0, 0.0).astype(BF16)
    lower = jnp.where(row_id >= col_id, 1.0, 0.0).astype(BF16)
    keeps = jnp.concatenate([keep_f, keep_b, jnp.zeros((6, seq), F32)], axis=0)
    high = keeps.astype(BF16)
    mid = (keeps - high.astype(F32)).astype(BF16)
    low = (keeps - high.astype(F32) - mid.astype(F32)).astype(BF16)
    thirds = jnp.concatenate([high, mid, low, jnp.zeros_like(low)], axis=0)
    cums = dot(thirds, jnp.concatenate([upper, lower], axis=1))
    cums = cums[0:8] + cums[8:16] + cums[16:24]
    cum_f, cum_b = cums[0:1, :seq], cums[1:2, seq:]
    all_f, all_b = cum_f[:, seq - 1 : seq], cum_b[:, 0:1]
    rows_out[...] = jnp.concatenate(
        [cum_f, in_f - cum_f, cum_b, in_b - cum_b, jnp.zeros((4, seq), F32)], axis=0
    )
    keys_t = mixed_t[:key_width].astype(BF16).astype(F32) * key_width ** (-0.5)
    base = half + quarter
    weights = []
    for cum, log_in, total in ((cum_f, in_f, all_f), (cum_b, in_b, all_b)):
        logs = total - cum + log_in
        peak = jnp.max(logs, axis=1, keepdims=True).astype(BF16).astype(F32)
        weight = jnp.exp(logs - peak)
        weights.append((weight, peak, total))
    w_f, w_b = weights[0][0], weights[1][0]
    c_both = dot_split(jnp.concatenate([keys_t * w_f, keys_t * w_b], axis=0), values)
    n_both = dot_split(
        jnp.concatenate([w_f, w_b, jnp.zeros((6, seq), F32)], axis=0), keys.astype(BF16)
    )
    for index in range(2):
        _, peak, total = weights[index]
        c_part = c_both[index * key_width : (index + 1) * key_width]
        n_row = n_both[index : index + 1]
        zero = jnp.zeros_like(n_row)
        block = jnp.concatenate([c_part, aux_rows(n_row, zero + peak, zero + total)], axis=0)
        at = base + index * (key_width + AUX)
        message[at : at + key_width + AUX, :] = block.astype(BF16)


def thirds_of(x):
    high = x.astype(BF16)
    mid = (x - high.astype(F32)).astype(BF16)
    low = (x - high.astype(F32) - mid.astype(F32)).astype(BF16)
    return [high, mid, low]


def local_kernel(
    ids,
    normed_ref,
    keys_ref,
    values_ref,
    rows_ref,
    table_ref,
    query_down,
    query_gain,
    nope_up,
    rope_up_t,
    key_up,
    rec_query_t,
    init_state,
    init_norm,
    keep_out,
    share_out,
    whole,
    *,
    pieces,
):
    normed = normed_ref[...]
    seq = normed.shape[0]
    query_rows = jnp.concatenate([rec_query_t[...], jnp.zeros_like(rec_query_t)], axis=0)
    rec_q = dot_nt(normed, query_rows).astype(BF16)
    q_lat = rms(dot(normed, query_down[...]), query_gain[...]).astype(BF16)
    nope = dot(q_lat, nope_up[...]).astype(BF16)
    rope = rotated(dot_nt(q_lat, turned_rows(rope_up_t[...])), table_ref[...])
    lat = dot_nt(nope, key_up[...]).astype(BF16)
    width = rope_up_t.shape[0]
    lanes = iota2(seq, rope.shape[1], 1)
    low_rope = jnp.where(lanes < width, rope, 0.0).astype(BF16)
    high_rope = jnp.where(lanes >= width, rope, 0.0).astype(BF16)
    values = values_ref[...]
    wide = jnp.concatenate([values, jnp.ones_like(values)], axis=1)
    products = dot_nt(rec_q, keys_ref[...])
    row_id, col_id = iota2(seq, seq, 0), iota2(seq, seq, 1)
    rows = rows_ref[...]
    numers, denoms, marks = [], [], []
    for index in range(2):
        cum = jnp.transpose(jnp.broadcast_to(rows[2 * index : 2 * index + 1], (seq, seq)))
        seen = row_id >= col_id if index == 0 else row_id <= col_id
        logs = jnp.where(seen, cum + rows[2 * index + 1 : 2 * index + 2], NEG)
        peak = jnp.max(logs, axis=1, keepdims=True)
        gated = products * jnp.exp(logs - peak)
        sums = dot_split(gated, wide)
        numers.append(sums[:, : values.shape[1]].astype(BF16))
        denoms.append(sums[:, values.shape[1] :].astype(BF16))
        marks += thirds_of(jnp.broadcast_to(peak, (seq, seq))) + thirds_of(cum)
    columns = [lat, low_rope, high_rope] + numers + denoms + [rec_q] + marks
    step_cols = lat.shape[1]
    for index, column in enumerate(columns):
        whole[:, index * step_cols : (index + 1) * step_cols] = column
    mine = ids[0]
    pair, core = mine // 2, mine % 2
    step = seq // (2 * pieces)
    for side, out in ((core, keep_out), (1 - core, share_out)):
        for k in range(pieces):
            owner = lax.rem(pair + k, pieces) * 2 + side
            out[k * step : (k + 1) * step, 0 : whole.shape[1]] = whole[
                pl.ds(pl.multiple_of(owner * step, step), step), :
            ]
    lanes = init_state.shape[2]
    norms = init_norm[...]
    norms = jnp.concatenate([norms, jnp.zeros((2, lanes - norms.shape[1]), F32)], axis=1)
    rest = jnp.zeros((init_state.shape[1] - 2, lanes), F32)
    first = jnp.concatenate([norms, rest], axis=0).astype(BF16)
    starts = [init_state[0].astype(BF16), init_state[1].astype(BF16), first]
    for out in (keep_out, share_out):
        for index, block in enumerate(starts):
            at = whole.shape[1] + index * lanes
            out[0 : block.shape[0], at : at + lanes] = block


def fold_kernel(value_up, head_gain, out_attn, out_rec, out):
    rows = value_up.shape[0]
    out[0:rows, :] = dot(value_up[...], out_attn[...]).astype(BF16)
    gain = head_gain[...]
    width = gain.shape[1]
    column = jnp.transpose(jnp.broadcast_to(gain, (width, width)))[:, 0:1]
    out[rows:, :] = (column * out_rec[...].astype(F32)).astype(BF16)


def level_states(ids, slot, radix, fetch):
    digit = ids[slot]
    forward, backward = [], []
    for k in range(1, radix):
        source = peer_digit(digit, radix, k, False)
        forward.append(placed(fetch(k, 0), source, source < digit))
        backward.append(placed(fetch(k, 1), -source, source > digit))
    return forward, backward


def merge_kernel(ids, *refs, slot, radix, state_rows, last, next_radix):
    prefix_in = refs[0]
    own = refs[1]
    received = (own,) + refs[2 : 1 + radix]
    outs = refs[1 + radix :]
    prefix_out, sides_out, messages = outs[0], outs[1], outs[2:]
    kv_rows = own.shape[0] - 2 * state_rows

    def fetch(k, direction):
        at = kv_rows + direction * state_rows
        return read_state(received[k][at : at + state_rows, :])

    digit = ids[slot]
    totals = []
    for direction in range(2):
        sign = 1 - 2 * direction
        inner = placed(read_state(prefix_in[direction]), sign * digit)
        before, whole = [inner], [placed(fetch(0, direction), sign * digit)]
        for k in range(1, radix):
            source = peer_digit(digit, radix, k, False)
            state = fetch(k, direction)
            before.append(placed(state, sign * source, sign * source < sign * digit))
            whole.append(placed(state, sign * source))
        inside = joined(before)
        prefix_out[direction] = inside
        sides_out[direction * state_rows : (direction + 1) * state_rows, :] = inside.astype(BF16)
        totals.append(joined(whole).astype(BF16))
    total_f, total_b = totals
    part = kv_rows // 3
    for number, message in enumerate(messages):
        for section in range(3):
            for k in range(radix):
                to = (section * radix + k) * part
                message[to : to + part, :] = received[k][section * part : (section + 1) * part, :]
        at = radix * kv_rows
        if last:
            target = peer_digit(ids[slot + 1], next_radix, number + 1, True)
            ahead = target > ids[slot + 1]
            message[at : at + state_rows, :] = jnp.where(ahead, total_f, total_b)
        else:
            message[at : at + state_rows, :] = total_f
            message[at + state_rows : at + 2 * state_rows, :] = total_b


def load_kernel(*refs):
    count = (len(refs) - 1) // 2
    sems = refs[-1]
    copies = [
        pltpu.make_async_copy(refs[i], refs[count + i], sems.at[i]) for i in range(count)
    ]
    for copy in copies:
        copy.start()
    for copy in copies:
        copy.wait()


def pack_kernel(*refs, count, state_rows):
    received, out = refs[-1 - count : -1], refs[-1]
    part = (received[0].shape[0] - state_rows) // 3
    for k, message in enumerate(received):
        for section in range(3):
            to = (section * count + k) * part
            out[to : to + part, :] = message[section * part : (section + 1) * part, :]
        if k > 0:
            to = 3 * count * part + (k - 1) * state_rows
            out[to : to + state_rows, :] = message[3 * part : 3 * part + state_rows, :]


def attend(sections, keys, part, score_scale):
    rope = keys[2 * part : 3 * part, :]
    scores, lats = [], []
    for section in range(2):
        lat = keys[section * part : (section + 1) * part, :]
        lats.append(lat)
        scores.append(dot_nt(sections[section], jnp.concatenate([lat, rope], axis=1)) * score_scale)
    top = functools.reduce(jnp.maximum, [jnp.max(s, axis=1, keepdims=True) for s in scores])
    mass = accum = None
    for part_scores, lat in zip(scores, lats):
        expo = jnp.exp(part_scores - top)
        gain = dot(expo.astype(BF16), lat)
        total = jnp.sum(expo, axis=1, keepdims=True)
        accum = gain if accum is None else accum + gain
        mass = total if mass is None else mass + total
    return top, mass, accum


def sections_of(queries, width):
    return [
        queries[:, 0 : 2 * width],
        jnp.concatenate([queries[:, 0:width], queries[:, 2 * width :]], axis=1),
    ]


def finished(ids, block, first_ref, packed, sides, slot, radix, state_rows, floor_value):
    base = packed.shape[0] - (radix - 1) * state_rows
    width = packed.shape[1]

    def column(index):
        return block[:, index * width : (index + 1) * width].astype(F32)

    def triple(index):
        return column(index) + column(index + 1) + column(index + 2)

    def fetch(k, direction):
        at = base + (k - 1) * state_rows
        return read_state(packed[at : at + state_rows, :])

    levels = level_states(ids, slot, radix, fetch)
    rec_q = block[:, 7 * width : 8 * width]
    starts = []
    for index in range(2):
        inner = read_state(sides[index * state_rows : (index + 1) * state_rows, :])
        zero = jnp.zeros_like(inner[1])
        first = (
            first_ref[:, (20 + index) * width : (21 + index) * width].astype(F32),
            first_ref[0:8, 22 * width :].astype(F32)[index : index + 1],
            zero,
            zero,
        )
        states = [placed(first, -radix)] + levels[index]
        states.append(placed(inner, ids[slot] if index == 0 else -ids[slot]))
        logs, start_top, _ = chain(states)
        starts.append(weighted(states, logs, start_top) + (start_top,))
    c_start = jnp.concatenate([starts[0][0], starts[1][0]], axis=1)
    pad = jnp.zeros((rec_q.shape[1] - c_start.shape[0], c_start.shape[1]), F32)
    c_start = jnp.concatenate([c_start, pad], axis=0)
    high = c_start.astype(BF16)
    low = (c_start - high.astype(F32)).astype(BF16)
    products = dot(rec_q, high) + dot(rec_q, low)
    summed = None
    for index in range(2):
        _, n_start, start_top = starts[index]
        from_start = products[:, index * width : (index + 1) * width]
        norm_start = jnp.sum(rec_q.astype(F32) * n_start, axis=1, keepdims=True)
        numer, denom = column(3 + index), column(5 + index)
        peak, carry = triple(8 + 6 * index), triple(11 + 6 * index) + start_top
        row_max = jnp.maximum(peak, carry)
        here, there = jnp.exp(peak - row_max), jnp.exp(carry - row_max)
        numer = here * numer + there * from_start
        denom = here * denom + there * norm_start
        result = numer / jnp.maximum(jnp.abs(denom), floor_value * jnp.exp(-row_max))
        summed = result if summed is None else summed + result
    return rms(summed, 1.0).astype(BF16)


def half_kernel(
    ids,
    packed,
    sides,
    kept,
    shared,
    recurrent_out,
    top_out,
    mass_out,
    accum_out,
    *,
    slot,
    radix,
    state_rows,
    floor_value,
    score_scale,
):
    width = packed.shape[1]
    part = (packed.shape[0] - (radix - 1) * state_rows) // 3
    recurrent_out[...] = finished(
        ids, kept[...], kept, packed, sides, slot, radix, state_rows, floor_value
    )
    queries = jnp.concatenate([kept[:, 0 : 3 * width], shared[:, 0 : 3 * width]], axis=0)
    top, mass, accum = attend(sections_of(queries, width), packed, part, score_scale)
    top_out[...] = jnp.broadcast_to(top, top_out.shape)
    mass_out[...] = jnp.broadcast_to(mass, mass_out.shape)
    accum_out[...] = accum


def mix_kernel(
    ids,
    swapped,
    sides,
    kept,
    shared,
    recurrent,
    top_half,
    mass_half,
    accum_half,
    weights,
    other_weights,
    out,
    *,
    slot,
    radix,
    state_rows,
    floor_value,
    score_scale,
    piece,
    step,
):
    width = swapped.shape[1]
    part = (swapped.shape[0] - (radix - 1) * state_rows) // 3
    at = slice(piece * step, (piece + 1) * step)
    also = slice(kept.shape[0] + piece * step, kept.shape[0] + (piece + 1) * step)
    queries = jnp.concatenate([kept[at, 0 : 3 * width], shared[at, 0 : 3 * width]], axis=0)
    top, mass, accum = attend(sections_of(queries, width), swapped, part, score_scale)

    def both(ref):
        return jnp.concatenate([ref[at, :], ref[also, :]], axis=0)

    other_top = both(top_half)
    peak = jnp.maximum(top, other_top)
    here, there = jnp.exp(top - peak), jnp.exp(other_top - peak)
    accum = here * accum + there * both(accum_half)
    mass = here * mass + there * both(mass_half)
    attended = (accum / mass).astype(BF16)
    other = finished(
        ids, shared[at, :], shared, swapped, sides, slot, radix, state_rows, floor_value
    )
    mine = jnp.concatenate([attended[:step], recurrent[at, :]], axis=1)
    theirs = jnp.concatenate([attended[step:], other], axis=1)
    out[...] = (dot(mine, weights[...]) + dot(theirs, other_weights[...])).astype(out.dtype)


def call(kernel, outs, inputs, scratch=(), ids=True, limit=16 << 20, cost=None):
    vmem = pl.BlockSpec(memory_space=pltpu.VMEM)
    in_specs = [vmem] * len(inputs)
    if ids:
        in_specs[0] = pl.BlockSpec(memory_space=pltpu.SMEM)
    return pl.pallas_call(
        kernel,
        out_shape=[jax.ShapeDtypeStruct(shape, dtype) for shape, dtype in outs],
        in_specs=in_specs,
        out_specs=[vmem] * len(outs),
        scratch_shapes=scratch,
        cost_estimate=cost,
        compiler_params=pltpu.CompilerParams(vmem_limit_bytes=limit),
    )(*inputs)


def shards(
    rows_in,
    in_gain,
    query_down,
    query_gain,
    kv_down,
    kv_gain,
    rope_down,
    query_nope_up,
    query_rope_up,
    key_up,
    value_up,
    rec_query,
    rec_key,
    rec_value,
    gate_weight,
    forget_level,
    head_gain,
    init_state,
    init_norm,
    out_attn,
    out_rec,
):
    peers, lanes = lax.axis_size("sp"), lax.axis_size("tp")
    block, mine = lax.axis_index("sp"), lax.axis_index("tp")
    seq = forget_level.shape[0]
    width = rows_in.shape[1]
    nope, rope = key_up.shape[1], rope_down.shape[1]
    key_width, value_width = init_state.shape[2], init_state.shape[3]
    pieces = lanes // 2
    radices = radices_of(peers)
    strides = [int(np.prod(radices[:i])) for i in range(len(radices))]
    divide = np.array([1, 1] + strides, np.int32)
    modulo = np.array([lanes, peers] + radices, np.int32)
    first = np.arange(len(divide)) == 0
    ids = (jnp.where(first, mine, block).astype(jnp.int32) // divide) % modulo

    partner = [(i, i ^ 1) for i in range(lanes)]
    ring = [[(i, (i + 2 * k) % lanes) for i in range(lanes)] for k in range(pieces)]

    gathered = [rows_in]
    for k in range(1, pieces):
        gathered.append(lax.ppermute(rows_in, "tp", ring[k]))
    row_pieces = []
    for piece in gathered:
        row_pieces += [piece, lax.ppermute(piece, "tp", partner)]

    freq = 10000.0 ** (-np.arange(rope // 2, dtype=np.float64) / (rope // 2))
    freq = np.tile(freq, 4)[None, :]
    base = np.arange(peers, dtype=np.float64)[:, None] * seq * freq
    within = np.arange(seq, dtype=np.float64)[:, None] * freq
    tables = [np.cos(base), np.sin(base), np.cos(within), np.sin(within)]
    tables = [jnp.asarray(table.astype(np.float32)) for table in tables]

    held = [
        in_gain[None, :],
        kv_down,
        kv_gain[None, :],
        rope_down.T,
        rec_key.T,
        rec_value,
        gate_weight[:, :, 0].T,
        forget_level[:, :, 0].T,
        *tables,
        query_down,
        query_gain[None, :],
        query_nope_up,
        query_rope_up.T,
        key_up,
        rec_query.T,
        value_up,
        head_gain[None, :],
        init_state[:, 0],
        init_norm[:, 0],
        out_attn,
        out_rec,
    ]
    held = list(
        pl.pallas_call(
            load_kernel,
            out_shape=[pltpu.VMEM(array.shape, array.dtype) for array in held],
            in_specs=[pl.BlockSpec(memory_space=pltpu.HBM)] * len(held),
            out_specs=[pl.BlockSpec(memory_space=pltpu.VMEM)] * len(held),
            scratch_shapes=[pltpu.SemaphoreType.DMA((len(held),))],
            name="load",
            cost_estimate=pl.CostEstimate(flops=10**8, bytes_accessed=1 << 22, transcendentals=0),
            compiler_params=pltpu.CompilerParams(vmem_limit_bytes=16 << 20),
        )(*[pltpu.with_memory_space_constraint(array, pltpu.HBM) for array in held])
    )
    head_args, local_args = held[:12], held[12:18]
    value_up, head_gain, init_state, init_norm, out_attn, out_rec = held[18:]

    state_rows = key_width + AUX
    kv_rows = seq // 2 + seq // 4
    message, normed, keys, values, gate_rows, table = call(
        functools.partial(head_kernel, pieces=pieces, key_width=key_width),
        [
            ((kv_rows + 2 * state_rows, value_width), BF16),
            ((seq, width), BF16),
            ((seq, 2 * key_width), BF16),
            ((seq, value_width), BF16),
            ((8, seq), F32),
            ((seq, 2 * rope), F32),
        ],
        [ids]
        + row_pieces
        + head_args,
        scratch=[pltpu.VMEM((seq, width), BF16)],
    )
    columns = 20 * value_width
    assert key_width == seq // 2
    kept, share = call(
        functools.partial(local_kernel, pieces=pieces),
        [((seq // 2, columns + 3 * value_width), BF16)] * 2,
        [
            ids,
            normed,
            keys,
            values,
            gate_rows,
            table,
            *local_args,
            init_state,
            init_norm,
        ],
        scratch=[pltpu.VMEM((seq, columns), BF16)],
        cost=pl.CostEstimate(flops=10**8, bytes_accessed=1 << 20, transcendentals=0),
    )
    (weights,) = call(
        fold_kernel,
        [((2 * value_width, width), BF16)],
        [value_up, head_gain, out_attn, out_rec],
        ids=False,
        cost=pl.CostEstimate(flops=10**8, bytes_accessed=1 << 20, transcendentals=0),
    )
    other_weights = lax.ppermute(weights, "tp", partner)
    shared = lax.ppermute(share, "tp", partner)

    blank = np.zeros((2, state_rows, value_width), np.float32)
    blank[:, key_width + 1] = NEG
    prefix = jnp.asarray(blank)
    wide = (16 << 20) if peers <= 16 else (40 << 20)
    for level, radix in enumerate(radices[:-1]):
        received = [
            lax.ppermute(message, "sp", digit_pairs(peers, strides[level], radix, k))
            for k in range(1, radix)
        ]
        last = level == len(radices) - 2
        kv_rows *= radix
        count = radices[-1] - 1 if last else 1
        out_rows = kv_rows + (1 if last else 2) * state_rows
        prefix, sides, *messages = call(
            functools.partial(
                merge_kernel,
                slot=2 + level,
                radix=radix,
                state_rows=state_rows,
                last=last,
                next_radix=radices[level + 1],
            ),
            [((2, state_rows, value_width), F32), ((2 * state_rows, value_width), BF16)]
            + [((out_rows, value_width), BF16)] * max(count, 1),
            [ids, prefix, message] + received,
            limit=wide,
        )
        message = messages[0]
    level, radix = len(radices) - 1, radices[-1]
    received = []
    for k in range(1, radix):
        pairs = digit_pairs(peers, strides[level], radix, k)
        received.append(lax.ppermute(messages[k - 1], "sp", pairs))
    other_sides = lax.ppermute(sides, "tp", partner)
    (packed,) = call(
        functools.partial(pack_kernel, count=radix, state_rows=state_rows),
        [((radix * kv_rows + (radix - 1) * state_rows, value_width), BF16)],
        [other_weights, shared, other_sides, message] + received,
        ids=False,
        limit=wide,
    )
    swapped = lax.ppermute(packed, "tp", partner)
    level_facts = dict(
        slot=2 + level,
        radix=radix,
        state_rows=state_rows,
        floor_value=float(seq * peers) ** 0.5,
        score_scale=(nope + rope) ** (-0.5),
    )
    half = call(
        functools.partial(half_kernel, **level_facts),
        [((seq // 2, value_width), BF16)] + [((seq, value_width), F32)] * 3,
        [ids, packed, sides, kept, shared],
        limit=wide,
        cost=pl.CostEstimate(flops=10**8, bytes_accessed=1 << 20, transcendentals=0),
    )
    step = seq // lanes

    def mixed(piece, dtype):
        return call(
            functools.partial(
                mix_kernel,
                piece=piece,
                step=step,
                **level_facts,
            ),
            [((step, width), dtype)],
            [
                ids,
                swapped,
                other_sides,
                kept,
                shared,
                *half,
                weights,
                other_weights,
            ],
            limit=wide if peers <= 16 else 56 << 20,
            cost=pl.CostEstimate(flops=10**8, bytes_accessed=1 << 20, transcendentals=0),
        )[0]

    arrived = []
    for k in range(1, pieces):
        piece = mixed(k, BF16)
        arrived.append(lax.ppermute(piece, "tp", ring[k]))
    total = mixed(0, F32)
    for piece in arrived:
        total = total + piece.astype(F32)
    return total.astype(BF16)


def solution(mesh):
    in_specs = (
        P(("sp", "tp"), None),
        P(),
        P(),
        P(),
        P(),
        P(),
        P(),
        P(None, "tp"),
        P(None, "tp"),
        P(None, "tp"),
        P(None, "tp"),
        P(None, "tp"),
        P(None, "tp"),
        P(None, "tp"),
        P(None, None, "tp"),
        P("sp", None, "tp"),
        P("tp"),
        P(None, "tp", None, None),
        P(None, "tp", None),
        P("tp", None),
        P("tp", None),
    )
    out_specs = P(("sp", "tp"), None)

    return jax.shard_map(shards, mesh=mesh, in_specs=in_specs, out_specs=out_specs, check_vma=False)
```

profile of v0, /device:TPU:0, one launch (start us, length us, event | category | flops | bytes accessed | tf_op | source)
XLA Modules:
  0.0 51.5 jit_solution(12294315408646411743)
XLA Ops:
  0.0 2.5 %load.1 = (f32[1,2048]{1,0:T(1,128)S(1)}, bf16[2048,128]{1,0:T(8,128)(2,1)S(1)}, f32[1,128]{1,0:T(1,128)S(1)}, bf16[64,2048]{1,0:T(8,128)(2,1)S(1)}, bf16[64,204...) custom-call(f32[1,2048]{1,0:T(1,128)} %bitcast.22, ...), custom_call_target="tpu_custom_call" | custom-call | flops 100000000 | bytes 4194304 | tf_op jit(solution)/shard_map/load/pallas_call | solution.py:668
  2.5 0.8 %copy-done = bf16[2048,128]{1,0:T(8,128)(2,1)} copy-done((bf16[2048,128]{1,0:T(8,128)(2,1)}, bf16[2048,128]{1,0:T(8,128)(2,1)S(1)}, u32[]{:S(2)}) %copy-start) | copy-done | bytes 524312
  3.3 0.8 %copy-done.2 = bf16[2048,128]{1,0:T(8,128)(2,1)} copy-done((bf16[2048,128]{1,0:T(8,128)(2,1)}, bf16[2048,128]{1,0:T(8,128)(2,1)S(1)}, u32[]{:S(2)}) %copy-start.2) | copy-done | bytes 524312
  4.1 0.6 %copy-done.28 = f32[2,128]{1,0:T(2,128)} copy-done((f32[2,128]{1,0:T(2,128)}, f32[2,128]{1,0:T(2,128)S(1)}, u32[]{:S(2)}) %copy-start.28) | copy-done | bytes 1048
  4.7 0.6 %copy-done.30 = f32[1,256]{1,0:T(1,128)} copy-done((f32[1,256]{1,0:T(1,128)}, f32[1,256]{1,0:T(1,128)S(1)}, u32[]{:S(2)}) %copy-start.30) | copy-done | bytes 1048
  5.2 0.5 %copy-done.32 = f32[2,64]{1,0:T(2,128)} copy-done((f32[2,64]{1,0:T(2,128)}, f32[2,64]{1,0:T(2,128)S(1)}, u32[]{:S(2)}) %copy-start.32) | copy-done | bytes 536
  5.8 0.6 %copy-done.34 = f32[1,128]{1,0:T(1,128)} copy-done((f32[1,128]{1,0:T(1,128)}, f32[1,128]{1,0:T(1,128)S(1)}, u32[]{:S(2)}) %copy-start.34) | copy-done | bytes 536
  6.5 0.3 shard_map.271.weights
  6.7 0.3 copy-done.4
  7.1 0.1 copy-done.6
  7.2 0.0 copy-done.10
  7.2 0.0 copy-done.14
  7.2 0.0 copy-done.16
  7.2 0.0 copy-done.20
  7.2 0.6 %collective-permute-start = (bf16[256,2048]{1,0:T(8,128)(2,1)S(1)}, bf16[256,2048]{1,0:T(8,128)(2,1)S(1)}, u32[]{:S(2)}, u32[]{:S(2)}) collective-permute-start(bf16[256,2048]{1,0:T(8,128)(2,1)S(1)} %shard_map.271.weights), channel_id=1, source_target_pairs={{0,1},{1,0},{2,3},{3,2},{4,5},{5,4},{6,7},{7,6},{8,9},{9,8},{10,11... | collective-permute-start | bytes 3145736 | tf_op jit(solution)/shard_map/ppermute | solution.py:725
  7.8 2.7 %collective-permute-start.2 = (bf16[32,2048]{1,0:T(8,128)(2,1)S(1)}, bf16[32,2048]{1,0:T(8,128)(2,1)}, u32[]{:S(2)}, u32[]{:S(2)}) collective-permute-start(bf16[32,2048]{1,0:T(8,128)(2,1)S(1)} %copy-done.8), channel_id=1, source_target_pairs={{0,2},{1,3},{2,0},{3,1},{4,6},{5,7},{6,4},{7,5},{8,10},{9,11},{10,... | collective-permute-start | bytes 393224 | tf_op jit(solution)/shard_map/ppermute | solution.py:632
  10.5 0.1 collective-permute-start.1
  10.5 4.0 %collective-permute-done.2.refs_2_ = bf16[32,2048]{1,0:T(8,128)(2,1)} collective-permute-done((bf16[32,2048]{1,0:T(8,128)(2,1)S(1)}, bf16[32,2048]{1,0:T(8,128)(2,1)}, u32[]{:S(2)}, u32[]{:S(2)}) %collective-permute-start.2) | collective-permute-done | bytes 131104 | tf_op jit(solution)/shard_map/ppermute | solution.py:632
  14.6 0.9 %and_select_fusion.ids = s32[4]{0:T(128)S(1)} fusion(s32[4]{0:T(128)} %constant.51, s32[4]{0:T(128)} %constant.38.clone, pred[4]{0:T(512)(128)(4,1)} %constant.37.clone, s32[]{:T(128)S(6)} %axis_index.25, s32[]{:T(128)S(6)} %axis_index.22), kind=kLoop, calls=%fused_computation.1 | loop fusion | flops 60 | bytes 60 | tf_op jit(solution)/shard_map/jit(remainder)/select_n | solution.py:625
  15.5 0.6 %collective-permute-done.3.refs_3_ = bf16[32,2048]{1,0:T(8,128)(2,1)S(1)} collective-permute-done((bf16[32,2048]{1,0:T(8,128)(2,1)}, bf16[32,2048]{1,0:T(8,128)(2,1)S(1)}, u32[]{:S(2)}, u32[]{:S(2)}) %collective-permute-start.3) | collective-permute-done | bytes 131104 | tf_op jit(solution)/shard_map/ppermute | solution.py:635
  16.2 0.7 %copy-done.35 = f32[1,128]{1,0:T(1,128)S(1)} copy-done((f32[1,128]{1,0:T(1,128)S(1)}, f32[1,128]{1,0:T(1,128)}, u32[]{:S(2)}) %copy-start.35) | copy-done | bytes 536
  16.8 0.0 copy-done.23
  16.9 1.0 %copy-done.1 = bf16[2048,128]{1,0:T(8,128)(2,1)S(1)} copy-done((bf16[2048,128]{1,0:T(8,128)(2,1)S(1)}, bf16[2048,128]{1,0:T(8,128)(2,1)}, u32[]{:S(2)}) %copy-start.1) | copy-done | bytes 524312
  17.9 1.0 %copy-done.3 = bf16[2048,128]{1,0:T(8,128)(2,1)S(1)} copy-done((bf16[2048,128]{1,0:T(8,128)(2,1)S(1)}, bf16[2048,128]{1,0:T(8,128)(2,1)}, u32[]{:S(2)}) %copy-start.3) | copy-done | bytes 524312
  18.9 0.9 %copy-done.5 = bf16[64,2048]{1,0:T(8,128)(2,1)S(1)} copy-done((bf16[64,2048]{1,0:T(8,128)(2,1)S(1)}, bf16[64,2048]{1,0:T(8,128)(2,1)}, u32[]{:S(2)}) %copy-start.5) | copy-done | bytes 262168
  19.9 0.8 %copy-done.15 = f32[128,128]{1,0:T(8,128)S(1)} copy-done((f32[128,128]{1,0:T(8,128)S(1)}, f32[128,128]{1,0:T(8,128)}, u32[]{:S(2)}) %copy-start.15) | copy-done | bytes 65560
  20.7 0.8 %copy-done.17 = f32[128,128]{1,0:T(8,128)S(1)} copy-done((f32[128,128]{1,0:T(8,128)S(1)}, f32[128,128]{1,0:T(8,128)}, u32[]{:S(2)}) %copy-start.17) | copy-done | bytes 65560
  21.6 2.3 %shard_map.272 = (bf16[240,128]{1,0:T(8,128)(2,1)S(1)}, bf16[128,2048]{1,0:T(8,128)(2,1)S(1)}, bf16[128,128]{1,0:T(8,128)(2,1)S(1)}, bf16[128,128]{1,0:T(8,128)(...) custom-call(s32[4]{0:T(128)S(1)} %and_select_fusion.ids, bf16[32,2048]{1,0:T(8,128)(2,1)S(1)} %copy-done.8, ...), custom_call_target="tpu_custom_call" | custom-call | tf_op jit(solution)/shard_map/pallas_call | solution.py:579
  24.0 0.6 %copy-done.33 = f32[2,64]{1,0:T(2,128)S(1)} copy-done((f32[2,64]{1,0:T(2,128)S(1)}, f32[2,64]{1,0:T(2,128)}, u32[]{:S(2)}) %copy-start.33) | copy-done | bytes 536
  24.5 0.0 copy-done.31
  24.6 1.5 %shard_map.273 = (bf16[64,2944]{1,0:T(8,128)(2,1)S(1)}, bf16[64,2944]{1,0:T(8,128)(2,1)S(1)}) custom-call(s32[4]{0:T(128)S(1)} %and_select_fusion.ids, bf16[128,2048]{1,0:T(8,128)(2,1)S(1)} %get-tuple-element.61.normed_ref, bf16[128,128]{1,0:T(8,128)(2,1)S(1)} %get-tuple-element.62.keys_ref, bf16[128,128]{1,0:T(8,128)(2,1)S(1)} %get-tuple-element.63.values_ref, ...), custom_call_target="tpu_custom_call" | custom-call | flops 100000000 | bytes 1048576 | tf_op jit(solution)/shard_map/pallas_call | solution.py:579
  26.0 0.2 collective-permute-start.4
  26.3 1.7 %collective-permute-start.5 = (bf16[240,128]{1,0:T(8,128)(2,1)S(1)}, bf16[240,128]{1,0:T(8,128)(2,1)S(1)}, u32[]{:S(2)}, u32[]{:S(2)}) collective-permute-start(bf16[240,128]{1,0:T(8,128)(2,1)S(1)} %get-tuple-element.75.refs_1_), channel_id=1, source_target_pairs={{0,4},{4,0},{8,12},{12,8},{16,20},{20,16},{24,28},{28,24},{1,5},{5... | collective-permute-start | bytes 184328 | tf_op jit(solution)/shard_map/ppermute | solution.py:734
  28.0 2.6 %collective-permute-done.5.refs_2_ = bf16[240,128]{1,0:T(8,128)(2,1)S(1)} collective-permute-done((bf16[240,128]{1,0:T(8,128)(2,1)S(1)}, bf16[240,128]{1,0:T(8,128)(2,1)S(1)}, u32[]{:S(2)}, u32[]{:S(2)}) %collective-permute-start.5) | collective-permute-done | bytes 61472 | tf_op jit(solution)/shard_map/ppermute | solution.py:734
  30.5 1.2 %shard_map.274 = (f32[2,72,128]{2,1,0:T(8,128)}, bf16[144,128]{1,0:T(8,128)(2,1)S(1)}, bf16[264,128]{1,0:T(8,128)(2,1)S(1)}, bf16[264,128]{1,0:T(8,128)(2,1)S(1)}, bf16[264,128]{1,0:T(8,128)(2,1)S(1)}) custom-call(s32[4]{0:T(128)S(1)} %and_select_fusion.ids, f32[2,72,128]{2,1,0:T(8,128)S(1)} %copy-done.9, bf16[240,128]{1,0:T(8,128)(2,1)S(1)} %get-tuple-element.75.refs_1_, ...), custom_call_target="tpu_custom_call" | custom-call | tf_op jit(solution)/shard_map/pallas_call | solution.py:579
  31.8 1.8 %collective-permute-start.7 = (bf16[264,128]{1,0:T(8,128)(2,1)S(1)}, bf16[264,128]{1,0:T(8,128)(2,1)S(1)}, u32[]{:S(2)}, u32[]{:S(2)}) collective-permute-start(bf16[264,128]{1,0:T(8,128)(2,1)S(1)} %get-tuple-element.77.refs_3_), channel_id=1, source_target_pairs={{0,8},{4,12},{8,0},{12,4},{16,24},{20,28},{24,16},{28,20},{1,9},{5... | collective-permute-start | bytes 202760 | tf_op jit(solution)/shard_map/ppermute | solution.py:760
  33.6 2.6 %collective-permute-start.8 = (bf16[264,128]{1,0:T(8,128)(2,1)S(1)}, bf16[264,128]{1,0:T(8,128)(2,1)S(1)}, u32[]{:S(2)}, u32[]{:S(2)}) collective-permute-start(bf16[264,128]{1,0:T(8,128)(2,1)S(1)} %get-tuple-element.78), channel_id=1, source_target_pairs={{0,16},{4,20},{8,24},{12,28},{16,0},{20,4},{24,8},{28,12},{1,17},{... | collective-permute-start | bytes 202760 | tf_op jit(solution)/shard_map/ppermute | solution.py:760
  36.2 0.6 %collective-permute-start.9 = (bf16[264,128]{1,0:T(8,128)(2,1)S(1)}, bf16[264,128]{1,0:T(8,128)(2,1)S(1)}, u32[]{:S(2)}, u32[]{:S(2)}) collective-permute-start(bf16[264,128]{1,0:T(8,128)(2,1)S(1)} %get-tuple-element.79), channel_id=1, source_target_pairs={{0,24},{4,28},{8,16},{12,20},{16,8},{20,12},{24,0},{28,4},{1,25},{... | collective-permute-start | bytes 202760 | tf_op jit(solution)/shard_map/ppermute | solution.py:760
  36.8 4.5 %collective-permute-done.8.refs_5_ = bf16[264,128]{1,0:T(8,128)(2,1)S(1)} collective-permute-done((bf16[264,128]{1,0:T(8,128)(2,1)S(1)}, bf16[264,128]{1,0:T(8,128)(2,1)S(1)}, u32[]{:S(2)}, u32[]{:S(2)}) %collective-permute-start.8) | collective-permute-done | bytes 67616 | tf_op jit(solution)/shard_map/ppermute | solution.py:760
  41.3 0.9 %collective-permute-done.9.refs_6_ = bf16[264,128]{1,0:T(8,128)(2,1)S(1)} collective-permute-done((bf16[264,128]{1,0:T(8,128)(2,1)S(1)}, bf16[264,128]{1,0:T(8,128)(2,1)S(1)}, u32[]{:S(2)}, u32[]{:S(2)}) %collective-permute-start.9) | collective-permute-done | bytes 67616 | tf_op jit(solution)/shard_map/ppermute | solution.py:760
  42.3 0.1 collective-permute-start.10
  42.4 1.1 %shard_map.276 = (bf16[64,128]{1,0:T(8,128)(2,1)S(1)}, f32[128,128]{1,0:T(8,128)S(1)}, f32[128,128]{1,0:T(8,128)S(1)}, f32[128,128]{1,0:T(8,128)S(1)}) custom-call(s32[4]{0:T(128)S(1)} %and_select_fusion.ids, bf16[984,128]{1,0:T(8,128)(2,1)S(1)} %shard_map.275.packed, bf16[144,128]{1,0:T(8,128)(2,1)S(1)} %get-tuple-element.76.sides, ...), custom_call_target="tpu_custom_call" | custom-call | flops 100000000 | bytes 1048576 | tf_op jit(solution)/shard_map/pallas_call | solution.py:579
  43.5 0.4 collective-permute-done.10.swapped
  43.9 1.4 %shard_map.278 = bf16[32,2048]{1,0:T(8,128)(2,1)S(1)} custom-call(s32[4]{0:T(128)S(1)} %and_select_fusion.ids, bf16[984,128]{1,0:T(8,128)(2,1)S(1)} %collective-permute-done.10.swapped, bf16[144,128]{1,0:T(8,128)(2,1)S(1)} %collective-permute-done.6.refs_2_.sides, bf16[64,2944]{1,0:T(8,128)(2,1)S(1)} %get-tuple-element.80.kept, ...), custom_call_target="tpu_custom_call" | custom-call | flops 100000000 | bytes 1048576 | tf_op jit(solution)/shard_map/pallas_call | solution.py:579
  45.3 1.6 %collective-permute-start.11 = (bf16[32,2048]{1,0:T(8,128)(2,1)S(1)}, bf16[32,2048]{1,0:T(8,128)(2,1)S(1)}, u32[]{:S(2)}, u32[]{:S(2)}) collective-permute-start(bf16[32,2048]{1,0:T(8,128)(2,1)S(1)} %shard_map.278), channel_id=1, source_target_pairs={{0,2},{1,3},{2,0},{3,1},{4,6},{5,7},{6,4},{7,5},{8,10},{9,11},{10,... | collective-permute-start | bytes 393224 | tf_op jit(solution)/shard_map/ppermute | solution.py:812
  46.8 1.4 %shard_map.277 = f32[32,2048]{1,0:T(8,128)S(1)} custom-call(s32[4]{0:T(128)S(1)} %and_select_fusion.ids, bf16[984,128]{1,0:T(8,128)(2,1)S(1)} %collective-permute-done.10.swapped, bf16[144,128]{1,0:T(8,128)(2,1)S(1)} %collective-permute-done.6.refs_2_.sides, bf16[64,2944]{1,0:T(8,128)(2,1)S(1)} %get-tuple-element.80.kept, ...), custom_call_target="tpu_custom_call" | custom-call | flops 100000000 | bytes 1048576 | tf_op jit(solution)/shard_map/pallas_call | solution.py:579
  48.2 2.6 %collective-permute-done.11 = bf16[32,2048]{1,0:T(8,128)(2,1)S(1)} collective-permute-done((bf16[32,2048]{1,0:T(8,128)(2,1)S(1)}, bf16[32,2048]{1,0:T(8,128)(2,1)S(1)}, u32[]{:S(2)}, u32[]{:S(2)}) %collective-permute-start.11) | collective-permute-done | bytes 131104 | tf_op jit(solution)/shard_map/ppermute | solution.py:812
  50.9 0.7 %add_convert_fusion = bf16[32,2048]{1,0:T(8,128)(2,1)} fusion(f32[32,2048]{1,0:T(8,128)S(1)} %shard_map.277, bf16[32,2048]{1,0:T(8,128)(2,1)S(1)} %collective-permute-done.11), kind=kLoop, calls=%fused_computation | loop fusion | flops 196608 | bytes 524288 | tf_op jit(solution)/shard_map/convert_element_type | solution.py:816
  (59 shorter events, 0.1 us)
Async XLA Ops:
  2.5 0.8 %copy-start = (bf16[2048,128]{1,0:T(8,128)(2,1)}, bf16[2048,128]{1,0:T(8,128)(2,1)S(1)}, u32[]{:S(2)}) copy-start(bf16[2048,128]{1,0:T(8,128)(2,1)S(1)} %get-tuple-element.50.refs_5_) | copy-start | bytes 1572868
  3.3 0.8 %copy-start.2 = (bf16[2048,128]{1,0:T(8,128)(2,1)}, bf16[2048,128]{1,0:T(8,128)(2,1)S(1)}, u32[]{:S(2)}) copy-start(bf16[2048,128]{1,0:T(8,128)(2,1)S(1)} %get-tuple-element.54.refs_9_) | copy-start | bytes 1572868
  4.1 0.6 %copy-start.28 = (f32[2,128]{1,0:T(2,128)}, f32[2,128]{1,0:T(2,128)S(1)}, u32[]{:S(2)}) copy-start(f32[2,128]{1,0:T(2,128)S(1)} %get-tuple-element.56.refs_11_) | copy-start | bytes 3076
  4.7 0.6 %copy-start.30 = (f32[1,256]{1,0:T(1,128)}, f32[1,256]{1,0:T(1,128)S(1)}, u32[]{:S(2)}) copy-start(f32[1,256]{1,0:T(1,128)S(1)} %get-tuple-element.67.query_gain) | copy-start | bytes 3076
  5.2 0.5 %copy-start.32 = (f32[2,64]{1,0:T(2,128)}, f32[2,64]{1,0:T(2,128)S(1)}, u32[]{:S(2)}) copy-start(f32[2,64]{1,0:T(2,128)S(1)} %get-tuple-element.73.init_norm) | copy-start | bytes 1540
  5.8 0.6 %copy-start.34 = (f32[1,128]{1,0:T(1,128)}, f32[1,128]{1,0:T(1,128)S(1)}, u32[]{:S(2)}) copy-start(f32[1,128]{1,0:T(1,128)S(1)} %get-tuple-element.51.refs_6_) | copy-start | bytes 1540
  6.4 0.7 %copy-start.4 = (bf16[64,2048]{1,0:T(8,128)(2,1)}, bf16[64,2048]{1,0:T(8,128)(2,1)S(1)}, u32[]{:S(2)}) copy-start(bf16[64,2048]{1,0:T(8,128)(2,1)S(1)} %get-tuple-element.53.refs_8_) | copy-start | bytes 786436
  6.4 0.8 %copy-start.6 = (bf16[64,2048]{1,0:T(8,128)(2,1)}, bf16[64,2048]{1,0:T(8,128)(2,1)S(1)}, u32[]{:S(2)}) copy-start(bf16[64,2048]{1,0:T(8,128)(2,1)S(1)} %get-tuple-element.71.rec_query_t) | copy-start | bytes 786436
  6.4 0.8 %copy-start.10 = (bf16[256,128]{1,0:T(8,128)(2,1)}, bf16[256,128]{1,0:T(8,128)(2,1)S(1)}, u32[]{:S(2)}) copy-start(bf16[256,128]{1,0:T(8,128)(2,1)S(1)} %get-tuple-element.68.nope_up) | copy-start | bytes 196612
  6.4 0.8 %copy-start.12 = (f32[2,64,128]{2,1,0:T(8,128)}, f32[2,64,128]{2,1,0:T(8,128)S(1)}, u32[]{:S(2)}) copy-start(f32[2,64,128]{2,1,0:T(8,128)S(1)} %get-tuple-element.72.init_state) | copy-start | bytes 196612
  6.4 0.8 %copy-start.14 = (f32[128,128]{1,0:T(8,128)}, f32[128,128]{1,0:T(8,128)S(1)}, u32[]{:S(2)}) copy-start(f32[128,128]{1,0:T(8,128)S(1)} %get-tuple-element.59.refs_14_) | copy-start | bytes 196612
  6.4 0.8 %copy-start.16 = (f32[128,128]{1,0:T(8,128)}, f32[128,128]{1,0:T(8,128)S(1)}, u32[]{:S(2)}) copy-start(f32[128,128]{1,0:T(8,128)S(1)} %get-tuple-element.60.refs_15_) | copy-start | bytes 196612
  6.4 0.8 %copy-start.18 = (bf16[64,256]{1,0:T(8,128)(2,1)}, bf16[64,256]{1,0:T(8,128)(2,1)S(1)}, u32[]{:S(2)}) copy-start(bf16[64,256]{1,0:T(8,128)(2,1)S(1)} %get-tuple-element.69.rope_up_t) | copy-start | bytes 98308
  6.4 0.8 %copy-start.20 = (bf16[128,128]{1,0:T(8,128)(2,1)}, bf16[128,128]{1,0:T(8,128)(2,1)S(1)}, u32[]{:S(2)}) copy-start(bf16[128,128]{1,0:T(8,128)(2,1)S(1)} %get-tuple-element.70.key_up) | copy-start | bytes 98308
  6.4 0.8 %copy-start.22 = (f32[1,2048]{1,0:T(1,128)}, f32[1,2048]{1,0:T(1,128)S(1)}, u32[]{:S(2)}) copy-start(f32[1,2048]{1,0:T(1,128)S(1)} %get-tuple-element.49.refs_4_) | copy-start | bytes 24580
  6.4 0.8 %copy-start.24 = (f32[8,128]{1,0:T(8,128)}, f32[8,128]{1,0:T(8,128)S(1)}, u32[]{:S(2)}) copy-start(f32[8,128]{1,0:T(8,128)S(1)} %get-tuple-element.57.refs_12_) | copy-start | bytes 12292
  6.4 0.8 %copy-start.26 = (f32[8,128]{1,0:T(8,128)}, f32[8,128]{1,0:T(8,128)S(1)}, u32[]{:S(2)}) copy-start(f32[8,128]{1,0:T(8,128)S(1)} %get-tuple-element.58.refs_13_) | copy-start | bytes 12292
  6.4 1.4 %copy-start.8 = (bf16[32,2048]{1,0:T(8,128)(2,1)S(1)}, bf16[32,2048]{1,0:T(8,128)(2,1)}, u32[]{:S(2)}) copy-start(bf16[32,2048]{1,0:T(8,128)(2,1)} %refs_0_.2) | copy-start | bytes 393220
  7.2 35.0 %collective-permute-start = (bf16[256,2048]{1,0:T(8,128)(2,1)S(1)}, bf16[256,2048]{1,0:T(8,128)(2,1)S(1)}, u32[]{:S(2)}, u32[]{:S(2)}) collective-permute-start(bf16[256,2048]{1,0:T(8,128)(2,1)S(1)} %shard_map.271.weights), channel_id=1, source_target_pairs={{0,1},{1,0},{2,3},{3,2},{4,5},{5,4},{6,7},{7,6},{8,9},{9,8},{10,11... | collective-permute-start | bytes 3145736 | tf_op jit(solution)/shard_map/ppermute | solution.py:725
  7.8 6.8 %collective-permute-start.2 = (bf16[32,2048]{1,0:T(8,128)(2,1)S(1)}, bf16[32,2048]{1,0:T(8,128)(2,1)}, u32[]{:S(2)}, u32[]{:S(2)}) collective-permute-start(bf16[32,2048]{1,0:T(8,128)(2,1)S(1)} %copy-done.8), channel_id=1, source_target_pairs={{0,2},{1,3},{2,0},{3,1},{4,6},{5,7},{6,4},{7,5},{8,10},{9,11},{10,... | collective-permute-start | bytes 393224 | tf_op jit(solution)/shard_map/ppermute | solution.py:632
  10.5 5.0 %collective-permute-start.1 = (bf16[32,2048]{1,0:T(8,128)(2,1)S(1)}, bf16[32,2048]{1,0:T(8,128)(2,1)}, u32[]{:S(2)}, u32[]{:S(2)}) collective-permute-start(bf16[32,2048]{1,0:T(8,128)(2,1)S(1)} %copy-done.8), channel_id=1, source_target_pairs={{0,1},{1,0},{2,3},{3,2},{4,5},{5,4},{6,7},{7,6},{8,9},{9,8},{10,11... | collective-permute-start | bytes 393224 | tf_op jit(solution)/shard_map/ppermute | solution.py:635
  14.6 1.6 %collective-permute-start.3 = (bf16[32,2048]{1,0:T(8,128)(2,1)}, bf16[32,2048]{1,0:T(8,128)(2,1)S(1)}, u32[]{:S(2)}, u32[]{:S(2)}) collective-permute-start(bf16[32,2048]{1,0:T(8,128)(2,1)} %collective-permute-done.2.refs_2_), channel_id=1, source_target_pairs={{0,1},{1,0},{2,3},{3,2},{4,5},{5,4},{6,7},{7,6},{8,9},{9,8},{10,11... | collective-permute-start | bytes 393224 | tf_op jit(solution)/shard_map/ppermute | solution.py:635
  16.1 0.7 %copy-start.35 = (f32[1,128]{1,0:T(1,128)S(1)}, f32[1,128]{1,0:T(1,128)}, u32[]{:S(2)}) copy-start(f32[1,128]{1,0:T(1,128)} %copy-done.34) | copy-start | bytes 1540
  16.1 0.7 %copy-start.27 = (f32[8,128]{1,0:T(8,128)S(1)}, f32[8,128]{1,0:T(8,128)}, u32[]{:S(2)}) copy-start(f32[8,128]{1,0:T(8,128)} %copy-done.26) | copy-start | bytes 12292
  16.1 0.7 %copy-start.23 = (f32[1,2048]{1,0:T(1,128)S(1)}, f32[1,2048]{1,0:T(1,128)}, u32[]{:S(2)}) copy-start(f32[1,2048]{1,0:T(1,128)} %copy-done.22) | copy-start | bytes 24580
  16.2 0.7 %copy-start.25 = (f32[8,128]{1,0:T(8,128)S(1)}, f32[8,128]{1,0:T(8,128)}, u32[]{:S(2)}) copy-start(f32[8,128]{1,0:T(8,128)} %copy-done.24) | copy-start | bytes 12292
  16.2 0.7 %copy-start.29 = (f32[2,128]{1,0:T(2,128)S(1)}, f32[2,128]{1,0:T(2,128)}, u32[]{:S(2)}) copy-start(f32[2,128]{1,0:T(2,128)} %copy-done.28) | copy-start | bytes 3076
  16.9 1.0 %copy-start.1 = (bf16[2048,128]{1,0:T(8,128)(2,1)S(1)}, bf16[2048,128]{1,0:T(8,128)(2,1)}, u32[]{:S(2)}) copy-start(bf16[2048,128]{1,0:T(8,128)(2,1)} %copy-done) | copy-start | bytes 1572868
  17.9 1.0 %copy-start.3 = (bf16[2048,128]{1,0:T(8,128)(2,1)S(1)}, bf16[2048,128]{1,0:T(8,128)(2,1)}, u32[]{:S(2)}) copy-start(bf16[2048,128]{1,0:T(8,128)(2,1)} %copy-done.2) | copy-start | bytes 1572868
  18.9 0.9 %copy-start.5 = (bf16[64,2048]{1,0:T(8,128)(2,1)S(1)}, bf16[64,2048]{1,0:T(8,128)(2,1)}, u32[]{:S(2)}) copy-start(bf16[64,2048]{1,0:T(8,128)(2,1)} %copy-done.4) | copy-start | bytes 786436
  19.9 0.8 %copy-start.15 = (f32[128,128]{1,0:T(8,128)S(1)}, f32[128,128]{1,0:T(8,128)}, u32[]{:S(2)}) copy-start(f32[128,128]{1,0:T(8,128)} %copy-done.14) | copy-start | bytes 196612
  20.7 0.8 %copy-start.17 = (f32[128,128]{1,0:T(8,128)S(1)}, f32[128,128]{1,0:T(8,128)}, u32[]{:S(2)}) copy-start(f32[128,128]{1,0:T(8,128)} %copy-done.16) | copy-start | bytes 196612
  21.6 2.3 %copy-start.7 = (bf16[64,2048]{1,0:T(8,128)(2,1)S(1)}, bf16[64,2048]{1,0:T(8,128)(2,1)}, u32[]{:S(2)}) copy-start(bf16[64,2048]{1,0:T(8,128)(2,1)} %copy-done.6) | copy-start | bytes 786436
  21.6 2.3 %copy-start.11 = (bf16[256,128]{1,0:T(8,128)(2,1)S(1)}, bf16[256,128]{1,0:T(8,128)(2,1)}, u32[]{:S(2)}) copy-start(bf16[256,128]{1,0:T(8,128)(2,1)} %copy-done.10) | copy-start | bytes 196612
  21.6 2.3 %copy-start.13 = (f32[2,64,128]{2,1,0:T(8,128)S(1)}, f32[2,64,128]{2,1,0:T(8,128)}, u32[]{:S(2)}) copy-start(f32[2,64,128]{2,1,0:T(8,128)} %copy-done.12) | copy-start | bytes 196612
  21.6 2.4 %copy-start.19 = (bf16[64,256]{1,0:T(8,128)(2,1)S(1)}, bf16[64,256]{1,0:T(8,128)(2,1)}, u32[]{:S(2)}) copy-start(bf16[64,256]{1,0:T(8,128)(2,1)} %copy-done.18) | copy-start | bytes 98308
  21.6 2.4 %copy-start.21 = (bf16[128,128]{1,0:T(8,128)(2,1)S(1)}, bf16[128,128]{1,0:T(8,128)(2,1)}, u32[]{:S(2)}) copy-start(bf16[128,128]{1,0:T(8,128)(2,1)} %copy-done.20) | copy-start | bytes 98308
  23.9 0.6 %copy-start.33 = (f32[2,64]{1,0:T(2,128)S(1)}, f32[2,64]{1,0:T(2,128)}, u32[]{:S(2)}) copy-start(f32[2,64]{1,0:T(2,128)} %copy-done.32) | copy-start | bytes 1540
  23.9 0.7 %copy-start.31 = (f32[1,256]{1,0:T(1,128)S(1)}, f32[1,256]{1,0:T(1,128)}, u32[]{:S(2)}) copy-start(f32[1,256]{1,0:T(1,128)} %copy-done.30) | copy-start | bytes 3076
  24.6 6.0 %copy-start.9 = (f32[2,72,128]{2,1,0:T(8,128)S(1)}, f32[2,72,128]{2,1,0:T(8,128)}, u32[]{:S(2)}) copy-start(f32[2,72,128]{2,1,0:T(8,128)} %constant.44.clone.refs_0_) | copy-start | bytes 221188
  26.0 16.2 %collective-permute-start.4 = (bf16[64,2944]{1,0:T(8,128)(2,1)S(1)}, bf16[64,2944]{1,0:T(8,128)(2,1)S(1)}, u32[]{:S(2)}, u32[]{:S(2)}) collective-permute-start(bf16[64,2944]{1,0:T(8,128)(2,1)S(1)} %get-tuple-element.74), channel_id=1, source_target_pairs={{0,1},{1,0},{2,3},{3,2},{4,5},{5,4},{6,7},{7,6},{8,9},{9,8},{10,11... | collective-permute-start | bytes 1130504 | tf_op jit(solution)/shard_map/ppermute | solution.py:726
  26.3 4.3 %collective-permute-start.5 = (bf16[240,128]{1,0:T(8,128)(2,1)S(1)}, bf16[240,128]{1,0:T(8,128)(2,1)S(1)}, u32[]{:S(2)}, u32[]{:S(2)}) collective-permute-start(bf16[240,128]{1,0:T(8,128)(2,1)S(1)} %get-tuple-element.75.refs_1_), channel_id=1, source_target_pairs={{0,4},{4,0},{8,12},{12,8},{16,20},{20,16},{24,28},{28,24},{1,5},{5... | collective-permute-start | bytes 184328 | tf_op jit(solution)/shard_map/ppermute | solution.py:734
  31.8 4.4 %collective-permute-start.6 = (bf16[144,128]{1,0:T(8,128)(2,1)S(1)}, bf16[144,128]{1,0:T(8,128)(2,1)S(1)}, u32[]{:S(2)}, u32[]{:S(2)}) collective-permute-start(bf16[144,128]{1,0:T(8,128)(2,1)S(1)} %get-tuple-element.76.sides), channel_id=1, source_target_pairs={{0,1},{1,0},{2,3},{3,2},{4,5},{5,4},{6,7},{7,6},{8,9},{9,8},{10,11... | collective-permute-start | bytes 110600 | tf_op jit(solution)/shard_map/ppermute | solution.py:761
  31.8 5.0 %collective-permute-start.7 = (bf16[264,128]{1,0:T(8,128)(2,1)S(1)}, bf16[264,128]{1,0:T(8,128)(2,1)S(1)}, u32[]{:S(2)}, u32[]{:S(2)}) collective-permute-start(bf16[264,128]{1,0:T(8,128)(2,1)S(1)} %get-tuple-element.77.refs_3_), channel_id=1, source_target_pairs={{0,8},{4,12},{8,0},{12,4},{16,24},{20,28},{24,16},{28,20},{1,9},{5... | collective-permute-start | bytes 202760 | tf_op jit(solution)/shard_map/ppermute | solution.py:760
  33.6 7.8 %collective-permute-start.8 = (bf16[264,128]{1,0:T(8,128)(2,1)S(1)}, bf16[264,128]{1,0:T(8,128)(2,1)S(1)}, u32[]{:S(2)}, u32[]{:S(2)}) collective-permute-start(bf16[264,128]{1,0:T(8,128)(2,1)S(1)} %get-tuple-element.78), channel_id=1, source_target_pairs={{0,16},{4,20},{8,24},{12,28},{16,0},{20,4},{24,8},{28,12},{1,17},{... | collective-permute-start | bytes 202760 | tf_op jit(solution)/shard_map/ppermute | solution.py:760
  36.2 6.1 %collective-permute-start.9 = (bf16[264,128]{1,0:T(8,128)(2,1)S(1)}, bf16[264,128]{1,0:T(8,128)(2,1)S(1)}, u32[]{:S(2)}, u32[]{:S(2)}) collective-permute-start(bf16[264,128]{1,0:T(8,128)(2,1)S(1)} %get-tuple-element.79), channel_id=1, source_target_pairs={{0,24},{4,28},{8,16},{12,20},{16,8},{20,12},{24,0},{28,4},{1,25},{... | collective-permute-start | bytes 202760 | tf_op jit(solution)/shard_map/ppermute | solution.py:760
  42.3 1.6 %collective-permute-start.10 = (bf16[984,128]{1,0:T(8,128)(2,1)S(1)}, bf16[984,128]{1,0:T(8,128)(2,1)S(1)}, u32[]{:S(2)}, u32[]{:S(2)}) collective-permute-start(bf16[984,128]{1,0:T(8,128)(2,1)S(1)} %shard_map.275.packed), channel_id=1, source_target_pairs={{0,1},{1,0},{2,3},{3,2},{4,5},{5,4},{6,7},{7,6},{8,9},{9,8},{10,11... | collective-permute-start | bytes 755720 | tf_op jit(solution)/shard_map/ppermute | solution.py:769
  45.3 5.6 %collective-permute-start.11 = (bf16[32,2048]{1,0:T(8,128)(2,1)S(1)}, bf16[32,2048]{1,0:T(8,128)(2,1)S(1)}, u32[]{:S(2)}, u32[]{:S(2)}) collective-permute-start(bf16[32,2048]{1,0:T(8,128)(2,1)S(1)} %shard_map.278), channel_id=1, source_target_pairs={{0,2},{1,3},{2,0},{3,1},{4,6},{5,7},{6,4},{7,5},{8,10},{9,11},{10,... | collective-permute-start | bytes 393224 | tf_op jit(solution)/shard_map/ppermute | solution.py:812
where the time goes:
time: 52 us; the launch traced here: 51.5 us
  waiting for transfers between devices  15.7 us (30%)
  starting transfers between devices  11.9 us (23%)
  Pallas kernels  11.7 us (22%)
  local copies, waits for them, and re-layouts  10.4 us (20%)
  other arithmetic  1.62 us (3%)
    unnamed x72, local copies, waits for them, and re-layouts  10.4 us
    pallas_call x8, Pallas kernels, call(): pl.pallas_call(kernel, out_shape=[jax.ShapeDtypeStruct(shape, dtype) for...  9.22 us
    ppermute x3, waiting for transfers between devices, shards(): received.append(lax.ppermute(messages[k - 1], 'sp', pairs))  5.45 us
    ppermute x3, starting transfers between devices, shards(): received.append(lax.ppermute(messages[k - 1], 'sp', pairs))  5.03 us
    ppermute x1, waiting for transfers between devices, shards(): gathered.append(lax.ppermute(rows_in, 'tp', ring[k]))  4.04 us
    ppermute x1, starting transfers between devices, shards(): gathered.append(lax.ppermute(rows_in, 'tp', ring[k]))  2.68 us
    ppermute x1, waiting for transfers between devices, shards(): arrived.append(lax.ppermute(piece, 'tp', ring[k]))  2.62 us
    ppermute x1, waiting for transfers between devices, shards(): lax.ppermute(message, 'sp', digit_pairs(peers, strides[level], radix, k))  2.56 us
  transfers between devices with their start and end apart: 12, of which 7 were waited for; matrix products, arithmetic and copies ran while one was open for 2% of the time, Pallas kernels for 15%

commit v1 on v0

--- a/solution.py
+++ b/solution.py
@@ -356,7 +356,7 @@
     own = refs[1]
     received = (own,) + refs[2 : 1 + radix]
     outs = refs[1 + radix :]
-    prefix_out, sides_out, messages = outs[0], outs[1], outs[2:]
+    state_out, messages = outs[0], outs[1:]
     kv_rows = own.shape[0] - 2 * state_rows
 
     def fetch(k, direction):
@@ -367,16 +367,16 @@
     totals = []
     for direction in range(2):
         sign = 1 - 2 * direction
-        inner = placed(read_state(prefix_in[direction]), sign * digit)
+        at = slice(direction * state_rows, (direction + 1) * state_rows)
+        inner = placed(read_state(prefix_in[at, :]), sign * digit)
         before, whole = [inner], [placed(fetch(0, direction), sign * digit)]
         for k in range(1, radix):
             source = peer_digit(digit, radix, k, False)
             state = fetch(k, direction)
             before.append(placed(state, sign * source, sign * source < sign * digit))
             whole.append(placed(state, sign * source))
-        inside = joined(before)
-        prefix_out[direction] = inside
-        sides_out[direction * state_rows : (direction + 1) * state_rows, :] = inside.astype(BF16)
+        at = slice(direction * state_rows, (direction + 1) * state_rows)
+        state_out[at, :] = joined(before).astype(state_out.dtype)
         totals.append(joined(whole).astype(BF16))
     total_f, total_b = totals
     part = kv_rows // 3
@@ -727,7 +727,7 @@
 
     blank = np.zeros((2, state_rows, value_width), np.float32)
     blank[:, key_width + 1] = NEG
-    prefix = jnp.asarray(blank)
+    sides = jnp.asarray(blank.reshape(2 * state_rows, value_width))
     wide = (16 << 20) if peers <= 16 else (40 << 20)
     for level, radix in enumerate(radices[:-1]):
         received = [
@@ -738,7 +738,7 @@
         kv_rows *= radix
         count = radices[-1] - 1 if last else 1
         out_rows = kv_rows + (1 if last else 2) * state_rows
-        prefix, sides, *messages = call(
+        sides, *messages = call(
             functools.partial(
                 merge_kernel,
                 slot=2 + level,
@@ -747,9 +747,9 @@
                 last=last,
                 next_radix=radices[level + 1],
             ),
-            [((2, state_rows, value_width), F32), ((2 * state_rows, value_width), BF16)]
+            [((2 * state_rows, value_width), BF16 if last else F32)]
             + [((out_rows, value_width), BF16)] * max(count, 1),
-            [ids, prefix, message] + received,
+            [ids, sides, message] + received,
             limit=wide,
         )
         message = messages[0]

time: 52 us -> 51.5 us (level)
  Pallas kernels: 11.7 us -> 11.1 us
    pallas_call x8, Pallas kernels: 9.22 us -> 8.6 us  [call(): pl.pallas_call(kernel, out_shape=[jax.ShapeDtypeStruct(shape, dtype) for...]
  transfers between devices with their start and end apart: 12 -> 12, of which waited for: 7 -> 7; matrix products, arithmetic and copies ran while one was open for 2% -> 2% of each run, Pallas kernels for 15% -> 14%
where the time goes in v1:
time: 51.5 us; the launch traced here: 51.1 us
  waiting for transfers between devices  15.7 us (30%)
  starting transfers between devices  12 us (23%)
  Pallas kernels  11.1 us (22%)
  local copies, waits for them, and re-layouts  10.4 us (20%)
  other arithmetic  1.62 us (3%)
    unnamed x72, local copies, waits for them, and re-layouts  10.4 us
    pallas_call x8, Pallas kernels, call(): pl.pallas_call(kernel, out_shape=[jax.ShapeDtypeStruct(shape, dtype) for...  8.6 us
    ppermute x3, waiting for transfers between devices, shards(): received.append(lax.ppermute(messages[k - 1], 'sp', pairs))  5.52 us
    ppermute x3, starting transfers between devices, shards(): received.append(lax.ppermute(messages[k - 1], 'sp', pairs))  5.02 us
    ppermute x1, waiting for transfers between devices, shards(): gathered.append(lax.ppermute(rows_in, 'tp', ring[k]))  4.04 us
    ppermute x1, starting transfers between devices, shards(): gathered.append(lax.ppermute(rows_in, 'tp', ring[k]))  2.68 us
    ppermute x1, waiting for transfers between devices, shards(): arrived.append(lax.ppermute(piece, 'tp', ring[k]))  2.61 us
    ppermute x1, waiting for transfers between devices, shards(): lax.ppermute(message, 'sp', digit_pairs(peers, strides[level], radix, k))  2.56 us
  transfers between devices with their start and end apart: 12, of which 7 were waited for; matrix products, arithmetic and copies ran while one was open for 2% of the time, Pallas kernels for 14%

profile of v1, /device:TPU:0, one launch (start us, length us, event | category | flops | bytes accessed | tf_op | source)
XLA Modules:
  0.0 51.1 jit_solution(6068219817374028483)
XLA Ops:
  0.0 2.5 %load.1 = (f32[1,2048]{1,0:T(1,128)S(1)}, bf16[2048,128]{1,0:T(8,128)(2,1)S(1)}, f32[1,128]{1,0:T(1,128)S(1)}, bf16[64,2048]{1,0:T(8,128)(2,1)S(1)}, bf16[64,204...) custom-call(f32[1,2048]{1,0:T(1,128)} %bitcast.22, ...), custom_call_target="tpu_custom_call" | custom-call | flops 100000000 | bytes 4194304 | tf_op jit(solution)/shard_map/load/pallas_call | solution.py:668
  2.5 0.8 %copy-done = bf16[2048,128]{1,0:T(8,128)(2,1)} copy-done((bf16[2048,128]{1,0:T(8,128)(2,1)}, bf16[2048,128]{1,0:T(8,128)(2,1)S(1)}, u32[]{:S(2)}) %copy-start) | copy-done | bytes 524312
  3.3 0.8 %copy-done.2 = bf16[2048,128]{1,0:T(8,128)(2,1)} copy-done((bf16[2048,128]{1,0:T(8,128)(2,1)}, bf16[2048,128]{1,0:T(8,128)(2,1)S(1)}, u32[]{:S(2)}) %copy-start.2) | copy-done | bytes 524312
  4.1 0.6 %copy-done.28 = f32[2,128]{1,0:T(2,128)} copy-done((f32[2,128]{1,0:T(2,128)}, f32[2,128]{1,0:T(2,128)S(1)}, u32[]{:S(2)}) %copy-start.28) | copy-done | bytes 1048
  4.7 0.6 %copy-done.30 = f32[1,256]{1,0:T(1,128)} copy-done((f32[1,256]{1,0:T(1,128)}, f32[1,256]{1,0:T(1,128)S(1)}, u32[]{:S(2)}) %copy-start.30) | copy-done | bytes 1048
  5.2 0.5 %copy-done.32 = f32[2,64]{1,0:T(2,128)} copy-done((f32[2,64]{1,0:T(2,128)}, f32[2,64]{1,0:T(2,128)S(1)}, u32[]{:S(2)}) %copy-start.32) | copy-done | bytes 536
  5.8 0.6 %copy-done.34 = f32[1,128]{1,0:T(1,128)} copy-done((f32[1,128]{1,0:T(1,128)}, f32[1,128]{1,0:T(1,128)S(1)}, u32[]{:S(2)}) %copy-start.34) | copy-done | bytes 536
  6.5 0.3 shard_map.271.weights
  6.7 0.3 copy-done.4
  7.1 0.1 copy-done.6
  7.2 0.0 copy-done.10
  7.2 0.0 copy-done.16
  7.2 0.0 copy-done.20
  7.2 0.6 %collective-permute-start = (bf16[256,2048]{1,0:T(8,128)(2,1)S(1)}, bf16[256,2048]{1,0:T(8,128)(2,1)S(1)}, u32[]{:S(2)}, u32[]{:S(2)}) collective-permute-start(bf16[256,2048]{1,0:T(8,128)(2,1)S(1)} %shard_map.271.weights), channel_id=1, source_target_pairs={{0,1},{1,0},{2,3},{3,2},{4,5},{5,4},{6,7},{7,6},{8,9},{9,8},{10,11... | collective-permute-start | bytes 3145736 | tf_op jit(solution)/shard_map/ppermute | solution.py:725
  7.8 2.7 %collective-permute-start.2 = (bf16[32,2048]{1,0:T(8,128)(2,1)S(1)}, bf16[32,2048]{1,0:T(8,128)(2,1)}, u32[]{:S(2)}, u32[]{:S(2)}) collective-permute-start(bf16[32,2048]{1,0:T(8,128)(2,1)S(1)} %copy-done.8), channel_id=1, source_target_pairs={{0,2},{1,3},{2,0},{3,1},{4,6},{5,7},{6,4},{7,5},{8,10},{9,11},{10,... | collective-permute-start | bytes 393224 | tf_op jit(solution)/shard_map/ppermute | solution.py:632
  10.5 0.1 collective-permute-start.1
  10.5 4.0 %collective-permute-done.2.refs_2_ = bf16[32,2048]{1,0:T(8,128)(2,1)} collective-permute-done((bf16[32,2048]{1,0:T(8,128)(2,1)S(1)}, bf16[32,2048]{1,0:T(8,128)(2,1)}, u32[]{:S(2)}, u32[]{:S(2)}) %collective-permute-start.2) | collective-permute-done | bytes 131104 | tf_op jit(solution)/shard_map/ppermute | solution.py:632
  14.6 0.9 %and_select_fusion.ids = s32[4]{0:T(128)S(1)} fusion(s32[4]{0:T(128)} %constant.51, s32[4]{0:T(128)} %constant.38.clone, pred[4]{0:T(512)(128)(4,1)} %constant.37.clone, s32[]{:T(128)S(6)} %axis_index.25, s32[]{:T(128)S(6)} %axis_index.22), kind=kLoop, calls=%fused_computation.1 | loop fusion | flops 60 | bytes 60 | tf_op jit(solution)/shard_map/jit(remainder)/select_n | solution.py:625
  15.5 0.6 %collective-permute-done.3.refs_3_ = bf16[32,2048]{1,0:T(8,128)(2,1)S(1)} collective-permute-done((bf16[32,2048]{1,0:T(8,128)(2,1)}, bf16[32,2048]{1,0:T(8,128)(2,1)S(1)}, u32[]{:S(2)}, u32[]{:S(2)}) %collective-permute-start.3) | collective-permute-done | bytes 131104 | tf_op jit(solution)/shard_map/ppermute | solution.py:635
  16.2 0.7 %copy-done.35 = f32[1,128]{1,0:T(1,128)S(1)} copy-done((f32[1,128]{1,0:T(1,128)S(1)}, f32[1,128]{1,0:T(1,128)}, u32[]{:S(2)}) %copy-start.35) | copy-done | bytes 536
  16.8 0.0 copy-done.23
  16.9 1.0 %copy-done.1 = bf16[2048,128]{1,0:T(8,128)(2,1)S(1)} copy-done((bf16[2048,128]{1,0:T(8,128)(2,1)S(1)}, bf16[2048,128]{1,0:T(8,128)(2,1)}, u32[]{:S(2)}) %copy-start.1) | copy-done | bytes 524312
  17.9 1.0 %copy-done.3 = bf16[2048,128]{1,0:T(8,128)(2,1)S(1)} copy-done((bf16[2048,128]{1,0:T(8,128)(2,1)S(1)}, bf16[2048,128]{1,0:T(8,128)(2,1)}, u32[]{:S(2)}) %copy-start.3) | copy-done | bytes 524312
  18.9 0.9 %copy-done.5 = bf16[64,2048]{1,0:T(8,128)(2,1)S(1)} copy-done((bf16[64,2048]{1,0:T(8,128)(2,1)S(1)}, bf16[64,2048]{1,0:T(8,128)(2,1)}, u32[]{:S(2)}) %copy-start.5) | copy-done | bytes 262168
  19.9 0.8 %copy-done.15 = f32[128,128]{1,0:T(8,128)S(1)} copy-done((f32[128,128]{1,0:T(8,128)S(1)}, f32[128,128]{1,0:T(8,128)}, u32[]{:S(2)}) %copy-start.15) | copy-done | bytes 65560
  20.7 0.8 %copy-done.17 = f32[128,128]{1,0:T(8,128)S(1)} copy-done((f32[128,128]{1,0:T(8,128)S(1)}, f32[128,128]{1,0:T(8,128)}, u32[]{:S(2)}) %copy-start.17) | copy-done | bytes 65560
  21.6 2.3 %shard_map.272 = (bf16[240,128]{1,0:T(8,128)(2,1)S(1)}, bf16[128,2048]{1,0:T(8,128)(2,1)S(1)}, bf16[128,128]{1,0:T(8,128)(2,1)S(1)}, bf16[128,128]{1,0:T(8,128)(...) custom-call(s32[4]{0:T(128)S(1)} %and_select_fusion.ids, bf16[32,2048]{1,0:T(8,128)(2,1)S(1)} %copy-done.8, ...), custom_call_target="tpu_custom_call" | custom-call | tf_op jit(solution)/shard_map/pallas_call | solution.py:579
  24.0 0.6 %copy-done.33 = f32[2,64]{1,0:T(2,128)S(1)} copy-done((f32[2,64]{1,0:T(2,128)S(1)}, f32[2,64]{1,0:T(2,128)}, u32[]{:S(2)}) %copy-start.33) | copy-done | bytes 536
  24.5 0.0 copy-done.31
  24.6 1.5 %shard_map.273 = (bf16[64,2944]{1,0:T(8,128)(2,1)S(1)}, bf16[64,2944]{1,0:T(8,128)(2,1)S(1)}) custom-call(s32[4]{0:T(128)S(1)} %and_select_fusion.ids, bf16[128,2048]{1,0:T(8,128)(2,1)S(1)} %get-tuple-element.61.normed_ref, bf16[128,128]{1,0:T(8,128)(2,1)S(1)} %get-tuple-element.62.keys_ref, bf16[128,128]{1,0:T(8,128)(2,1)S(1)} %get-tuple-element.63.values_ref, ...), custom_call_target="tpu_custom_call" | custom-call | flops 100000000 | bytes 1048576 | tf_op jit(solution)/shard_map/pallas_call | solution.py:579
  26.0 0.2 collective-permute-start.4
  26.3 1.7 %collective-permute-start.5 = (bf16[240,128]{1,0:T(8,128)(2,1)S(1)}, bf16[240,128]{1,0:T(8,128)(2,1)S(1)}, u32[]{:S(2)}, u32[]{:S(2)}) collective-permute-start(bf16[240,128]{1,0:T(8,128)(2,1)S(1)} %get-tuple-element.75.refs_1_), channel_id=1, source_target_pairs={{0,4},{4,0},{8,12},{12,8},{16,20},{20,16},{24,28},{28,24},{1,5},{5... | collective-permute-start | bytes 184328 | tf_op jit(solution)/shard_map/ppermute | solution.py:734
  28.0 2.6 %collective-permute-done.5.refs_2_ = bf16[240,128]{1,0:T(8,128)(2,1)S(1)} collective-permute-done((bf16[240,128]{1,0:T(8,128)(2,1)S(1)}, bf16[240,128]{1,0:T(8,128)(2,1)S(1)}, u32[]{:S(2)}, u32[]{:S(2)}) %collective-permute-start.5) | collective-permute-done | bytes 61472 | tf_op jit(solution)/shard_map/ppermute | solution.py:734
  30.5 0.6 %shard_map.274 = (bf16[144,128]{1,0:T(8,128)(2,1)S(1)}, bf16[264,128]{1,0:T(8,128)(2,1)S(1)}, bf16[264,128]{1,0:T(8,128)(2,1)S(1)}, bf16[264,128]{1,0:T(8,128)(2,1)S(1)}) custom-call(s32[4]{0:T(128)S(1)} %and_select_fusion.ids, f32[144,128]{1,0:T(8,128)S(1)} %copy-done.9, bf16[240,128]{1,0:T(8,128)(2,1)S(1)} %get-tuple-element.75.refs_1_, ...), custom_call_target="tpu_custom_call" | custom-call | tf_op jit(solution)/shard_map/pallas_call | solution.py:579
  31.1 0.1 collective-permute-start.6
  31.2 1.9 %collective-permute-start.7 = (bf16[264,128]{1,0:T(8,128)(2,1)S(1)}, bf16[264,128]{1,0:T(8,128)(2,1)S(1)}, u32[]{:S(2)}, u32[]{:S(2)}) collective-permute-start(bf16[264,128]{1,0:T(8,128)(2,1)S(1)} %get-tuple-element.77.refs_3_), channel_id=1, source_target_pairs={{0,8},{4,12},{8,0},{12,4},{16,24},{20,28},{24,16},{28,20},{1,9},{5... | collective-permute-start | bytes 202760 | tf_op jit(solution)/shard_map/ppermute | solution.py:760
  33.1 2.6 %collective-permute-start.8 = (bf16[264,128]{1,0:T(8,128)(2,1)S(1)}, bf16[264,128]{1,0:T(8,128)(2,1)S(1)}, u32[]{:S(2)}, u32[]{:S(2)}) collective-permute-start(bf16[264,128]{1,0:T(8,128)(2,1)S(1)} %get-tuple-element.78), channel_id=1, source_target_pairs={{0,16},{4,20},{8,24},{12,28},{16,0},{20,4},{24,8},{28,12},{1,17},{... | collective-permute-start | bytes 202760 | tf_op jit(solution)/shard_map/ppermute | solution.py:760
  35.7 0.6 %collective-permute-start.9 = (bf16[264,128]{1,0:T(8,128)(2,1)S(1)}, bf16[264,128]{1,0:T(8,128)(2,1)S(1)}, u32[]{:S(2)}, u32[]{:S(2)}) collective-permute-start(bf16[264,128]{1,0:T(8,128)(2,1)S(1)} %get-tuple-element.79), channel_id=1, source_target_pairs={{0,24},{4,28},{8,16},{12,20},{16,8},{20,12},{24,0},{28,4},{1,25},{... | collective-permute-start | bytes 202760 | tf_op jit(solution)/shard_map/ppermute | solution.py:760
  36.3 4.6 %collective-permute-done.8.refs_5_ = bf16[264,128]{1,0:T(8,128)(2,1)S(1)} collective-permute-done((bf16[264,128]{1,0:T(8,128)(2,1)S(1)}, bf16[264,128]{1,0:T(8,128)(2,1)S(1)}, u32[]{:S(2)}, u32[]{:S(2)}) %collective-permute-start.8) | collective-permute-done | bytes 67616 | tf_op jit(solution)/shard_map/ppermute | solution.py:760
  40.9 0.9 %collective-permute-done.9.refs_6_ = bf16[264,128]{1,0:T(8,128)(2,1)S(1)} collective-permute-done((bf16[264,128]{1,0:T(8,128)(2,1)S(1)}, bf16[264,128]{1,0:T(8,128)(2,1)S(1)}, u32[]{:S(2)}, u32[]{:S(2)}) %collective-permute-start.9) | collective-permute-done | bytes 67616 | tf_op jit(solution)/shard_map/ppermute | solution.py:760
  41.8 0.1 collective-permute-start.10
  41.9 1.1 %shard_map.276 = (bf16[64,128]{1,0:T(8,128)(2,1)S(1)}, f32[128,128]{1,0:T(8,128)S(1)}, f32[128,128]{1,0:T(8,128)S(1)}, f32[128,128]{1,0:T(8,128)S(1)}) custom-call(s32[4]{0:T(128)S(1)} %and_select_fusion.ids, bf16[984,128]{1,0:T(8,128)(2,1)S(1)} %shard_map.275.packed, bf16[144,128]{1,0:T(8,128)(2,1)S(1)} %get-tuple-element.76.sides, ...), custom_call_target="tpu_custom_call" | custom-call | flops 100000000 | bytes 1048576 | tf_op jit(solution)/shard_map/pallas_call | solution.py:579
  43.0 0.4 collective-permute-done.10.swapped
  43.4 1.4 %shard_map.278 = bf16[32,2048]{1,0:T(8,128)(2,1)S(1)} custom-call(s32[4]{0:T(128)S(1)} %and_select_fusion.ids, bf16[984,128]{1,0:T(8,128)(2,1)S(1)} %collective-permute-done.10.swapped, bf16[144,128]{1,0:T(8,128)(2,1)S(1)} %collective-permute-done.6.refs_2_.sides, bf16[64,2944]{1,0:T(8,128)(2,1)S(1)} %get-tuple-element.80.kept, ...), custom_call_target="tpu_custom_call" | custom-call | flops 100000000 | bytes 1048576 | tf_op jit(solution)/shard_map/pallas_call | solution.py:579
  44.8 1.6 %collective-permute-start.11 = (bf16[32,2048]{1,0:T(8,128)(2,1)S(1)}, bf16[32,2048]{1,0:T(8,128)(2,1)S(1)}, u32[]{:S(2)}, u32[]{:S(2)}) collective-permute-start(bf16[32,2048]{1,0:T(8,128)(2,1)S(1)} %shard_map.278), channel_id=1, source_target_pairs={{0,2},{1,3},{2,0},{3,1},{4,6},{5,7},{6,4},{7,5},{8,10},{9,11},{10,... | collective-permute-start | bytes 393224 | tf_op jit(solution)/shard_map/ppermute | solution.py:812
  46.4 1.4 %shard_map.277 = f32[32,2048]{1,0:T(8,128)S(1)} custom-call(s32[4]{0:T(128)S(1)} %and_select_fusion.ids, bf16[984,128]{1,0:T(8,128)(2,1)S(1)} %collective-permute-done.10.swapped, bf16[144,128]{1,0:T(8,128)(2,1)S(1)} %collective-permute-done.6.refs_2_.sides, bf16[64,2944]{1,0:T(8,128)(2,1)S(1)} %get-tuple-element.80.kept, ...), custom_call_target="tpu_custom_call" | custom-call | flops 100000000 | bytes 1048576 | tf_op jit(solution)/shard_map/pallas_call | solution.py:579
  47.8 2.6 %collective-permute-done.11 = bf16[32,2048]{1,0:T(8,128)(2,1)S(1)} collective-permute-done((bf16[32,2048]{1,0:T(8,128)(2,1)S(1)}, bf16[32,2048]{1,0:T(8,128)(2,1)S(1)}, u32[]{:S(2)}, u32[]{:S(2)}) %collective-permute-start.11) | collective-permute-done | bytes 131104 | tf_op jit(solution)/shard_map/ppermute | solution.py:812
  50.4 0.7 %add_convert_fusion = bf16[32,2048]{1,0:T(8,128)(2,1)} fusion(f32[32,2048]{1,0:T(8,128)S(1)} %shard_map.277, bf16[32,2048]{1,0:T(8,128)(2,1)S(1)} %collective-permute-done.11), kind=kLoop, calls=%fused_computation | loop fusion | flops 196608 | bytes 524288 | tf_op jit(solution)/shard_map/convert_element_type | solution.py:816
  (59 shorter events, 0.1 us)
Async XLA Ops:
  2.5 0.8 %copy-start = (bf16[2048,128]{1,0:T(8,128)(2,1)}, bf16[2048,128]{1,0:T(8,128)(2,1)S(1)}, u32[]{:S(2)}) copy-start(bf16[2048,128]{1,0:T(8,128)(2,1)S(1)} %get-tuple-element.50.refs_5_) | copy-start | bytes 1572868
  3.3 0.8 %copy-start.2 = (bf16[2048,128]{1,0:T(8,128)(2,1)}, bf16[2048,128]{1,0:T(8,128)(2,1)S(1)}, u32[]{:S(2)}) copy-start(bf16[2048,128]{1,0:T(8,128)(2,1)S(1)} %get-tuple-element.54.refs_9_) | copy-start | bytes 1572868
  4.1 0.6 %copy-start.28 = (f32[2,128]{1,0:T(2,128)}, f32[2,128]{1,0:T(2,128)S(1)}, u32[]{:S(2)}) copy-start(f32[2,128]{1,0:T(2,128)S(1)} %get-tuple-element.56.refs_11_) | copy-start | bytes 3076
  4.7 0.6 %copy-start.30 = (f32[1,256]{1,0:T(1,128)}, f32[1,256]{1,0:T(1,128)S(1)}, u32[]{:S(2)}) copy-start(f32[1,256]{1,0:T(1,128)S(1)} %get-tuple-element.67.query_gain) | copy-start | bytes 3076
  5.2 0.5 %copy-start.32 = (f32[2,64]{1,0:T(2,128)}, f32[2,64]{1,0:T(2,128)S(1)}, u32[]{:S(2)}) copy-start(f32[2,64]{1,0:T(2,128)S(1)} %get-tuple-element.73.init_norm) | copy-start | bytes 1540
  5.8 0.6 %copy-start.34 = (f32[1,128]{1,0:T(1,128)}, f32[1,128]{1,0:T(1,128)S(1)}, u32[]{:S(2)}) copy-start(f32[1,128]{1,0:T(1,128)S(1)} %get-tuple-element.51.refs_6_) | copy-start | bytes 1540
  6.4 0.7 %copy-start.4 = (bf16[64,2048]{1,0:T(8,128)(2,1)}, bf16[64,2048]{1,0:T(8,128)(2,1)S(1)}, u32[]{:S(2)}) copy-start(bf16[64,2048]{1,0:T(8,128)(2,1)S(1)} %get-tuple-element.53.refs_8_) | copy-start | bytes 786436
  6.4 0.8 %copy-start.6 = (bf16[64,2048]{1,0:T(8,128)(2,1)}, bf16[64,2048]{1,0:T(8,128)(2,1)S(1)}, u32[]{:S(2)}) copy-start(bf16[64,2048]{1,0:T(8,128)(2,1)S(1)} %get-tuple-element.71.rec_query_t) | copy-start | bytes 786436
  6.4 0.8 %copy-start.10 = (bf16[256,128]{1,0:T(8,128)(2,1)}, bf16[256,128]{1,0:T(8,128)(2,1)S(1)}, u32[]{:S(2)}) copy-start(bf16[256,128]{1,0:T(8,128)(2,1)S(1)} %get-tuple-element.68.nope_up) | copy-start | bytes 196612
  6.4 0.8 %copy-start.12 = (f32[2,64,128]{2,1,0:T(8,128)}, f32[2,64,128]{2,1,0:T(8,128)S(1)}, u32[]{:S(2)}) copy-start(f32[2,64,128]{2,1,0:T(8,128)S(1)} %get-tuple-element.72.init_state) | copy-start | bytes 196612
  6.4 0.8 %copy-start.14 = (f32[128,128]{1,0:T(8,128)}, f32[128,128]{1,0:T(8,128)S(1)}, u32[]{:S(2)}) copy-start(f32[128,128]{1,0:T(8,128)S(1)} %get-tuple-element.59.refs_14_) | copy-start | bytes 196612
  6.4 0.8 %copy-start.16 = (f32[128,128]{1,0:T(8,128)}, f32[128,128]{1,0:T(8,128)S(1)}, u32[]{:S(2)}) copy-start(f32[128,128]{1,0:T(8,128)S(1)} %get-tuple-element.60.refs_15_) | copy-start | bytes 196612
  6.4 0.8 %copy-start.18 = (bf16[64,256]{1,0:T(8,128)(2,1)}, bf16[64,256]{1,0:T(8,128)(2,1)S(1)}, u32[]{:S(2)}) copy-start(bf16[64,256]{1,0:T(8,128)(2,1)S(1)} %get-tuple-element.69.rope_up_t) | copy-start | bytes 98308
  6.4 0.8 %copy-start.20 = (bf16[128,128]{1,0:T(8,128)(2,1)}, bf16[128,128]{1,0:T(8,128)(2,1)S(1)}, u32[]{:S(2)}) copy-start(bf16[128,128]{1,0:T(8,128)(2,1)S(1)} %get-tuple-element.70.key_up) | copy-start | bytes 98308
  6.4 0.8 %copy-start.22 = (f32[1,2048]{1,0:T(1,128)}, f32[1,2048]{1,0:T(1,128)S(1)}, u32[]{:S(2)}) copy-start(f32[1,2048]{1,0:T(1,128)S(1)} %get-tuple-element.49.refs_4_) | copy-start | bytes 24580
  6.4 0.8 %copy-start.24 = (f32[8,128]{1,0:T(8,128)}, f32[8,128]{1,0:T(8,128)S(1)}, u32[]{:S(2)}) copy-start(f32[8,128]{1,0:T(8,128)S(1)} %get-tuple-element.57.refs_12_) | copy-start | bytes 12292
  6.4 0.8 %copy-start.26 = (f32[8,128]{1,0:T(8,128)}, f32[8,128]{1,0:T(8,128)S(1)}, u32[]{:S(2)}) copy-start(f32[8,128]{1,0:T(8,128)S(1)} %get-tuple-element.58.refs_13_) | copy-start | bytes 12292
  6.4 1.4 %copy-start.8 = (bf16[32,2048]{1,0:T(8,128)(2,1)S(1)}, bf16[32,2048]{1,0:T(8,128)(2,1)}, u32[]{:S(2)}) copy-start(bf16[32,2048]{1,0:T(8,128)(2,1)} %refs_0_.2) | copy-start | bytes 393220
  7.2 34.5 %collective-permute-start = (bf16[256,2048]{1,0:T(8,128)(2,1)S(1)}, bf16[256,2048]{1,0:T(8,128)(2,1)S(1)}, u32[]{:S(2)}, u32[]{:S(2)}) collective-permute-start(bf16[256,2048]{1,0:T(8,128)(2,1)S(1)} %shard_map.271.weights), channel_id=1, source_target_pairs={{0,1},{1,0},{2,3},{3,2},{4,5},{5,4},{6,7},{7,6},{8,9},{9,8},{10,11... | collective-permute-start | bytes 3145736 | tf_op jit(solution)/shard_map/ppermute | solution.py:725
  7.8 6.8 %collective-permute-start.2 = (bf16[32,2048]{1,0:T(8,128)(2,1)S(1)}, bf16[32,2048]{1,0:T(8,128)(2,1)}, u32[]{:S(2)}, u32[]{:S(2)}) collective-permute-start(bf16[32,2048]{1,0:T(8,128)(2,1)S(1)} %copy-done.8), channel_id=1, source_target_pairs={{0,2},{1,3},{2,0},{3,1},{4,6},{5,7},{6,4},{7,5},{8,10},{9,11},{10,... | collective-permute-start | bytes 393224 | tf_op jit(solution)/shard_map/ppermute | solution.py:632
  10.5 5.0 %collective-permute-start.1 = (bf16[32,2048]{1,0:T(8,128)(2,1)S(1)}, bf16[32,2048]{1,0:T(8,128)(2,1)}, u32[]{:S(2)}, u32[]{:S(2)}) collective-permute-start(bf16[32,2048]{1,0:T(8,128)(2,1)S(1)} %copy-done.8), channel_id=1, source_target_pairs={{0,1},{1,0},{2,3},{3,2},{4,5},{5,4},{6,7},{7,6},{8,9},{9,8},{10,11... | collective-permute-start | bytes 393224 | tf_op jit(solution)/shard_map/ppermute | solution.py:635
  14.6 1.6 %collective-permute-start.3 = (bf16[32,2048]{1,0:T(8,128)(2,1)}, bf16[32,2048]{1,0:T(8,128)(2,1)S(1)}, u32[]{:S(2)}, u32[]{:S(2)}) collective-permute-start(bf16[32,2048]{1,0:T(8,128)(2,1)} %collective-permute-done.2.refs_2_), channel_id=1, source_target_pairs={{0,1},{1,0},{2,3},{3,2},{4,5},{5,4},{6,7},{7,6},{8,9},{9,8},{10,11... | collective-permute-start | bytes 393224 | tf_op jit(solution)/shard_map/ppermute | solution.py:635
  16.1 0.7 %copy-start.35 = (f32[1,128]{1,0:T(1,128)S(1)}, f32[1,128]{1,0:T(1,128)}, u32[]{:S(2)}) copy-start(f32[1,128]{1,0:T(1,128)} %copy-done.34) | copy-start | bytes 1540
  16.1 0.7 %copy-start.27 = (f32[8,128]{1,0:T(8,128)S(1)}, f32[8,128]{1,0:T(8,128)}, u32[]{:S(2)}) copy-start(f32[8,128]{1,0:T(8,128)} %copy-done.26) | copy-start | bytes 12292
  16.1 0.7 %copy-start.23 = (f32[1,2048]{1,0:T(1,128)S(1)}, f32[1,2048]{1,0:T(1,128)}, u32[]{:S(2)}) copy-start(f32[1,2048]{1,0:T(1,128)} %copy-done.22) | copy-start | bytes 24580
  16.2 0.7 %copy-start.25 = (f32[8,128]{1,0:T(8,128)S(1)}, f32[8,128]{1,0:T(8,128)}, u32[]{:S(2)}) copy-start(f32[8,128]{1,0:T(8,128)} %copy-done.24) | copy-start | bytes 12292
  16.2 0.7 %copy-start.29 = (f32[2,128]{1,0:T(2,128)S(1)}, f32[2,128]{1,0:T(2,128)}, u32[]{:S(2)}) copy-start(f32[2,128]{1,0:T(2,128)} %copy-done.28) | copy-start | bytes 3076
  16.9 1.0 %copy-start.1 = (bf16[2048,128]{1,0:T(8,128)(2,1)S(1)}, bf16[2048,128]{1,0:T(8,128)(2,1)}, u32[]{:S(2)}) copy-start(bf16[2048,128]{1,0:T(8,128)(2,1)} %copy-done) | copy-start | bytes 1572868
  17.9 1.0 %copy-start.3 = (bf16[2048,128]{1,0:T(8,128)(2,1)S(1)}, bf16[2048,128]{1,0:T(8,128)(2,1)}, u32[]{:S(2)}) copy-start(bf16[2048,128]{1,0:T(8,128)(2,1)} %copy-done.2) | copy-start | bytes 1572868
  18.9 0.9 %copy-start.5 = (bf16[64,2048]{1,0:T(8,128)(2,1)S(1)}, bf16[64,2048]{1,0:T(8,128)(2,1)}, u32[]{:S(2)}) copy-start(bf16[64,2048]{1,0:T(8,128)(2,1)} %copy-done.4) | copy-start | bytes 786436
  19.9 0.8 %copy-start.15 = (f32[128,128]{1,0:T(8,128)S(1)}, f32[128,128]{1,0:T(8,128)}, u32[]{:S(2)}) copy-start(f32[128,128]{1,0:T(8,128)} %copy-done.14) | copy-start | bytes 196612
  20.7 0.8 %copy-start.17 = (f32[128,128]{1,0:T(8,128)S(1)}, f32[128,128]{1,0:T(8,128)}, u32[]{:S(2)}) copy-start(f32[128,128]{1,0:T(8,128)} %copy-done.16) | copy-start | bytes 196612
  21.6 2.3 %copy-start.7 = (bf16[64,2048]{1,0:T(8,128)(2,1)S(1)}, bf16[64,2048]{1,0:T(8,128)(2,1)}, u32[]{:S(2)}) copy-start(bf16[64,2048]{1,0:T(8,128)(2,1)} %copy-done.6) | copy-start | bytes 786436
  21.6 2.3 %copy-start.11 = (bf16[256,128]{1,0:T(8,128)(2,1)S(1)}, bf16[256,128]{1,0:T(8,128)(2,1)}, u32[]{:S(2)}) copy-start(bf16[256,128]{1,0:T(8,128)(2,1)} %copy-done.10) | copy-start | bytes 196612
  21.6 2.3 %copy-start.13 = (f32[2,64,128]{2,1,0:T(8,128)S(1)}, f32[2,64,128]{2,1,0:T(8,128)}, u32[]{:S(2)}) copy-start(f32[2,64,128]{2,1,0:T(8,128)} %copy-done.12) | copy-start | bytes 196612
  21.6 2.4 %copy-start.19 = (bf16[64,256]{1,0:T(8,128)(2,1)S(1)}, bf16[64,256]{1,0:T(8,128)(2,1)}, u32[]{:S(2)}) copy-start(bf16[64,256]{1,0:T(8,128)(2,1)} %copy-done.18) | copy-start | bytes 98308
  21.6 2.4 %copy-start.21 = (bf16[128,128]{1,0:T(8,128)(2,1)S(1)}, bf16[128,128]{1,0:T(8,128)(2,1)}, u32[]{:S(2)}) copy-start(bf16[128,128]{1,0:T(8,128)(2,1)} %copy-done.20) | copy-start | bytes 98308
  23.9 0.6 %copy-start.33 = (f32[2,64]{1,0:T(2,128)S(1)}, f32[2,64]{1,0:T(2,128)}, u32[]{:S(2)}) copy-start(f32[2,64]{1,0:T(2,128)} %copy-done.32) | copy-start | bytes 1540
  23.9 0.7 %copy-start.31 = (f32[1,256]{1,0:T(1,128)S(1)}, f32[1,256]{1,0:T(1,128)}, u32[]{:S(2)}) copy-start(f32[1,256]{1,0:T(1,128)} %copy-done.30) | copy-start | bytes 3076
  24.6 6.0 %copy-start.9 = (f32[144,128]{1,0:T(8,128)S(1)}, f32[144,128]{1,0:T(8,128)}, u32[]{:S(2)}) copy-start(f32[144,128]{1,0:T(8,128)} %constant.44.clone.refs_0_) | copy-start | bytes 221188
  26.0 15.7 %collective-permute-start.4 = (bf16[64,2944]{1,0:T(8,128)(2,1)S(1)}, bf16[64,2944]{1,0:T(8,128)(2,1)S(1)}, u32[]{:S(2)}, u32[]{:S(2)}) collective-permute-start(bf16[64,2944]{1,0:T(8,128)(2,1)S(1)} %get-tuple-element.74), channel_id=1, source_target_pairs={{0,1},{1,0},{2,3},{3,2},{4,5},{5,4},{6,7},{7,6},{8,9},{9,8},{10,11... | collective-permute-start | bytes 1130504 | tf_op jit(solution)/shard_map/ppermute | solution.py:726
  26.3 4.3 %collective-permute-start.5 = (bf16[240,128]{1,0:T(8,128)(2,1)S(1)}, bf16[240,128]{1,0:T(8,128)(2,1)S(1)}, u32[]{:S(2)}, u32[]{:S(2)}) collective-permute-start(bf16[240,128]{1,0:T(8,128)(2,1)S(1)} %get-tuple-element.75.refs_1_), channel_id=1, source_target_pairs={{0,4},{4,0},{8,12},{12,8},{16,20},{20,16},{24,28},{28,24},{1,5},{5... | collective-permute-start | bytes 184328 | tf_op jit(solution)/shard_map/ppermute | solution.py:734
  31.1 4.5 %collective-permute-start.6 = (bf16[144,128]{1,0:T(8,128)(2,1)S(1)}, bf16[144,128]{1,0:T(8,128)(2,1)S(1)}, u32[]{:S(2)}, u32[]{:S(2)}) collective-permute-start(bf16[144,128]{1,0:T(8,128)(2,1)S(1)} %get-tuple-element.76.sides), channel_id=1, source_target_pairs={{0,1},{1,0},{2,3},{3,2},{4,5},{5,4},{6,7},{7,6},{8,9},{9,8},{10,11... | collective-permute-start | bytes 110600 | tf_op jit(solution)/shard_map/ppermute | solution.py:761
  31.2 5.0 %collective-permute-start.7 = (bf16[264,128]{1,0:T(8,128)(2,1)S(1)}, bf16[264,128]{1,0:T(8,128)(2,1)S(1)}, u32[]{:S(2)}, u32[]{:S(2)}) collective-permute-start(bf16[264,128]{1,0:T(8,128)(2,1)S(1)} %get-tuple-element.77.refs_3_), channel_id=1, source_target_pairs={{0,8},{4,12},{8,0},{12,4},{16,24},{20,28},{24,16},{28,20},{1,9},{5... | collective-permute-start | bytes 202760 | tf_op jit(solution)/shard_map/ppermute | solution.py:760
  33.1 7.8 %collective-permute-start.8 = (bf16[264,128]{1,0:T(8,128)(2,1)S(1)}, bf16[264,128]{1,0:T(8,128)(2,1)S(1)}, u32[]{:S(2)}, u32[]{:S(2)}) collective-permute-start(bf16[264,128]{1,0:T(8,128)(2,1)S(1)} %get-tuple-element.78), channel_id=1, source_target_pairs={{0,16},{4,20},{8,24},{12,28},{16,0},{20,4},{24,8},{28,12},{1,17},{... | collective-permute-start | bytes 202760 | tf_op jit(solution)/shard_map/ppermute | solution.py:760
  35.7 6.1 %collective-permute-start.9 = (bf16[264,128]{1,0:T(8,128)(2,1)S(1)}, bf16[264,128]{1,0:T(8,128)(2,1)S(1)}, u32[]{:S(2)}, u32[]{:S(2)}) collective-permute-start(bf16[264,128]{1,0:T(8,128)(2,1)S(1)} %get-tuple-element.79), channel_id=1, source_target_pairs={{0,24},{4,28},{8,16},{12,20},{16,8},{20,12},{24,0},{28,4},{1,25},{... | collective-permute-start | bytes 202760 | tf_op jit(solution)/shard_map/ppermute | solution.py:760
  41.8 1.6 %collective-permute-start.10 = (bf16[984,128]{1,0:T(8,128)(2,1)S(1)}, bf16[984,128]{1,0:T(8,128)(2,1)S(1)}, u32[]{:S(2)}, u32[]{:S(2)}) collective-permute-start(bf16[984,128]{1,0:T(8,128)(2,1)S(1)} %shard_map.275.packed), channel_id=1, source_target_pairs={{0,1},{1,0},{2,3},{3,2},{4,5},{5,4},{6,7},{7,6},{8,9},{9,8},{10,11... | collective-permute-start | bytes 755720 | tf_op jit(solution)/shard_map/ppermute | solution.py:769
  44.8 5.6 %collective-permute-start.11 = (bf16[32,2048]{1,0:T(8,128)(2,1)S(1)}, bf16[32,2048]{1,0:T(8,128)(2,1)S(1)}, u32[]{:S(2)}, u32[]{:S(2)}) collective-permute-start(bf16[32,2048]{1,0:T(8,128)(2,1)S(1)} %shard_map.278), channel_id=1, source_target_pairs={{0,2},{1,3},{2,0},{3,1},{4,6},{5,7},{6,4},{7,5},{8,10},{9,11},{10,... | collective-permute-start | bytes 393224 | tf_op jit(solution)/shard_map/ppermute | solution.py:812

commit v2 on v1

--- a/solution.py
+++ b/solution.py
@@ -139,13 +139,22 @@
     return jnp.minimum(x, 0.0) - jnp.log(1.0 + jnp.exp(-jnp.abs(x)))
 
 
+def norms_kernel(*refs):
+    pieces, in_gain, out = refs[:-2], refs[-2], refs[-1]
+    step = pieces[0].shape[0]
+    for index, piece in enumerate(pieces):
+        at = slice(index * step, (index + 1) * step)
+        out[at, :] = rms(piece[...].astype(F32), in_gain[...]).astype(BF16)
+
+
 def head_kernel(
     ids,
+    ready,
+    late,
     *refs,
     pieces,
     key_width,
 ):
-    piece_refs = refs[: 2 * pieces]
     (
         in_gain,
         kv_down,
@@ -165,20 +174,21 @@
         values_out,
         rows_out,
         table_out,
-        rows,
-    ) = refs[2 * pieces :]
+    ) = refs
     mine = ids[0]
     pair, core = mine // 2, mine % 2
-    step = piece_refs[0].shape[0]
-    seq = rows.shape[0]
-    for k in range(pieces):
-        source = lax.rem(pair - k + pieces, pieces) * 2
-        rows[pl.ds(pl.multiple_of((source + core) * step, step), step), :] = piece_refs[2 * k][...]
-        rows[pl.ds(pl.multiple_of((source + 1 - core) * step, step), step), :] = piece_refs[
-            2 * k + 1
-        ][...]
-    normed = rms(rows[...].astype(F32), in_gain[...]).astype(BF16)
-    normed_out[...] = normed
+    step = late.shape[0]
+    seq = normed_out.shape[0]
+    last = rms(late[...].astype(F32), in_gain[...]).astype(BF16)
+    for index in range(2 * pieces):
+        source = lax.rem(pair - index // 2 + pieces, pieces) * 2
+        source += core if index % 2 == 0 else 1 - core
+        if index < 2 * pieces - 1:
+            block = ready[index * step : (index + 1) * step, :]
+        else:
+            block = last
+        normed_out[pl.ds(pl.multiple_of(source * step, step), step), :] = block
+    normed = normed_out[...]
     table = angle_table(ids, cos_base, sin_base, cos_row, sin_row)
     table_out[...] = table
     latent = kv_down.shape[1]
@@ -237,10 +247,9 @@
         weight = jnp.exp(logs - peak)
         weights.append((weight, peak, total))
     w_f, w_b = weights[0][0], weights[1][0]
-    c_both = dot_split(jnp.concatenate([keys_t * w_f, keys_t * w_b], axis=0), values)
-    n_both = dot_split(
-        jnp.concatenate([w_f, w_b, jnp.zeros((6, seq), F32)], axis=0), keys.astype(BF16)
-    )
+    c_both = dot(jnp.concatenate([keys_t * w_f, keys_t * w_b], axis=0).astype(BF16), values)
+    sums = jnp.concatenate([w_f, w_b, jnp.zeros((6, seq), F32)], axis=0)
+    n_both = dot(sums.astype(BF16), keys.astype(BF16))
     for index in range(2):
         _, peak, total = weights[index]
         c_part = c_both[index * key_width : (index + 1) * key_width]
@@ -332,13 +341,17 @@
             out[0 : block.shape[0], at : at + lanes] = block
 
 
-def fold_kernel(value_up, head_gain, out_attn, out_rec, out):
+def fold_kernel(value_up, head_gain, out_attn, out_rec, out, ahead):
     rows = value_up.shape[0]
-    out[0:rows, :] = dot(value_up[...], out_attn[...]).astype(BF16)
+    top = dot(value_up[...], out_attn[...]).astype(BF16)
+    out[0:rows, :] = top
     gain = head_gain[...]
     width = gain.shape[1]
     column = jnp.transpose(jnp.broadcast_to(gain, (width, width)))[:, 0:1]
-    out[rows:, :] = (column * out_rec[...].astype(F32)).astype(BF16)
+    bottom = (column * out_rec[...].astype(F32)).astype(BF16)
+    out[rows:, :] = bottom
+    ahead[0:rows, :] = top[:, : ahead.shape[1]]
+    ahead[rows:, :] = bottom[:, : ahead.shape[1]]
 
 
 def level_states(ids, slot, radix, fetch):
@@ -351,11 +364,11 @@
     return forward, backward
 
 
-def merge_kernel(ids, *refs, slot, radix, state_rows, last, next_radix):
-    prefix_in = refs[0]
-    own = refs[1]
-    received = (own,) + refs[2 : 1 + radix]
-    outs = refs[1 + radix :]
+def merge_kernel(ids, *refs, slot, radix, state_rows, start, last, next_radix):
+    carried = 0 if start else 1
+    own = refs[carried]
+    received = (own,) + refs[carried + 1 : carried + radix]
+    outs = refs[carried + radix :]
     state_out, messages = outs[0], outs[1:]
     kv_rows = own.shape[0] - 2 * state_rows
 
@@ -368,7 +381,12 @@
     for direction in range(2):
         sign = 1 - 2 * direction
         at = slice(direction * state_rows, (direction + 1) * state_rows)
-        inner = placed(read_state(prefix_in[at, :]), sign * digit)
+        if start:
+            zero = jnp.zeros((1, own.shape[1]), F32)
+            none = jnp.zeros((state_rows - AUX, own.shape[1]), F32)
+            inner = placed((none, zero, zero + NEG, zero), sign * digit)
+        else:
+            inner = placed(read_state(refs[0][at, :]), sign * digit)
         before, whole = [inner], [placed(fetch(0, direction), sign * digit)]
         for k in range(1, radix):
             source = peer_digit(digit, radix, k, False)
@@ -568,7 +586,29 @@
     )
     mine = jnp.concatenate([attended[:step], recurrent[at, :]], axis=1)
     theirs = jnp.concatenate([attended[step:], other], axis=1)
-    out[...] = (dot(mine, weights[...]) + dot(theirs, other_weights[...])).astype(out.dtype)
+    if piece == 0:
+        out[...] = dot(mine, weights[...]) + dot(theirs, other_weights[...])
+    else:
+        tail = out.shape[1] - 4 * width
+        skip = weights.shape[1] - tail
+        out[:, 0 : 2 * width] = mine
+        out[:, 2 * width : 4 * width] = theirs
+        part = dot(mine, weights[:, skip:]) + dot(theirs, other_weights[:, skip:])
+        out[:, 4 * width :] = part.astype(BF16)
+
+
+def last_kernel(total, *refs):
+    out = refs[-1]
+    split = refs[1].shape[1]
+    rows = refs[1].shape[0]
+    left, right = total[:, :split], total[:, split:]
+    for at in range(0, len(refs) - 1, 3):
+        piece, weights, other_weights = refs[at : at + 3]
+        left = left + dot(piece[:, 0:rows], weights[...])
+        left = left + dot(piece[:, rows : 2 * rows], other_weights[...])
+        right = right + piece[:, 2 * rows :].astype(F32)
+    out[:, :split] = left.astype(BF16)
+    out[:, split:] = right.astype(BF16)
 
 
 def call(kernel, outs, inputs, scratch=(), ids=True, limit=16 << 20, cost=None):
@@ -679,6 +719,13 @@
     head_args, local_args = held[:12], held[12:18]
     value_up, head_gain, init_state, init_norm, out_attn, out_rec = held[18:]
 
+    (ready,) = call(
+        norms_kernel,
+        [((seq - seq // lanes, width), BF16)],
+        row_pieces[:-1] + [held[0]],
+        ids=False,
+        cost=pl.CostEstimate(flops=10**7, bytes_accessed=1 << 20, transcendentals=0),
+    )
     state_rows = key_width + AUX
     kv_rows = seq // 2 + seq // 4
     message, normed, keys, values, gate_rows, table = call(
@@ -691,10 +738,7 @@
             ((8, seq), F32),
             ((seq, 2 * rope), F32),
         ],
-        [ids]
-        + row_pieces
-        + head_args,
-        scratch=[pltpu.VMEM((seq, width), BF16)],
+        [ids, ready, row_pieces[-1]] + head_args,
     )
     columns = 20 * value_width
     assert key_width == seq // 2
@@ -715,19 +759,22 @@
         scratch=[pltpu.VMEM((seq, columns), BF16)],
         cost=pl.CostEstimate(flops=10**8, bytes_accessed=1 << 20, transcendentals=0),
     )
-    (weights,) = call(
+    tail = 3 * width // 8
+    weights, ahead = call(
         fold_kernel,
-        [((2 * value_width, width), BF16)],
+        [((2 * value_width, width), BF16), ((2 * value_width, width - tail), BF16)],
         [value_up, head_gain, out_attn, out_rec],
         ids=False,
         cost=pl.CostEstimate(flops=10**8, bytes_accessed=1 << 20, transcendentals=0),
     )
     other_weights = lax.ppermute(weights, "tp", partner)
+    crossed = []
+    for k in range(1, pieces):
+        there = lax.ppermute(ahead, "tp", ring[k])
+        crossed.append((there, lax.ppermute(there, "tp", partner)))
     shared = lax.ppermute(share, "tp", partner)
 
-    blank = np.zeros((2, state_rows, value_width), np.float32)
-    blank[:, key_width + 1] = NEG
-    sides = jnp.asarray(blank.reshape(2 * state_rows, value_width))
+    carried = []
     wide = (16 << 20) if peers <= 16 else (40 << 20)
     for level, radix in enumerate(radices[:-1]):
         received = [
@@ -744,15 +791,17 @@
                 slot=2 + level,
                 radix=radix,
                 state_rows=state_rows,
+                start=level == 0,
                 last=last,
                 next_radix=radices[level + 1],
             ),
             [((2 * state_rows, value_width), BF16 if last else F32)]
             + [((out_rows, value_width), BF16)] * max(count, 1),
-            [ids, sides, message] + received,
+            [ids, *carried, message] + received,
             limit=wide,
         )
         message = messages[0]
+        carried = [sides]
     level, radix = len(radices) - 1, radices[-1]
     received = []
     for k in range(1, radix):
@@ -783,7 +832,7 @@
     )
     step = seq // lanes
 
-    def mixed(piece, dtype):
+    def mixed(piece, shape, dtype):
         return call(
             functools.partial(
                 mix_kernel,
@@ -791,7 +840,7 @@
                 step=step,
                 **level_facts,
             ),
-            [((step, width), dtype)],
+            [(shape, dtype)],
             [
                 ids,
                 swapped,
@@ -808,12 +857,11 @@
 
     arrived = []
     for k in range(1, pieces):
-        piece = mixed(k, BF16)
-        arrived.append(lax.ppermute(piece, "tp", ring[k]))
-    total = mixed(0, F32)
-    for piece in arrived:
-        total = total + piece.astype(F32)
-    return total.astype(BF16)
+        piece = mixed(k, (step, 4 * value_width + tail), BF16)
+        arrived += [lax.ppermute(piece, "tp", ring[k]), *crossed[k - 1]]
+    total = mixed(0, (step, width), F32)
+    (result,) = call(last_kernel, [((step, width), BF16)], [total] + arrived, ids=False)
+    return result
 
 
 def solution(mesh):

time: 51.5 us -> 65.1 us (1.26)
  waiting for transfers between devices: 15.7 us -> 27.9 us
  Pallas kernels: 11.1 us -> 14.5 us
  local copies, waits for them, and re-layouts: 10.4 us -> 7.85 us
  starting transfers between devices: 12 us -> 13.2 us
  other arithmetic: 1.62 us -> 0.94 us
    ppermute x1, waiting for transfers between devices: 4.04 us -> 18.3 us  [shards(): gathered.append(lax.ppermute(rows_in, 'tp', ring[k]))]
    pallas_call x8 -> x10, Pallas kernels: 8.6 us -> 12.1 us  [call(): pl.pallas_call(kernel, out_shape=[jax.ShapeDtypeStruct(shape, dtype) for...]
    ppermute x1 -> x3, starting transfers between devices: 1.57 us -> 4.25 us  [the longest x1 2.58 us: shards(): there = lax.ppermute(ahead, 'tp', ring[k])]
    ppermute x1, starting transfers between devices: 2.68 us -> 0.09 us  [shards(): gathered.append(lax.ppermute(rows_in, 'tp', ring[k]))]
    unnamed x72 -> x62, local copies, waits for them, and re-layouts: 10.4 us -> 7.85 us
    ppermute x3, waiting for transfers between devices: 5.52 us -> 3.81 us  [shards(): received.append(lax.ppermute(messages[k - 1], 'sp', pairs))]
    ppermute x1, waiting for transfers between devices: 0.01 us -> 1.21 us  [shards(): other_sides = lax.ppermute(sides, 'tp', partner)]
    ppermute x1 -> x3, waiting for transfers between devices: 2.61 us -> 1.56 us  [the longest x1 1.55 us: shards(): arrived += [lax.ppermute(piece, 'tp', ring[k]), *crossed[k - 1]]]
  transfers between devices with their start and end apart: 12 -> 14, of which waited for: 7 -> 8; matrix products, arithmetic and copies ran while one was open for 2% -> 1% of each run, Pallas kernels for 14% -> 14%
where the time goes in v2:
time: 65.1 us; the launch traced here: 64.7 us
  waiting for transfers between devices  27.9 us (43%)
  Pallas kernels  14.5 us (22%)
  starting transfers between devices  13.2 us (20%)
  local copies, waits for them, and re-layouts  7.85 us (12%)
  other arithmetic  0.94 us (1%)
    ppermute x1, waiting for transfers between devices, shards(): gathered.append(lax.ppermute(rows_in, 'tp', ring[k]))  18.3 us
    pallas_call x10, Pallas kernels, call(): pl.pallas_call(kernel, out_shape=[jax.ShapeDtypeStruct(shape, dtype) for...  12.1 us
    unnamed x62, local copies, waits for them, and re-layouts  7.85 us
    ppermute x3, starting transfers between devices, shards(): received.append(lax.ppermute(messages[k - 1], 'sp', pairs))  5.86 us
    ppermute x3, waiting for transfers between devices, shards(): received.append(lax.ppermute(messages[k - 1], 'sp', pairs))  3.81 us
    ppermute x1, waiting for transfers between devices, shards(): lax.ppermute(message, 'sp', digit_pairs(peers, strides[level], radix, k))  2.62 us
    ppermute x1, starting transfers between devices, shards(): there = lax.ppermute(ahead, 'tp', ring[k])  2.58 us
    pallas_call x1, Pallas kernels, shards(): pl.pallas_call(load_kernel, out_shape=[pltpu.VMEM(array.shape, array.dtyp...  2.47 us
  transfers between devices with their start and end apart: 14, of which 8 were waited for; matrix products, arithmetic and copies ran while one was open for 1% of the time, Pallas kernels for 14%

profile of v2, /device:TPU:0, one launch (start us, length us, event | category | flops | bytes accessed | tf_op | source)
XLA Modules:
  0.0 64.7 jit_solution(570409288809398234)
XLA Ops:
  0.0 2.5 %load.1 = (f32[1,2048]{1,0:T(1,128)S(1)}, bf16[2048,128]{1,0:T(8,128)(2,1)S(1)}, f32[1,128]{1,0:T(1,128)S(1)}, bf16[64,2048]{1,0:T(8,128)(2,1)S(1)}, bf16[64,204...) custom-call(f32[1,2048]{1,0:T(1,128)} %bitcast.22, ...), custom_call_target="tpu_custom_call" | custom-call | flops 100000000 | bytes 4194304 | tf_op jit(solution)/shard_map/load/pallas_call | solution.py:708
  2.5 0.8 %copy-done = bf16[2048,128]{1,0:T(8,128)(2,1)} copy-done((bf16[2048,128]{1,0:T(8,128)(2,1)}, bf16[2048,128]{1,0:T(8,128)(2,1)S(1)}, u32[]{:S(2)}) %copy-start) | copy-done | bytes 524312
  3.3 0.8 %copy-done.2 = bf16[2048,128]{1,0:T(8,128)(2,1)} copy-done((bf16[2048,128]{1,0:T(8,128)(2,1)}, bf16[2048,128]{1,0:T(8,128)(2,1)S(1)}, u32[]{:S(2)}) %copy-start.2) | copy-done | bytes 524312
  4.1 0.5 copy-done.23
  4.6 0.6 copy-done.25
  5.2 0.6 copy-done.27
  5.8 0.5 copy-done.29
  6.3 0.0 copy-start.13
  6.3 0.0 copy-start.8
  6.4 1.2 %shard_map.262 = (bf16[256,2048]{1,0:T(8,128)(2,1)S(1)}, bf16[256,1280]{1,0:T(8,128)(2,1)}) custom-call(bf16[128,128]{1,0:T(8,128)(2,1)S(1)} %get-tuple-element.47.value_up, f32[1,128]{1,0:T(1,128)S(1)} %get-tuple-element.48.head_gain, bf16[128,2048]{1,0:T(8,128)(2,1)S(1)} %get-tuple-element.49.out_attn, bf16[128,2048]{1,0:T(8,128)(2,1)S(1)} %get-tuple-element.50.out_rec), custom_call_target="tpu_custom_call" | custom-call | flops 100000000 | bytes 1048576 | tf_op jit(solution)/shard_map/pallas_call | solution.py:619
  7.6 0.6 collective-permute-start
  8.1 2.6 %collective-permute-start.12 = (bf16[256,1280]{1,0:T(8,128)(2,1)}, bf16[256,1280]{1,0:T(8,128)(2,1)}, u32[]{:S(2)}, u32[]{:S(2)}) collective-permute-start(bf16[256,1280]{1,0:T(8,128)(2,1)} %get-tuple-element.88), channel_id=1, source_target_pairs={{0,2},{1,3},{2,0},{3,1},{4,6},{5,7},{6,4},{7,5},{8,10},{9,11},{10,... | collective-permute-start | bytes 1966088 | tf_op jit(solution)/shard_map/ppermute | solution.py:773
  10.7 0.1 collective-permute-start.2
  10.8 0.1 collective-permute-start.1
  10.9 18.3 %collective-permute-done.2.refs_2_ = bf16[32,2048]{1,0:T(8,128)(2,1)} collective-permute-done((bf16[32,2048]{1,0:T(8,128)(2,1)S(1)}, bf16[32,2048]{1,0:T(8,128)(2,1)}, u32[]{:S(2)}, u32[]{:S(2)}) %collective-permute-start.2) | collective-permute-done | bytes 131104 | tf_op jit(solution)/shard_map/ppermute | solution.py:672
  29.2 0.0 collective-permute-start.3
  29.2 0.9 %and_select_fusion.ids = s32[4]{0:T(128)S(1)} fusion(s32[4]{0:T(128)} %constant.48, s32[4]{0:T(128)} %constant.36.clone, pred[4]{0:T(512)(128)(4,1)} %constant.35.clone, s32[]{:T(128)S(6)} %axis_index.25, s32[]{:T(128)S(6)} %axis_index.22), kind=kLoop, calls=%fused_computation | loop fusion | flops 60 | bytes 60 | tf_op jit(solution)/shard_map/jit(remainder)/select_n | solution.py:665
  30.1 0.0 collective-permute-done.1.refs_1_
  30.1 1.2 %shard_map.263.ready = bf16[96,2048]{1,0:T(8,128)(2,1)S(1)} custom-call(bf16[32,2048]{1,0:T(8,128)(2,1)S(1)} %copy-done.8, bf16[32,2048]{1,0:T(8,128)(2,1)} %collective-permute-done.1.refs_1_, bf16[32,2048]{1,0:T(8,128)(2,1)} %collective-permute-done.2.refs_2_, f32[1,2048]{1,0:T(1,128)S(1)} %get-tuple-element.52.refs_3_.refs_0_), custom_call_target="tpu_custom_call" | custom-call | flops 10000000 | bytes 1048576 | tf_op jit(solution)/shard_map/pallas_call | solution.py:619
  31.4 0.7 %copy-done.22 = bf16[4,2048]{1,0:T(4,128)(2,1)S(1)} copy-done((bf16[4,2048]{1,0:T(4,128)(2,1)S(1)}, bf16[4,2048]{1,0:T(4,128)(2,1)}, u32[]{:S(2)}) %copy-start.22) | copy-done | bytes 16408
  32.0 1.0 %copy-done.3 = bf16[2048,128]{1,0:T(8,128)(2,1)S(1)} copy-done((bf16[2048,128]{1,0:T(8,128)(2,1)S(1)}, bf16[2048,128]{1,0:T(8,128)(2,1)}, u32[]{:S(2)}) %copy-start.3) | copy-done | bytes 524312
  33.1 0.8 %copy-done.14 = f32[128,128]{1,0:T(8,128)S(1)} copy-done((f32[128,128]{1,0:T(8,128)S(1)}, f32[128,128]{1,0:T(8,128)}, u32[]{:S(2)}) %copy-start.14) | copy-done | bytes 65560
  33.9 0.8 %copy-done.16 = f32[128,128]{1,0:T(8,128)S(1)} copy-done((f32[128,128]{1,0:T(8,128)S(1)}, f32[128,128]{1,0:T(8,128)}, u32[]{:S(2)}) %copy-start.16) | copy-done | bytes 65560
  34.8 1.7 %shard_map.264 = (bf16[240,128]{1,0:T(8,128)(2,1)S(1)}, bf16[128,2048]{1,0:T(8,128)(2,1)S(1)}, bf16[128,128]{1,0:T(8,128)(2,1)S(1)}, bf16[128,128]{1,0:T(8,128)(...) custom-call(s32[4]{0:T(128)S(1)} %and_select_fusion.ids, bf16[96,2048]{1,0:T(8,128)(2,1)S(1)} %shard_map.263.ready, ...), custom_call_target="tpu_custom_call" | custom-call | tf_op jit(solution)/shard_map/pallas_call | solution.py:619
  36.6 0.6 copy-done.26
  37.2 1.5 %shard_map.265 = (bf16[64,2944]{1,0:T(8,128)(2,1)S(1)}, bf16[64,2944]{1,0:T(8,128)(2,1)S(1)}) custom-call(s32[4]{0:T(128)S(1)} %and_select_fusion.ids, bf16[128,2048]{1,0:T(8,128)(2,1)S(1)} %get-tuple-element.64.normed_ref, bf16[128,128]{1,0:T(8,128)(2,1)S(1)} %get-tuple-element.65.keys_ref, bf16[128,128]{1,0:T(8,128)(2,1)S(1)} %get-tuple-element.66.values_ref, ...), custom_call_target="tpu_custom_call" | custom-call | flops 100000000 | bytes 1048576 | tf_op jit(solution)/shard_map/pallas_call | solution.py:619
  38.7 0.6 collective-permute-start.4
  39.3 0.1 collective-permute-start.13
  39.3 1.7 %collective-permute-start.5 = (bf16[240,128]{1,0:T(8,128)(2,1)S(1)}, bf16[240,128]{1,0:T(8,128)(2,1)S(1)}, u32[]{:S(2)}, u32[]{:S(2)}) collective-permute-start(bf16[240,128]{1,0:T(8,128)(2,1)S(1)} %get-tuple-element.78.refs_0_), channel_id=1, source_target_pairs={{0,4},{4,0},{8,12},{12,8},{16,20},{20,16},{24,28},{28,24},{1,5},{5... | collective-permute-start | bytes 184328 | tf_op jit(solution)/shard_map/ppermute | solution.py:781
  41.1 2.6 %collective-permute-done.5.refs_1_ = bf16[240,128]{1,0:T(8,128)(2,1)S(1)} collective-permute-done((bf16[240,128]{1,0:T(8,128)(2,1)S(1)}, bf16[240,128]{1,0:T(8,128)(2,1)S(1)}, u32[]{:S(2)}, u32[]{:S(2)}) %collective-permute-start.5) | collective-permute-done | bytes 61472 | tf_op jit(solution)/shard_map/ppermute | solution.py:781
  43.7 0.6 shard_map.266
  44.3 2.9 %collective-permute-start.8 = (bf16[264,128]{1,0:T(8,128)(2,1)S(1)}, bf16[264,128]{1,0:T(8,128)(2,1)S(1)}, u32[]{:S(2)}, u32[]{:S(2)}) collective-permute-start(bf16[264,128]{1,0:T(8,128)(2,1)S(1)} %get-tuple-element.81), channel_id=1, source_target_pairs={{0,16},{4,20},{8,24},{12,28},{16,0},{20,4},{24,8},{28,12},{1,17},{... | collective-permute-start | bytes 202760 | tf_op jit(solution)/shard_map/ppermute | solution.py:809
  47.2 0.0 collective-permute-start.6
  47.2 1.2 %collective-permute-done.6.refs_2_.sides = bf16[144,128]{1,0:T(8,128)(2,1)S(1)} collective-permute-done((bf16[144,128]{1,0:T(8,128)(2,1)S(1)}, bf16[144,128]{1,0:T(8,128)(2,1)S(1)}, u32[]{:S(2)}, u32[]{:S(2)}) %collective-permute-start.6) | collective-permute-done | bytes 36896 | tf_op jit(solution)/shard_map/ppermute | solution.py:810
  48.4 1.3 %collective-permute-start.9 = (bf16[264,128]{1,0:T(8,128)(2,1)S(1)}, bf16[264,128]{1,0:T(8,128)(2,1)S(1)}, u32[]{:S(2)}, u32[]{:S(2)}) collective-permute-start(bf16[264,128]{1,0:T(8,128)(2,1)S(1)} %get-tuple-element.82), channel_id=1, source_target_pairs={{0,24},{4,28},{8,16},{12,20},{16,8},{20,12},{24,0},{28,4},{1,25},{... | collective-permute-start | bytes 202760 | tf_op jit(solution)/shard_map/ppermute | solution.py:809
  49.7 0.4 collective-permute-done.8.refs_5_
  50.1 1.6 %collective-permute-start.7 = (bf16[264,128]{1,0:T(8,128)(2,1)S(1)}, bf16[264,128]{1,0:T(8,128)(2,1)S(1)}, u32[]{:S(2)}, u32[]{:S(2)}) collective-permute-start(bf16[264,128]{1,0:T(8,128)(2,1)S(1)} %get-tuple-element.80.refs_3_), channel_id=1, source_target_pairs={{0,8},{4,12},{8,0},{12,4},{16,24},{20,28},{24,16},{28,20},{1,9},{5... | collective-permute-start | bytes 202760 | tf_op jit(solution)/shard_map/ppermute | solution.py:809
  51.7 3.4 %collective-permute-done.9.refs_6_ = bf16[264,128]{1,0:T(8,128)(2,1)S(1)} collective-permute-done((bf16[264,128]{1,0:T(8,128)(2,1)S(1)}, bf16[264,128]{1,0:T(8,128)(2,1)S(1)}, u32[]{:S(2)}, u32[]{:S(2)}) %collective-permute-start.9) | collective-permute-done | bytes 67616 | tf_op jit(solution)/shard_map/ppermute | solution.py:809
  55.1 0.1 collective-permute-done.7.refs_4_
  55.2 0.1 collective-permute-start.10
  55.3 1.1 %shard_map.268 = (bf16[64,128]{1,0:T(8,128)(2,1)S(1)}, f32[128,128]{1,0:T(8,128)S(1)}, f32[128,128]{1,0:T(8,128)S(1)}, f32[128,128]{1,0:T(8,128)S(1)}) custom-call(s32[4]{0:T(128)S(1)} %and_select_fusion.ids, bf16[984,128]{1,0:T(8,128)(2,1)S(1)} %shard_map.267.packed, bf16[144,128]{1,0:T(8,128)(2,1)S(1)} %get-tuple-element.79.sides, ...), custom_call_target="tpu_custom_call" | custom-call | flops 100000000 | bytes 1048576 | tf_op jit(solution)/shard_map/pallas_call | solution.py:619
  56.4 0.4 collective-permute-done.10.swapped
  56.8 1.3 %shard_map.270 = bf16[32,1280]{1,0:T(8,128)(2,1)S(1)} custom-call(s32[4]{0:T(128)S(1)} %and_select_fusion.ids, bf16[984,128]{1,0:T(8,128)(2,1)S(1)} %collective-permute-done.10.swapped, bf16[144,128]{1,0:T(8,128)(2,1)S(1)} %collective-permute-done.6.refs_2_.sides, bf16[64,2944]{1,0:T(8,128)(2,1)S(1)} %get-tuple-element.83.kept, ...), custom_call_target="tpu_custom_call" | custom-call | flops 100000000 | bytes 1048576 | tf_op jit(solution)/shard_map/pallas_call | solution.py:619
  58.1 1.6 %collective-permute-start.11 = (bf16[32,1280]{1,0:T(8,128)(2,1)S(1)}, bf16[32,1280]{1,0:T(8,128)(2,1)S(1)}, u32[]{:S(2)}, u32[]{:S(2)}) collective-permute-start(bf16[32,1280]{1,0:T(8,128)(2,1)S(1)} %shard_map.270), channel_id=1, source_target_pairs={{0,2},{1,3},{2,0},{3,1},{4,6},{5,7},{6,4},{7,5},{8,10},{9,11},{10,... | collective-permute-start | bytes 245768 | tf_op jit(solution)/shard_map/ppermute | solution.py:861
  59.7 1.4 %shard_map.269.total = f32[32,2048]{1,0:T(8,128)S(1)} custom-call(s32[4]{0:T(128)S(1)} %and_select_fusion.ids, bf16[984,128]{1,0:T(8,128)(2,1)S(1)} %collective-permute-done.10.swapped, bf16[144,128]{1,0:T(8,128)(2,1)S(1)} %collective-permute-done.6.refs_2_.sides, bf16[64,2944]{1,0:T(8,128)(2,1)S(1)} %get-tuple-element.83.kept, ...), custom_call_target="tpu_custom_call" | custom-call | flops 100000000 | bytes 1048576 | tf_op jit(solution)/shard_map/pallas_call | solution.py:619
  61.1 0.0 collective-permute-done.13.refs_2_
  61.1 1.6 %collective-permute-done.11.refs_0_ = bf16[32,1280]{1,0:T(8,128)(2,1)S(1)} collective-permute-done((bf16[32,1280]{1,0:T(8,128)(2,1)S(1)}, bf16[32,1280]{1,0:T(8,128)(2,1)S(1)}, u32[]{:S(2)}, u32[]{:S(2)}) %collective-permute-start.11) | collective-permute-done | bytes 81952 | tf_op jit(solution)/shard_map/ppermute | solution.py:861
  62.6 2.1 %shard_map.271 = bf16[32,2048]{1,0:T(8,128)(2,1)} custom-call(f32[32,2048]{1,0:T(8,128)S(1)} %shard_map.269.total, bf16[32,1280]{1,0:T(8,128)(2,1)S(1)} %collective-permute-done.11.refs_0_, bf16[256,1280]{1,0:T(8,128)(2,1)} %collective-permute-done.12.refs_1_, bf16[256,1280]{1,0:T(8,128)(2,1)S(1)} %collective-permute-done.13.refs_2_), custom_call_target="tpu_custom_call" | custom-call | tf_op jit(solution)/shard_map/pallas_call | solution.py:619
  (54 shorter events, 0.1 us)
Async XLA Ops:
  2.5 0.8 %copy-start = (bf16[2048,128]{1,0:T(8,128)(2,1)}, bf16[2048,128]{1,0:T(8,128)(2,1)S(1)}, u32[]{:S(2)}) copy-start(bf16[2048,128]{1,0:T(8,128)(2,1)S(1)} %get-tuple-element.53.refs_1_) | copy-start | bytes 1572868
  3.3 0.8 %copy-start.2 = (bf16[2048,128]{1,0:T(8,128)(2,1)}, bf16[2048,128]{1,0:T(8,128)(2,1)S(1)}, u32[]{:S(2)}) copy-start(bf16[2048,128]{1,0:T(8,128)(2,1)S(1)} %get-tuple-element.57.refs_5_) | copy-start | bytes 1572868
  4.1 0.5 copy-start.23
  4.6 0.6 copy-start.25
  5.2 0.6 copy-start.27
  5.8 0.5 copy-start.29
  6.3 1.2 %copy-start.4 = (bf16[64,2048]{1,0:T(8,128)(2,1)}, bf16[64,2048]{1,0:T(8,128)(2,1)S(1)}, u32[]{:S(2)}) copy-start(bf16[64,2048]{1,0:T(8,128)(2,1)S(1)} %get-tuple-element.56.refs_4_) | copy-start | bytes 786436
  6.3 1.2 %copy-start.6 = (bf16[64,2048]{1,0:T(8,128)(2,1)}, bf16[64,2048]{1,0:T(8,128)(2,1)S(1)}, u32[]{:S(2)}) copy-start(bf16[64,2048]{1,0:T(8,128)(2,1)S(1)} %get-tuple-element.74.rec_query_t) | copy-start | bytes 786436
  6.3 1.2 %copy-start.9 = (bf16[256,128]{1,0:T(8,128)(2,1)}, bf16[256,128]{1,0:T(8,128)(2,1)S(1)}, u32[]{:S(2)}) copy-start(bf16[256,128]{1,0:T(8,128)(2,1)S(1)} %get-tuple-element.71.nope_up) | copy-start | bytes 196612
  6.3 1.2 %copy-start.11 = (f32[2,64,128]{2,1,0:T(8,128)}, f32[2,64,128]{2,1,0:T(8,128)S(1)}, u32[]{:S(2)}) copy-start(f32[2,64,128]{2,1,0:T(8,128)S(1)} %get-tuple-element.75.init_state) | copy-start | bytes 196612
  6.3 1.2 %copy-start.13 = (f32[128,128]{1,0:T(8,128)}, f32[128,128]{1,0:T(8,128)S(1)}, u32[]{:S(2)}) copy-start(f32[128,128]{1,0:T(8,128)S(1)} %get-tuple-element.62.refs_10_) | copy-start | bytes 196612
  6.3 1.2 %copy-start.15 = (f32[128,128]{1,0:T(8,128)}, f32[128,128]{1,0:T(8,128)S(1)}, u32[]{:S(2)}) copy-start(f32[128,128]{1,0:T(8,128)S(1)} %get-tuple-element.63.refs_11_) | copy-start | bytes 196612
  6.3 1.2 %copy-start.17 = (bf16[64,256]{1,0:T(8,128)(2,1)}, bf16[64,256]{1,0:T(8,128)(2,1)S(1)}, u32[]{:S(2)}) copy-start(bf16[64,256]{1,0:T(8,128)(2,1)S(1)} %get-tuple-element.72.rope_up_t) | copy-start | bytes 98308
  6.3 1.2 %copy-start.19 = (bf16[128,128]{1,0:T(8,128)(2,1)}, bf16[128,128]{1,0:T(8,128)(2,1)S(1)}, u32[]{:S(2)}) copy-start(bf16[128,128]{1,0:T(8,128)(2,1)S(1)} %get-tuple-element.73.key_up) | copy-start | bytes 98308
  6.3 1.2 %copy-start.21 = (bf16[4,2048]{1,0:T(4,128)(2,1)}, bf16[4,2048]{1,0:T(4,128)(2,1)S(1)}, u32[]{:S(2)}) copy-start(bf16[4,2048]{1,0:T(4,128)(2,1)S(1)} %get-tuple-element.58.refs_6_) | copy-start | bytes 49156
  6.3 4.4 %copy-start.8 = (bf16[32,2048]{1,0:T(8,128)(2,1)S(1)}, bf16[32,2048]{1,0:T(8,128)(2,1)}, u32[]{:S(2)}) copy-start(bf16[32,2048]{1,0:T(8,128)(2,1)} %refs_0_.1) | copy-start | bytes 393220
  7.6 47.6 %collective-permute-start = (bf16[256,2048]{1,0:T(8,128)(2,1)S(1)}, bf16[256,2048]{1,0:T(8,128)(2,1)S(1)}, u32[]{:S(2)}, u32[]{:S(2)}) collective-permute-start(bf16[256,2048]{1,0:T(8,128)(2,1)S(1)} %get-tuple-element.51.weights), channel_id=1, source_target_pairs={{0,1},{1,0},{2,3},{3,2},{4,5},{5,4},{6,7},{7,6},{8,9},{9,8},{10,11... | collective-permute-start | bytes 3145736 | tf_op jit(solution)/shard_map/ppermute | solution.py:770
  8.1 31.1 %collective-permute-start.12 = (bf16[256,1280]{1,0:T(8,128)(2,1)}, bf16[256,1280]{1,0:T(8,128)(2,1)}, u32[]{:S(2)}, u32[]{:S(2)}) collective-permute-start(bf16[256,1280]{1,0:T(8,128)(2,1)} %get-tuple-element.88), channel_id=1, source_target_pairs={{0,2},{1,3},{2,0},{3,1},{4,6},{5,7},{6,4},{7,5},{8,10},{9,11},{10,... | collective-permute-start | bytes 1966088 | tf_op jit(solution)/shard_map/ppermute | solution.py:773
  10.7 18.4 %collective-permute-start.2 = (bf16[32,2048]{1,0:T(8,128)(2,1)S(1)}, bf16[32,2048]{1,0:T(8,128)(2,1)}, u32[]{:S(2)}, u32[]{:S(2)}) collective-permute-start(bf16[32,2048]{1,0:T(8,128)(2,1)S(1)} %copy-done.8), channel_id=1, source_target_pairs={{0,2},{1,3},{2,0},{3,1},{4,6},{5,7},{6,4},{7,5},{8,10},{9,11},{10,... | collective-permute-start | bytes 393224 | tf_op jit(solution)/shard_map/ppermute | solution.py:672
  10.8 19.3 %collective-permute-start.1 = (bf16[32,2048]{1,0:T(8,128)(2,1)S(1)}, bf16[32,2048]{1,0:T(8,128)(2,1)}, u32[]{:S(2)}, u32[]{:S(2)}) collective-permute-start(bf16[32,2048]{1,0:T(8,128)(2,1)S(1)} %copy-done.8), channel_id=1, source_target_pairs={{0,1},{1,0},{2,3},{3,2},{4,5},{5,4},{6,7},{7,6},{8,9},{9,8},{10,11... | collective-permute-start | bytes 393224 | tf_op jit(solution)/shard_map/ppermute | solution.py:675
  10.9 20.5 %copy-start.1 = (bf16[2048,128]{1,0:T(8,128)(2,1)S(1)}, bf16[2048,128]{1,0:T(8,128)(2,1)}, u32[]{:S(2)}) copy-start(bf16[2048,128]{1,0:T(8,128)(2,1)} %copy-done) | copy-start | bytes 1572868
  29.2 2.2 %collective-permute-start.3 = (bf16[32,2048]{1,0:T(8,128)(2,1)}, bf16[32,2048]{1,0:T(8,128)(2,1)S(1)}, u32[]{:S(2)}, u32[]{:S(2)}) collective-permute-start(bf16[32,2048]{1,0:T(8,128)(2,1)} %collective-permute-done.2.refs_2_), channel_id=1, source_target_pairs={{0,1},{1,0},{2,3},{3,2},{4,5},{5,4},{6,7},{7,6},{8,9},{9,8},{10,11... | collective-permute-start | bytes 393224 | tf_op jit(solution)/shard_map/ppermute | solution.py:675
  30.1 1.3 %copy-start.5 = (bf16[64,2048]{1,0:T(8,128)(2,1)S(1)}, bf16[64,2048]{1,0:T(8,128)(2,1)}, u32[]{:S(2)}) copy-start(bf16[64,2048]{1,0:T(8,128)(2,1)} %copy-done.4) | copy-start | bytes 786436
  31.3 0.7 %copy-start.22 = (bf16[4,2048]{1,0:T(4,128)(2,1)S(1)}, bf16[4,2048]{1,0:T(4,128)(2,1)}, u32[]{:S(2)}) copy-start(bf16[4,2048]{1,0:T(4,128)(2,1)} %copy-done.21) | copy-start | bytes 49156
  31.3 0.7 %copy-start.24 = (f32[2,128]{1,0:T(2,128)S(1)}, f32[2,128]{1,0:T(2,128)}, u32[]{:S(2)}) copy-start(f32[2,128]{1,0:T(2,128)} %copy-done.23) | copy-start | bytes 3076
  31.3 0.7 %copy-start.30 = (f32[1,128]{1,0:T(1,128)S(1)}, f32[1,128]{1,0:T(1,128)}, u32[]{:S(2)}) copy-start(f32[1,128]{1,0:T(1,128)} %copy-done.29) | copy-start | bytes 1540
  32.0 1.0 %copy-start.3 = (bf16[2048,128]{1,0:T(8,128)(2,1)S(1)}, bf16[2048,128]{1,0:T(8,128)(2,1)}, u32[]{:S(2)}) copy-start(bf16[2048,128]{1,0:T(8,128)(2,1)} %copy-done.2) | copy-start | bytes 1572868
  33.1 0.8 %copy-start.14 = (f32[128,128]{1,0:T(8,128)S(1)}, f32[128,128]{1,0:T(8,128)}, u32[]{:S(2)}) copy-start(f32[128,128]{1,0:T(8,128)} %copy-done.13) | copy-start | bytes 196612
  33.9 0.8 %copy-start.16 = (f32[128,128]{1,0:T(8,128)S(1)}, f32[128,128]{1,0:T(8,128)}, u32[]{:S(2)}) copy-start(f32[128,128]{1,0:T(8,128)} %copy-done.15) | copy-start | bytes 196612
  34.8 1.8 %copy-start.7 = (bf16[64,2048]{1,0:T(8,128)(2,1)S(1)}, bf16[64,2048]{1,0:T(8,128)(2,1)}, u32[]{:S(2)}) copy-start(bf16[64,2048]{1,0:T(8,128)(2,1)} %copy-done.6) | copy-start | bytes 786436
  34.8 1.8 %copy-start.10 = (bf16[256,128]{1,0:T(8,128)(2,1)S(1)}, bf16[256,128]{1,0:T(8,128)(2,1)}, u32[]{:S(2)}) copy-start(bf16[256,128]{1,0:T(8,128)(2,1)} %copy-done.9) | copy-start | bytes 196612
  34.8 1.8 %copy-start.12 = (f32[2,64,128]{2,1,0:T(8,128)S(1)}, f32[2,64,128]{2,1,0:T(8,128)}, u32[]{:S(2)}) copy-start(f32[2,64,128]{2,1,0:T(8,128)} %copy-done.11) | copy-start | bytes 196612
  34.8 1.8 %copy-start.18 = (bf16[64,256]{1,0:T(8,128)(2,1)S(1)}, bf16[64,256]{1,0:T(8,128)(2,1)}, u32[]{:S(2)}) copy-start(bf16[64,256]{1,0:T(8,128)(2,1)} %copy-done.17) | copy-start | bytes 98308
  34.8 1.8 %copy-start.20 = (bf16[128,128]{1,0:T(8,128)(2,1)S(1)}, bf16[128,128]{1,0:T(8,128)(2,1)}, u32[]{:S(2)}) copy-start(bf16[128,128]{1,0:T(8,128)(2,1)} %copy-done.19) | copy-start | bytes 98308
  34.8 1.8 %copy-start.28 = (f32[2,64]{1,0:T(2,128)S(1)}, f32[2,64]{1,0:T(2,128)}, u32[]{:S(2)}) copy-start(f32[2,64]{1,0:T(2,128)} %copy-done.27) | copy-start | bytes 1540
  36.5 0.7 %copy-start.26 = (f32[1,256]{1,0:T(1,128)S(1)}, f32[1,256]{1,0:T(1,128)}, u32[]{:S(2)}) copy-start(f32[1,256]{1,0:T(1,128)} %copy-done.25) | copy-start | bytes 3076
  38.7 16.5 %collective-permute-start.4 = (bf16[64,2944]{1,0:T(8,128)(2,1)S(1)}, bf16[64,2944]{1,0:T(8,128)(2,1)S(1)}, u32[]{:S(2)}, u32[]{:S(2)}) collective-permute-start(bf16[64,2944]{1,0:T(8,128)(2,1)S(1)} %get-tuple-element.77), channel_id=1, source_target_pairs={{0,1},{1,0},{2,3},{3,2},{4,5},{5,4},{6,7},{7,6},{8,9},{9,8},{10,11... | collective-permute-start | bytes 1130504 | tf_op jit(solution)/shard_map/ppermute | solution.py:775
  39.3 21.8 %collective-permute-start.13 = (bf16[256,1280]{1,0:T(8,128)(2,1)}, bf16[256,1280]{1,0:T(8,128)(2,1)S(1)}, u32[]{:S(2)}, u32[]{:S(2)}) collective-permute-start(bf16[256,1280]{1,0:T(8,128)(2,1)} %collective-permute-done.12.refs_1_), channel_id=1, source_target_pairs={{0,1},{1,0},{2,3},{3,2},{4,5},{5,4},{6,7},{7,6},{8,9},{9,8},{10,11... | collective-permute-start | bytes 1966088 | tf_op jit(solution)/shard_map/ppermute | solution.py:774
  39.3 4.3 %collective-permute-start.5 = (bf16[240,128]{1,0:T(8,128)(2,1)S(1)}, bf16[240,128]{1,0:T(8,128)(2,1)S(1)}, u32[]{:S(2)}, u32[]{:S(2)}) collective-permute-start(bf16[240,128]{1,0:T(8,128)(2,1)S(1)} %get-tuple-element.78.refs_0_), channel_id=1, source_target_pairs={{0,4},{4,0},{8,12},{12,8},{16,20},{20,16},{24,28},{28,24},{1,5},{5... | collective-permute-start | bytes 184328 | tf_op jit(solution)/shard_map/ppermute | solution.py:781
  44.3 5.8 %collective-permute-start.8 = (bf16[264,128]{1,0:T(8,128)(2,1)S(1)}, bf16[264,128]{1,0:T(8,128)(2,1)S(1)}, u32[]{:S(2)}, u32[]{:S(2)}) collective-permute-start(bf16[264,128]{1,0:T(8,128)(2,1)S(1)} %get-tuple-element.81), channel_id=1, source_target_pairs={{0,16},{4,20},{8,24},{12,28},{16,0},{20,4},{24,8},{28,12},{1,17},{... | collective-permute-start | bytes 202760 | tf_op jit(solution)/shard_map/ppermute | solution.py:809
  47.2 1.2 %collective-permute-start.6 = (bf16[144,128]{1,0:T(8,128)(2,1)S(1)}, bf16[144,128]{1,0:T(8,128)(2,1)S(1)}, u32[]{:S(2)}, u32[]{:S(2)}) collective-permute-start(bf16[144,128]{1,0:T(8,128)(2,1)S(1)} %get-tuple-element.79.sides), channel_id=1, source_target_pairs={{0,1},{1,0},{2,3},{3,2},{4,5},{5,4},{6,7},{7,6},{8,9},{9,8},{10,11... | collective-permute-start | bytes 110600 | tf_op jit(solution)/shard_map/ppermute | solution.py:810
  48.4 6.7 %collective-permute-start.9 = (bf16[264,128]{1,0:T(8,128)(2,1)S(1)}, bf16[264,128]{1,0:T(8,128)(2,1)S(1)}, u32[]{:S(2)}, u32[]{:S(2)}) collective-permute-start(bf16[264,128]{1,0:T(8,128)(2,1)S(1)} %get-tuple-element.82), channel_id=1, source_target_pairs={{0,24},{4,28},{8,16},{12,20},{16,8},{20,12},{24,0},{28,4},{1,25},{... | collective-permute-start | bytes 202760 | tf_op jit(solution)/shard_map/ppermute | solution.py:809
  50.1 5.1 %collective-permute-start.7 = (bf16[264,128]{1,0:T(8,128)(2,1)S(1)}, bf16[264,128]{1,0:T(8,128)(2,1)S(1)}, u32[]{:S(2)}, u32[]{:S(2)}) collective-permute-start(bf16[264,128]{1,0:T(8,128)(2,1)S(1)} %get-tuple-element.80.refs_3_), channel_id=1, source_target_pairs={{0,8},{4,12},{8,0},{12,4},{16,24},{20,28},{24,16},{28,20},{1,9},{5... | collective-permute-start | bytes 202760 | tf_op jit(solution)/shard_map/ppermute | solution.py:809
  55.2 1.6 %collective-permute-start.10 = (bf16[984,128]{1,0:T(8,128)(2,1)S(1)}, bf16[984,128]{1,0:T(8,128)(2,1)S(1)}, u32[]{:S(2)}, u32[]{:S(2)}) collective-permute-start(bf16[984,128]{1,0:T(8,128)(2,1)S(1)} %shard_map.267.packed), channel_id=1, source_target_pairs={{0,1},{1,0},{2,3},{3,2},{4,5},{5,4},{6,7},{7,6},{8,9},{9,8},{10,11... | collective-permute-start | bytes 755720 | tf_op jit(solution)/shard_map/ppermute | solution.py:818
  58.1 4.5 %collective-permute-start.11 = (bf16[32,1280]{1,0:T(8,128)(2,1)S(1)}, bf16[32,1280]{1,0:T(8,128)(2,1)S(1)}, u32[]{:S(2)}, u32[]{:S(2)}) collective-permute-start(bf16[32,1280]{1,0:T(8,128)(2,1)S(1)} %shard_map.270), channel_id=1, source_target_pairs={{0,2},{1,3},{2,0},{3,1},{4,6},{5,7},{6,4},{7,5},{8,10},{9,11},{10,... | collective-permute-start | bytes 245768 | tf_op jit(solution)/shard_map/ppermute | solution.py:861

commit v3 on v2

--- a/solution.py
+++ b/solution.py
@@ -394,7 +394,12 @@
             before.append(placed(state, sign * source, sign * source < sign * digit))
             whole.append(placed(state, sign * source))
         at = slice(direction * state_rows, (direction + 1) * state_rows)
-        state_out[at, :] = joined(before).astype(state_out.dtype)
+        if start and radix == 2:
+            c_part, n_part, peak, keep, _ = before[1]
+            inside = jnp.concatenate([c_part, aux_rows(n_part, peak, keep)], axis=0)
+        else:
+            inside = joined(before)
+        state_out[at, :] = inside.astype(state_out.dtype)
         totals.append(joined(whole).astype(BF16))
     total_f, total_b = totals
     part = kv_rows // 3
@@ -425,6 +430,14 @@
         copy.wait()
 
 
+def late_of(radix):
+    return min(2, radix - 1)
+
+
+def early_of(radix):
+    return [k for k in range(1, radix) if k != late_of(radix)]
+
+
 def pack_kernel(*refs, count, state_rows):
     received, out = refs[-1 - count : -1], refs[-1]
     part = (received[0].shape[0] - state_rows) // 3
@@ -437,13 +450,16 @@
             out[to : to + state_rows, :] = message[3 * part : 3 * part + state_rows, :]
 
 
-def attend(sections, keys, part, score_scale):
-    rope = keys[2 * part : 3 * part, :]
+def attend(sections, sources, score_scale):
     scores, lats = [], []
-    for section in range(2):
-        lat = keys[section * part : (section + 1) * part, :]
-        lats.append(lat)
-        scores.append(dot_nt(sections[section], jnp.concatenate([lat, rope], axis=1)) * score_scale)
+    for keys, part in sources:
+        rope = keys[2 * part : 3 * part, :]
+        for section in range(2):
+            lat = keys[section * part : (section + 1) * part, :]
+            lats.append(lat)
+            scores.append(
+                dot_nt(sections[section], jnp.concatenate([lat, rope], axis=1)) * score_scale
+            )
     top = functools.reduce(jnp.maximum, [jnp.max(s, axis=1, keepdims=True) for s in scores])
     mass = accum = None
     for part_scores, lat in zip(scores, lats):
@@ -455,6 +471,11 @@
     return top, mass, accum
 
 
+def sources_of(packed, late, radix, state_rows):
+    part = (packed.shape[0] - (radix - 2) * state_rows) // 3
+    return [(packed, part), (late, (late.shape[0] - state_rows) // 3)]
+
+
 def sections_of(queries, width):
     return [
         queries[:, 0 : 2 * width],
@@ -462,8 +483,8 @@
     ]
 
 
-def finished(ids, block, first_ref, packed, sides, slot, radix, state_rows, floor_value):
-    base = packed.shape[0] - (radix - 1) * state_rows
+def finished(ids, block, first_ref, packed, late, sides, slot, radix, state_rows, floor_value):
+    base = packed.shape[0] - (radix - 2) * state_rows
     width = packed.shape[1]
 
     def column(index):
@@ -473,7 +494,9 @@
         return column(index) + column(index + 1) + column(index + 2)
 
     def fetch(k, direction):
-        at = base + (k - 1) * state_rows
+        if k == late_of(radix):
+            return read_state(late[late.shape[0] - state_rows :, :])
+        at = base + early_of(radix).index(k) * state_rows
         return read_state(packed[at : at + state_rows, :])
 
     levels = level_states(ids, slot, radix, fetch)
@@ -517,6 +540,7 @@
 def half_kernel(
     ids,
     packed,
+    late,
     sides,
     kept,
     shared,
@@ -532,12 +556,12 @@
     score_scale,
 ):
     width = packed.shape[1]
-    part = (packed.shape[0] - (radix - 1) * state_rows) // 3
     recurrent_out[...] = finished(
-        ids, kept[...], kept, packed, sides, slot, radix, state_rows, floor_value
+        ids, kept[...], kept, packed, late, sides, slot, radix, state_rows, floor_value
     )
     queries = jnp.concatenate([kept[:, 0 : 3 * width], shared[:, 0 : 3 * width]], axis=0)
-    top, mass, accum = attend(sections_of(queries, width), packed, part, score_scale)
+    sources = sources_of(packed, late, radix, state_rows)
+    top, mass, accum = attend(sections_of(queries, width), sources, score_scale)
     top_out[...] = jnp.broadcast_to(top, top_out.shape)
     mass_out[...] = jnp.broadcast_to(mass, mass_out.shape)
     accum_out[...] = accum
@@ -546,6 +570,7 @@
 def mix_kernel(
     ids,
     swapped,
+    late,
     sides,
     kept,
     shared,
@@ -566,11 +591,11 @@
     step,
 ):
     width = swapped.shape[1]
-    part = (swapped.shape[0] - (radix - 1) * state_rows) // 3
     at = slice(piece * step, (piece + 1) * step)
     also = slice(kept.shape[0] + piece * step, kept.shape[0] + (piece + 1) * step)
     queries = jnp.concatenate([kept[at, 0 : 3 * width], shared[at, 0 : 3 * width]], axis=0)
-    top, mass, accum = attend(sections_of(queries, width), swapped, part, score_scale)
+    sources = sources_of(swapped, late, radix, state_rows)
+    top, mass, accum = attend(sections_of(queries, width), sources, score_scale)
 
     def both(ref):
         return jnp.concatenate([ref[at, :], ref[also, :]], axis=0)
@@ -582,7 +607,7 @@
     mass = here * mass + there * both(mass_half)
     attended = (accum / mass).astype(BF16)
     other = finished(
-        ids, shared[at, :], shared, swapped, sides, slot, radix, state_rows, floor_value
+        ids, shared[at, :], shared, swapped, late, sides, slot, radix, state_rows, floor_value
     )
     mine = jnp.concatenate([attended[:step], recurrent[at, :]], axis=1)
     theirs = jnp.concatenate([attended[step:], other], axis=1)
@@ -808,14 +833,16 @@
         pairs = digit_pairs(peers, strides[level], radix, k)
         received.append(lax.ppermute(messages[k - 1], "sp", pairs))
     other_sides = lax.ppermute(sides, "tp", partner)
+    late = received.pop(late_of(radix) - 1)
     (packed,) = call(
-        functools.partial(pack_kernel, count=radix, state_rows=state_rows),
-        [((radix * kv_rows + (radix - 1) * state_rows, value_width), BF16)],
-        [other_weights, shared, other_sides, message] + received,
+        functools.partial(pack_kernel, count=radix - 1, state_rows=state_rows),
+        [(((radix - 1) * kv_rows + (radix - 2) * state_rows, value_width), BF16)],
+        [shared, other_sides, message] + received,
         ids=False,
         limit=wide,
     )
     swapped = lax.ppermute(packed, "tp", partner)
+    other_late = lax.ppermute(late, "tp", partner)
     level_facts = dict(
         slot=2 + level,
         radix=radix,
@@ -826,7 +853,7 @@
     half = call(
         functools.partial(half_kernel, **level_facts),
         [((seq // 2, value_width), BF16)] + [((seq, value_width), F32)] * 3,
-        [ids, packed, sides, kept, shared],
+        [ids, packed, late, sides, kept, shared],
         limit=wide,
         cost=pl.CostEstimate(flops=10**8, bytes_accessed=1 << 20, transcendentals=0),
     )
@@ -844,6 +871,7 @@
             [
                 ids,
                 swapped,
+                other_late,
                 other_sides,
                 kept,
                 shared,

time: 65.1 us -> 68.9 us (1.058)
  waiting for transfers between devices: 27.9 us -> 32.4 us
  starting transfers between devices: 13.2 us -> 12.3 us
    ppermute x3, waiting for transfers between devices: 3.81 us -> 10.6 us  [shards(): received.append(lax.ppermute(messages[k - 1], 'sp', pairs))]
    ppermute x3, starting transfers between devices: 5.86 us -> 4.48 us  [shards(): received.append(lax.ppermute(messages[k - 1], 'sp', pairs))]
    ppermute x1, waiting for transfers between devices: 1.21 us -> 0.01 us  [shards(): other_sides = lax.ppermute(sides, 'tp', partner)]
    ppermute x1, waiting for transfers between devices: 18.3 us -> 17.3 us  [shards(): gathered.append(lax.ppermute(rows_in, 'tp', ring[k]))]
  transfers between devices with their start and end apart: 14 -> 15, of which waited for: 8 -> 7; matrix products, arithmetic and copies ran while one was open for 1% -> 1% of each run, Pallas kernels for 14% -> 13%
where the time goes in v3:
time: 68.9 us; the launch traced here: 68.5 us
  waiting for transfers between devices  32.4 us (47%)
  Pallas kernels  14.6 us (21%)
  starting transfers between devices  12.3 us (18%)
  local copies, waits for them, and re-layouts  7.91 us (11%)
  other arithmetic  0.94 us (1%)
    ppermute x1, waiting for transfers between devices, shards(): gathered.append(lax.ppermute(rows_in, 'tp', ring[k]))  17.3 us
    pallas_call x10, Pallas kernels, call(): pl.pallas_call(kernel, out_shape=[jax.ShapeDtypeStruct(shape, dtype) for...  12.1 us
    ppermute x3, waiting for transfers between devices, shards(): received.append(lax.ppermute(messages[k - 1], 'sp', pairs))  10.6 us
    unnamed x62, local copies, waits for them, and re-layouts  7.91 us
    ppermute x3, starting transfers between devices, shards(): received.append(lax.ppermute(messages[k - 1], 'sp', pairs))  4.48 us
    ppermute x1, starting transfers between devices, shards(): there = lax.ppermute(ahead, 'tp', ring[k])  3.06 us
    ppermute x1, waiting for transfers between devices, shards(): lax.ppermute(message, 'sp', digit_pairs(peers, strides[level], radix, k))  2.63 us
    pallas_call x1, Pallas kernels, shards(): pl.pallas_call(load_kernel, out_shape=[pltpu.VMEM(array.shape, array.dtyp...  2.47 us
  transfers between devices with their start and end apart: 15, of which 7 were waited for; matrix products, arithmetic and copies ran while one was open for 1% of the time, Pallas kernels for 13%

profile of v3, /device:TPU:0, one launch (start us, length us, event | category | flops | bytes accessed | tf_op | source)
XLA Modules:
  0.0 68.5 jit_solution(2230218280615328050)
XLA Ops:
  0.0 2.5 %load.1 = (f32[1,2048]{1,0:T(1,128)S(1)}, bf16[2048,128]{1,0:T(8,128)(2,1)S(1)}, f32[1,128]{1,0:T(1,128)S(1)}, bf16[64,2048]{1,0:T(8,128)(2,1)S(1)}, bf16[64,204...) custom-call(f32[1,2048]{1,0:T(1,128)} %bitcast.22, ...), custom_call_target="tpu_custom_call" | custom-call | flops 100000000 | bytes 4194304 | tf_op jit(solution)/shard_map/load/pallas_call | solution.py:733
  2.5 0.8 %copy-done = bf16[2048,128]{1,0:T(8,128)(2,1)} copy-done((bf16[2048,128]{1,0:T(8,128)(2,1)}, bf16[2048,128]{1,0:T(8,128)(2,1)S(1)}, u32[]{:S(2)}) %copy-start) | copy-done | bytes 524312
  3.3 0.8 %copy-done.2 = bf16[2048,128]{1,0:T(8,128)(2,1)} copy-done((bf16[2048,128]{1,0:T(8,128)(2,1)}, bf16[2048,128]{1,0:T(8,128)(2,1)S(1)}, u32[]{:S(2)}) %copy-start.2) | copy-done | bytes 524312
  4.1 0.6 copy-done.23
  4.7 0.6 copy-done.25
  5.2 0.5 copy-done.27
  5.8 0.5 copy-done.29
  6.3 0.0 copy-start.13
  6.4 0.0 copy-start.8
  6.4 1.1 %shard_map.268 = (bf16[256,2048]{1,0:T(8,128)(2,1)S(1)}, bf16[256,1280]{1,0:T(8,128)(2,1)}) custom-call(bf16[128,128]{1,0:T(8,128)(2,1)S(1)} %get-tuple-element.83.value_up, f32[1,128]{1,0:T(1,128)S(1)} %get-tuple-element.84.head_gain, bf16[128,2048]{1,0:T(8,128)(2,1)S(1)} %get-tuple-element.85.out_attn, bf16[128,2048]{1,0:T(8,128)(2,1)S(1)} %get-tuple-element.86.out_rec), custom_call_target="tpu_custom_call" | custom-call | flops 100000000 | bytes 1048576 | tf_op jit(solution)/shard_map/pallas_call | solution.py:644
  7.6 3.1 %collective-permute-start.13 = (bf16[256,1280]{1,0:T(8,128)(2,1)}, bf16[256,1280]{1,0:T(8,128)(2,1)}, u32[]{:S(2)}, u32[]{:S(2)}) collective-permute-start(bf16[256,1280]{1,0:T(8,128)(2,1)} %get-tuple-element.88), channel_id=1, source_target_pairs={{0,2},{1,3},{2,0},{3,1},{4,6},{5,7},{6,4},{7,5},{8,10},{9,11},{10,... | collective-permute-start | bytes 1966088 | tf_op jit(solution)/shard_map/ppermute | solution.py:798
  10.6 0.0 collective-permute-start.11
  10.6 0.2 collective-permute-start.1
  10.8 0.3 collective-permute-start
  11.2 17.3 %collective-permute-done.1.refs_2_ = bf16[32,2048]{1,0:T(8,128)(2,1)} collective-permute-done((bf16[32,2048]{1,0:T(8,128)(2,1)S(1)}, bf16[32,2048]{1,0:T(8,128)(2,1)}, u32[]{:S(2)}, u32[]{:S(2)}) %collective-permute-start.1) | collective-permute-done | bytes 131104 | tf_op jit(solution)/shard_map/ppermute | solution.py:697
  28.5 0.0 collective-permute-start.2
  28.5 0.9 %and_select_fusion.ids = s32[4]{0:T(128)S(1)} fusion(s32[4]{0:T(128)} %constant.48, s32[4]{0:T(128)} %constant.36.clone, pred[4]{0:T(512)(128)(4,1)} %constant.35.clone, s32[]{:T(128)S(6)} %axis_index.25, s32[]{:T(128)S(6)} %axis_index.22), kind=kLoop, calls=%fused_computation | loop fusion | flops 60 | bytes 60 | tf_op jit(solution)/shard_map/jit(remainder)/select_n | solution.py:690
  29.5 1.2 %shard_map.262.ready = bf16[96,2048]{1,0:T(8,128)(2,1)S(1)} custom-call(bf16[32,2048]{1,0:T(8,128)(2,1)S(1)} %copy-done.8, bf16[32,2048]{1,0:T(8,128)(2,1)} %collective-permute-done.refs_1_, bf16[32,2048]{1,0:T(8,128)(2,1)} %collective-permute-done.1.refs_2_, f32[1,2048]{1,0:T(1,128)S(1)} %get-tuple-element.47.refs_3_.refs_0_), custom_call_target="tpu_custom_call" | custom-call | flops 10000000 | bytes 1048576 | tf_op jit(solution)/shard_map/pallas_call | solution.py:644
  30.7 0.0 collective-permute-done.2.late
  30.7 0.7 copy-done.22
  31.4 1.0 %copy-done.3 = bf16[2048,128]{1,0:T(8,128)(2,1)S(1)} copy-done((bf16[2048,128]{1,0:T(8,128)(2,1)S(1)}, bf16[2048,128]{1,0:T(8,128)(2,1)}, u32[]{:S(2)}) %copy-start.3) | copy-done | bytes 524312
  32.4 0.8 %copy-done.14 = f32[128,128]{1,0:T(8,128)S(1)} copy-done((f32[128,128]{1,0:T(8,128)S(1)}, f32[128,128]{1,0:T(8,128)}, u32[]{:S(2)}) %copy-start.14) | copy-done | bytes 65560
  33.3 0.8 %copy-done.16 = f32[128,128]{1,0:T(8,128)S(1)} copy-done((f32[128,128]{1,0:T(8,128)S(1)}, f32[128,128]{1,0:T(8,128)}, u32[]{:S(2)}) %copy-start.16) | copy-done | bytes 65560
  34.1 1.7 %shard_map.263 = (bf16[240,128]{1,0:T(8,128)(2,1)S(1)}, bf16[128,2048]{1,0:T(8,128)(2,1)S(1)}, bf16[128,128]{1,0:T(8,128)(2,1)S(1)}, bf16[128,128]{1,0:T(8,128)(...) custom-call(s32[4]{0:T(128)S(1)} %and_select_fusion.ids, bf16[96,2048]{1,0:T(8,128)(2,1)S(1)} %shard_map.262.ready, ...), custom_call_target="tpu_custom_call" | custom-call | tf_op jit(solution)/shard_map/pallas_call | solution.py:644
  35.9 0.6 collective-permute-start.14
  36.5 0.6 copy-done.26
  37.1 1.5 %shard_map.264 = (bf16[64,2944]{1,0:T(8,128)(2,1)S(1)}, bf16[64,2944]{1,0:T(8,128)(2,1)S(1)}) custom-call(s32[4]{0:T(128)S(1)} %and_select_fusion.ids, bf16[128,2048]{1,0:T(8,128)(2,1)S(1)} %get-tuple-element.59.normed_ref, bf16[128,128]{1,0:T(8,128)(2,1)S(1)} %get-tuple-element.60.keys_ref, bf16[128,128]{1,0:T(8,128)(2,1)S(1)} %get-tuple-element.61.values_ref, ...), custom_call_target="tpu_custom_call" | custom-call | flops 100000000 | bytes 1048576 | tf_op jit(solution)/shard_map/pallas_call | solution.py:644
  38.6 0.1 collective-permute-start.3
  38.7 1.8 %collective-permute-start.4 = (bf16[240,128]{1,0:T(8,128)(2,1)S(1)}, bf16[240,128]{1,0:T(8,128)(2,1)S(1)}, u32[]{:S(2)}, u32[]{:S(2)}) collective-permute-start(bf16[240,128]{1,0:T(8,128)(2,1)S(1)} %get-tuple-element.73.refs_0_), channel_id=1, source_target_pairs={{0,4},{4,0},{8,12},{12,8},{16,20},{20,16},{24,28},{28,24},{1,5},{5... | collective-permute-start | bytes 184328 | tf_op jit(solution)/shard_map/ppermute | solution.py:806
  40.4 2.6 %collective-permute-done.4.refs_1_ = bf16[240,128]{1,0:T(8,128)(2,1)S(1)} collective-permute-done((bf16[240,128]{1,0:T(8,128)(2,1)S(1)}, bf16[240,128]{1,0:T(8,128)(2,1)S(1)}, u32[]{:S(2)}, u32[]{:S(2)}) %collective-permute-start.4) | collective-permute-done | bytes 61472 | tf_op jit(solution)/shard_map/ppermute | solution.py:806
  43.1 0.6 shard_map.265
  43.7 0.1 collective-permute-start.5
  43.8 3.9 %collective-permute-start.7 = (bf16[264,128]{1,0:T(8,128)(2,1)S(1)}, bf16[264,128]{1,0:T(8,128)(2,1)S(1)}, u32[]{:S(2)}, u32[]{:S(2)}) collective-permute-start(bf16[264,128]{1,0:T(8,128)(2,1)S(1)} %get-tuple-element.76), channel_id=1, source_target_pairs={{0,24},{4,28},{8,16},{12,20},{16,8},{20,12},{24,0},{28,4},{1,25},{... | collective-permute-start | bytes 202760 | tf_op jit(solution)/shard_map/ppermute | solution.py:834
  47.6 0.0 collective-permute-done.5.refs_1_.sides
  47.6 0.0 collective-permute-start.6
  47.6 3.0 %collective-permute-done.7.refs_4_ = bf16[264,128]{1,0:T(8,128)(2,1)S(1)} collective-permute-done((bf16[264,128]{1,0:T(8,128)(2,1)S(1)}, bf16[264,128]{1,0:T(8,128)(2,1)S(1)}, u32[]{:S(2)}, u32[]{:S(2)}) %collective-permute-start.7) | collective-permute-done | bytes 67616 | tf_op jit(solution)/shard_map/ppermute | solution.py:834
  50.7 1.3 %collective-permute-done.6.refs_3_ = bf16[264,128]{1,0:T(8,128)(2,1)S(1)} collective-permute-done((bf16[264,128]{1,0:T(8,128)(2,1)S(1)}, bf16[264,128]{1,0:T(8,128)(2,1)S(1)}, u32[]{:S(2)}, u32[]{:S(2)}) %collective-permute-start.6) | collective-permute-done | bytes 67616 | tf_op jit(solution)/shard_map/ppermute | solution.py:834
  52.0 0.1 collective-permute-start.8
  52.1 0.6 collective-permute-start.9
  52.7 6.3 %collective-permute-done.9.late = bf16[264,128]{1,0:T(8,128)(2,1)S(1)} collective-permute-done((bf16[264,128]{1,0:T(8,128)(2,1)S(1)}, bf16[264,128]{1,0:T(8,128)(2,1)S(1)}, u32[]{:S(2)}, u32[]{:S(2)}) %collective-permute-start.9) | collective-permute-done | bytes 67616 | tf_op jit(solution)/shard_map/ppermute | solution.py:834
  59.0 1.2 %shard_map.267 = (bf16[64,128]{1,0:T(8,128)(2,1)S(1)}, f32[128,128]{1,0:T(8,128)S(1)}, f32[128,128]{1,0:T(8,128)S(1)}, f32[128,128]{1,0:T(8,128)S(1)}) custom-call(s32[4]{0:T(128)S(1)} %and_select_fusion.ids, bf16[720,128]{1,0:T(8,128)(2,1)S(1)} %shard_map.266.packed, bf16[264,128]{1,0:T(8,128)(2,1)S(1)} %collective-permute-done.9.late, ...), custom_call_target="tpu_custom_call" | custom-call | flops 100000000 | bytes 1048576 | tf_op jit(solution)/shard_map/pallas_call | solution.py:644
  60.2 0.1 collective-permute-done.10.late
  60.2 0.0 collective-permute-done.8.swapped
  60.2 1.2 %shard_map.270 = bf16[32,1280]{1,0:T(8,128)(2,1)S(1)} custom-call(s32[4]{0:T(128)S(1)} %and_select_fusion.ids, bf16[720,128]{1,0:T(8,128)(2,1)S(1)} %collective-permute-done.8.swapped, bf16[264,128]{1,0:T(8,128)(2,1)S(1)} %collective-permute-done.10.late, bf16[144,128]{1,0:T(8,128)(2,1)S(1)} %collective-permute-done.5.refs_1_.sides, ...), custom_call_target="tpu_custom_call" | custom-call | flops 100000000 | bytes 1048576 | tf_op jit(solution)/shard_map/pallas_call | solution.py:644
  61.5 1.7 %collective-permute-start.12 = (bf16[32,1280]{1,0:T(8,128)(2,1)S(1)}, bf16[32,1280]{1,0:T(8,128)(2,1)S(1)}, u32[]{:S(2)}, u32[]{:S(2)}) collective-permute-start(bf16[32,1280]{1,0:T(8,128)(2,1)S(1)} %shard_map.270), channel_id=1, source_target_pairs={{0,2},{1,3},{2,0},{3,1},{4,6},{5,7},{6,4},{7,5},{8,10},{9,11},{10,... | collective-permute-start | bytes 245768 | tf_op jit(solution)/shard_map/ppermute | solution.py:889
  63.2 1.5 %shard_map.269.total = f32[32,2048]{1,0:T(8,128)S(1)} custom-call(s32[4]{0:T(128)S(1)} %and_select_fusion.ids, bf16[720,128]{1,0:T(8,128)(2,1)S(1)} %collective-permute-done.8.swapped, bf16[264,128]{1,0:T(8,128)(2,1)S(1)} %collective-permute-done.10.late, bf16[144,128]{1,0:T(8,128)(2,1)S(1)} %collective-permute-done.5.refs_1_.sides, ...), custom_call_target="tpu_custom_call" | custom-call | flops 100000000 | bytes 1048576 | tf_op jit(solution)/shard_map/pallas_call | solution.py:644
  64.7 1.7 %collective-permute-done.12.refs_0_ = bf16[32,1280]{1,0:T(8,128)(2,1)S(1)} collective-permute-done((bf16[32,1280]{1,0:T(8,128)(2,1)S(1)}, bf16[32,1280]{1,0:T(8,128)(2,1)S(1)}, u32[]{:S(2)}, u32[]{:S(2)}) %collective-permute-start.12) | collective-permute-done | bytes 81952 | tf_op jit(solution)/shard_map/ppermute | solution.py:889
  66.4 2.1 %shard_map.271 = bf16[32,2048]{1,0:T(8,128)(2,1)} custom-call(f32[32,2048]{1,0:T(8,128)S(1)} %shard_map.269.total, bf16[32,1280]{1,0:T(8,128)(2,1)S(1)} %collective-permute-done.12.refs_0_, bf16[256,1280]{1,0:T(8,128)(2,1)} %collective-permute-done.13.refs_1_, bf16[256,1280]{1,0:T(8,128)(2,1)S(1)} %collective-permute-done.14.refs_2_), custom_call_target="tpu_custom_call" | custom-call | tf_op jit(solution)/shard_map/pallas_call | solution.py:644
  (56 shorter events, 0.1 us)
Async XLA Ops:
  2.5 0.8 %copy-start = (bf16[2048,128]{1,0:T(8,128)(2,1)}, bf16[2048,128]{1,0:T(8,128)(2,1)S(1)}, u32[]{:S(2)}) copy-start(bf16[2048,128]{1,0:T(8,128)(2,1)S(1)} %get-tuple-element.48.refs_1_) | copy-start | bytes 1572868
  3.3 0.8 %copy-start.2 = (bf16[2048,128]{1,0:T(8,128)(2,1)}, bf16[2048,128]{1,0:T(8,128)(2,1)S(1)}, u32[]{:S(2)}) copy-start(bf16[2048,128]{1,0:T(8,128)(2,1)S(1)} %get-tuple-element.52.refs_5_) | copy-start | bytes 1572868
  4.1 0.6 copy-start.23
  4.7 0.6 copy-start.25
  5.2 0.5 copy-start.27
  5.8 0.5 copy-start.29
  6.3 1.2 %copy-start.4 = (bf16[64,2048]{1,0:T(8,128)(2,1)}, bf16[64,2048]{1,0:T(8,128)(2,1)S(1)}, u32[]{:S(2)}) copy-start(bf16[64,2048]{1,0:T(8,128)(2,1)S(1)} %get-tuple-element.51.refs_4_) | copy-start | bytes 786436
  6.3 1.2 %copy-start.6 = (bf16[64,2048]{1,0:T(8,128)(2,1)}, bf16[64,2048]{1,0:T(8,128)(2,1)S(1)}, u32[]{:S(2)}) copy-start(bf16[64,2048]{1,0:T(8,128)(2,1)S(1)} %get-tuple-element.69.rec_query_t) | copy-start | bytes 786436
  6.3 1.2 %copy-start.9 = (bf16[256,128]{1,0:T(8,128)(2,1)}, bf16[256,128]{1,0:T(8,128)(2,1)S(1)}, u32[]{:S(2)}) copy-start(bf16[256,128]{1,0:T(8,128)(2,1)S(1)} %get-tuple-element.66.nope_up) | copy-start | bytes 196612
  6.3 1.2 %copy-start.11 = (f32[2,64,128]{2,1,0:T(8,128)}, f32[2,64,128]{2,1,0:T(8,128)S(1)}, u32[]{:S(2)}) copy-start(f32[2,64,128]{2,1,0:T(8,128)S(1)} %get-tuple-element.70.init_state) | copy-start | bytes 196612
  6.3 1.2 %copy-start.13 = (f32[128,128]{1,0:T(8,128)}, f32[128,128]{1,0:T(8,128)S(1)}, u32[]{:S(2)}) copy-start(f32[128,128]{1,0:T(8,128)S(1)} %get-tuple-element.57.refs_10_) | copy-start | bytes 196612
  6.3 1.2 %copy-start.15 = (f32[128,128]{1,0:T(8,128)}, f32[128,128]{1,0:T(8,128)S(1)}, u32[]{:S(2)}) copy-start(f32[128,128]{1,0:T(8,128)S(1)} %get-tuple-element.58.refs_11_) | copy-start | bytes 196612
  6.3 1.2 %copy-start.17 = (bf16[64,256]{1,0:T(8,128)(2,1)}, bf16[64,256]{1,0:T(8,128)(2,1)S(1)}, u32[]{:S(2)}) copy-start(bf16[64,256]{1,0:T(8,128)(2,1)S(1)} %get-tuple-element.67.rope_up_t) | copy-start | bytes 98308
  6.4 1.2 %copy-start.19 = (bf16[128,128]{1,0:T(8,128)(2,1)}, bf16[128,128]{1,0:T(8,128)(2,1)S(1)}, u32[]{:S(2)}) copy-start(bf16[128,128]{1,0:T(8,128)(2,1)S(1)} %get-tuple-element.68.key_up) | copy-start | bytes 98308
  6.4 1.2 %copy-start.21 = (bf16[4,2048]{1,0:T(4,128)(2,1)}, bf16[4,2048]{1,0:T(4,128)(2,1)S(1)}, u32[]{:S(2)}) copy-start(bf16[4,2048]{1,0:T(4,128)(2,1)S(1)} %get-tuple-element.53.refs_6_) | copy-start | bytes 49156
  6.4 4.3 %copy-start.8 = (bf16[32,2048]{1,0:T(8,128)(2,1)S(1)}, bf16[32,2048]{1,0:T(8,128)(2,1)}, u32[]{:S(2)}) copy-start(bf16[32,2048]{1,0:T(8,128)(2,1)} %refs_0_.1) | copy-start | bytes 393220
  7.6 28.3 %collective-permute-start.13 = (bf16[256,1280]{1,0:T(8,128)(2,1)}, bf16[256,1280]{1,0:T(8,128)(2,1)}, u32[]{:S(2)}, u32[]{:S(2)}) collective-permute-start(bf16[256,1280]{1,0:T(8,128)(2,1)} %get-tuple-element.88), channel_id=1, source_target_pairs={{0,2},{1,3},{2,0},{3,1},{4,6},{5,7},{6,4},{7,5},{8,10},{9,11},{10,... | collective-permute-start | bytes 1966088 | tf_op jit(solution)/shard_map/ppermute | solution.py:798
  10.6 49.6 %collective-permute-start.11 = (bf16[256,2048]{1,0:T(8,128)(2,1)S(1)}, bf16[256,2048]{1,0:T(8,128)(2,1)S(1)}, u32[]{:S(2)}, u32[]{:S(2)}) collective-permute-start(bf16[256,2048]{1,0:T(8,128)(2,1)S(1)} %get-tuple-element.87.weights), channel_id=1, source_target_pairs={{0,1},{1,0},{2,3},{3,2},{4,5},{5,4},{6,7},{7,6},{8,9},{9,8},{10,11... | collective-permute-start | bytes 3145736 | tf_op jit(solution)/shard_map/ppermute | solution.py:795
  10.6 17.9 %collective-permute-start.1 = (bf16[32,2048]{1,0:T(8,128)(2,1)S(1)}, bf16[32,2048]{1,0:T(8,128)(2,1)}, u32[]{:S(2)}, u32[]{:S(2)}) collective-permute-start(bf16[32,2048]{1,0:T(8,128)(2,1)S(1)} %copy-done.8), channel_id=1, source_target_pairs={{0,2},{1,3},{2,0},{3,1},{4,6},{5,7},{6,4},{7,5},{8,10},{9,11},{10,... | collective-permute-start | bytes 393224 | tf_op jit(solution)/shard_map/ppermute | solution.py:697
  10.8 18.6 %collective-permute-start = (bf16[32,2048]{1,0:T(8,128)(2,1)S(1)}, bf16[32,2048]{1,0:T(8,128)(2,1)}, u32[]{:S(2)}, u32[]{:S(2)}) collective-permute-start(bf16[32,2048]{1,0:T(8,128)(2,1)S(1)} %copy-done.8), channel_id=1, source_target_pairs={{0,1},{1,0},{2,3},{3,2},{4,5},{5,4},{6,7},{7,6},{8,9},{9,8},{10,11... | collective-permute-start | bytes 393224 | tf_op jit(solution)/shard_map/ppermute | solution.py:700
  11.2 19.5 %copy-start.1 = (bf16[2048,128]{1,0:T(8,128)(2,1)S(1)}, bf16[2048,128]{1,0:T(8,128)(2,1)}, u32[]{:S(2)}) copy-start(bf16[2048,128]{1,0:T(8,128)(2,1)} %copy-done) | copy-start | bytes 1572868
  28.5 2.2 %collective-permute-start.2 = (bf16[32,2048]{1,0:T(8,128)(2,1)}, bf16[32,2048]{1,0:T(8,128)(2,1)S(1)}, u32[]{:S(2)}, u32[]{:S(2)}) collective-permute-start(bf16[32,2048]{1,0:T(8,128)(2,1)} %collective-permute-done.1.refs_2_), channel_id=1, source_target_pairs={{0,1},{1,0},{2,3},{3,2},{4,5},{5,4},{6,7},{7,6},{8,9},{9,8},{10,11... | collective-permute-start | bytes 393224 | tf_op jit(solution)/shard_map/ppermute | solution.py:700
  29.4 1.3 %copy-start.5 = (bf16[64,2048]{1,0:T(8,128)(2,1)S(1)}, bf16[64,2048]{1,0:T(8,128)(2,1)}, u32[]{:S(2)}) copy-start(bf16[64,2048]{1,0:T(8,128)(2,1)} %copy-done.4) | copy-start | bytes 786436
  30.7 0.7 %copy-start.22 = (bf16[4,2048]{1,0:T(4,128)(2,1)S(1)}, bf16[4,2048]{1,0:T(4,128)(2,1)}, u32[]{:S(2)}) copy-start(bf16[4,2048]{1,0:T(4,128)(2,1)} %copy-done.21) | copy-start | bytes 49156
  30.7 0.7 %copy-start.24 = (f32[2,128]{1,0:T(2,128)S(1)}, f32[2,128]{1,0:T(2,128)}, u32[]{:S(2)}) copy-start(f32[2,128]{1,0:T(2,128)} %copy-done.23) | copy-start | bytes 3076
  30.7 0.7 %copy-start.30 = (f32[1,128]{1,0:T(1,128)S(1)}, f32[1,128]{1,0:T(1,128)}, u32[]{:S(2)}) copy-start(f32[1,128]{1,0:T(1,128)} %copy-done.29) | copy-start | bytes 1540
  31.4 1.0 %copy-start.3 = (bf16[2048,128]{1,0:T(8,128)(2,1)S(1)}, bf16[2048,128]{1,0:T(8,128)(2,1)}, u32[]{:S(2)}) copy-start(bf16[2048,128]{1,0:T(8,128)(2,1)} %copy-done.2) | copy-start | bytes 1572868
  32.4 0.8 %copy-start.14 = (f32[128,128]{1,0:T(8,128)S(1)}, f32[128,128]{1,0:T(8,128)}, u32[]{:S(2)}) copy-start(f32[128,128]{1,0:T(8,128)} %copy-done.13) | copy-start | bytes 196612
  33.3 0.8 %copy-start.16 = (f32[128,128]{1,0:T(8,128)S(1)}, f32[128,128]{1,0:T(8,128)}, u32[]{:S(2)}) copy-start(f32[128,128]{1,0:T(8,128)} %copy-done.15) | copy-start | bytes 196612
  34.1 2.3 %copy-start.7 = (bf16[64,2048]{1,0:T(8,128)(2,1)S(1)}, bf16[64,2048]{1,0:T(8,128)(2,1)}, u32[]{:S(2)}) copy-start(bf16[64,2048]{1,0:T(8,128)(2,1)} %copy-done.6) | copy-start | bytes 786436
  34.1 2.3 %copy-start.10 = (bf16[256,128]{1,0:T(8,128)(2,1)S(1)}, bf16[256,128]{1,0:T(8,128)(2,1)}, u32[]{:S(2)}) copy-start(bf16[256,128]{1,0:T(8,128)(2,1)} %copy-done.9) | copy-start | bytes 196612
  34.1 2.3 %copy-start.12 = (f32[2,64,128]{2,1,0:T(8,128)S(1)}, f32[2,64,128]{2,1,0:T(8,128)}, u32[]{:S(2)}) copy-start(f32[2,64,128]{2,1,0:T(8,128)} %copy-done.11) | copy-start | bytes 196612
  34.1 2.3 %copy-start.18 = (bf16[64,256]{1,0:T(8,128)(2,1)S(1)}, bf16[64,256]{1,0:T(8,128)(2,1)}, u32[]{:S(2)}) copy-start(bf16[64,256]{1,0:T(8,128)(2,1)} %copy-done.17) | copy-start | bytes 98308
  34.1 2.3 %copy-start.20 = (bf16[128,128]{1,0:T(8,128)(2,1)S(1)}, bf16[128,128]{1,0:T(8,128)(2,1)}, u32[]{:S(2)}) copy-start(bf16[128,128]{1,0:T(8,128)(2,1)} %copy-done.19) | copy-start | bytes 98308
  34.1 2.3 %copy-start.28 = (f32[2,64]{1,0:T(2,128)S(1)}, f32[2,64]{1,0:T(2,128)}, u32[]{:S(2)}) copy-start(f32[2,64]{1,0:T(2,128)} %copy-done.27) | copy-start | bytes 1540
  35.9 30.5 %collective-permute-start.14 = (bf16[256,1280]{1,0:T(8,128)(2,1)}, bf16[256,1280]{1,0:T(8,128)(2,1)S(1)}, u32[]{:S(2)}, u32[]{:S(2)}) collective-permute-start(bf16[256,1280]{1,0:T(8,128)(2,1)} %collective-permute-done.13.refs_1_), channel_id=1, source_target_pairs={{0,1},{1,0},{2,3},{3,2},{4,5},{5,4},{6,7},{7,6},{8,9},{9,8},{10,11... | collective-permute-start | bytes 1966088 | tf_op jit(solution)/shard_map/ppermute | solution.py:799
  36.4 0.7 copy-start.26
  38.6 13.4 %collective-permute-start.3 = (bf16[64,2944]{1,0:T(8,128)(2,1)S(1)}, bf16[64,2944]{1,0:T(8,128)(2,1)S(1)}, u32[]{:S(2)}, u32[]{:S(2)}) collective-permute-start(bf16[64,2944]{1,0:T(8,128)(2,1)S(1)} %get-tuple-element.72), channel_id=1, source_target_pairs={{0,1},{1,0},{2,3},{3,2},{4,5},{5,4},{6,7},{7,6},{8,9},{9,8},{10,11... | collective-permute-start | bytes 1130504 | tf_op jit(solution)/shard_map/ppermute | solution.py:800
  38.7 4.4 %collective-permute-start.4 = (bf16[240,128]{1,0:T(8,128)(2,1)S(1)}, bf16[240,128]{1,0:T(8,128)(2,1)S(1)}, u32[]{:S(2)}, u32[]{:S(2)}) collective-permute-start(bf16[240,128]{1,0:T(8,128)(2,1)S(1)} %get-tuple-element.73.refs_0_), channel_id=1, source_target_pairs={{0,4},{4,0},{8,12},{12,8},{16,20},{20,16},{24,28},{28,24},{1,5},{5... | collective-permute-start | bytes 184328 | tf_op jit(solution)/shard_map/ppermute | solution.py:806
  43.7 4.0 %collective-permute-start.5 = (bf16[144,128]{1,0:T(8,128)(2,1)S(1)}, bf16[144,128]{1,0:T(8,128)(2,1)S(1)}, u32[]{:S(2)}, u32[]{:S(2)}) collective-permute-start(bf16[144,128]{1,0:T(8,128)(2,1)S(1)} %get-tuple-element.74.sides), channel_id=1, source_target_pairs={{0,1},{1,0},{2,3},{3,2},{4,5},{5,4},{6,7},{7,6},{8,9},{9,8},{10,11... | collective-permute-start | bytes 110600 | tf_op jit(solution)/shard_map/ppermute | solution.py:835
  43.8 6.9 %collective-permute-start.7 = (bf16[264,128]{1,0:T(8,128)(2,1)S(1)}, bf16[264,128]{1,0:T(8,128)(2,1)S(1)}, u32[]{:S(2)}, u32[]{:S(2)}) collective-permute-start(bf16[264,128]{1,0:T(8,128)(2,1)S(1)} %get-tuple-element.76), channel_id=1, source_target_pairs={{0,24},{4,28},{8,16},{12,20},{16,8},{20,12},{24,0},{28,4},{1,25},{... | collective-permute-start | bytes 202760 | tf_op jit(solution)/shard_map/ppermute | solution.py:834
  47.6 4.3 %collective-permute-start.6 = (bf16[264,128]{1,0:T(8,128)(2,1)S(1)}, bf16[264,128]{1,0:T(8,128)(2,1)S(1)}, u32[]{:S(2)}, u32[]{:S(2)}) collective-permute-start(bf16[264,128]{1,0:T(8,128)(2,1)S(1)} %get-tuple-element.75.refs_2_), channel_id=1, source_target_pairs={{0,8},{4,12},{8,0},{12,4},{16,24},{20,28},{24,16},{28,20},{1,9},{5... | collective-permute-start | bytes 202760 | tf_op jit(solution)/shard_map/ppermute | solution.py:834
  52.0 8.2 %collective-permute-start.8 = (bf16[720,128]{1,0:T(8,128)(2,1)S(1)}, bf16[720,128]{1,0:T(8,128)(2,1)S(1)}, u32[]{:S(2)}, u32[]{:S(2)}) collective-permute-start(bf16[720,128]{1,0:T(8,128)(2,1)S(1)} %shard_map.266.packed), channel_id=1, source_target_pairs={{0,1},{1,0},{2,3},{3,2},{4,5},{5,4},{6,7},{7,6},{8,9},{9,8},{10,11... | collective-permute-start | bytes 552968 | tf_op jit(solution)/shard_map/ppermute | solution.py:844
  52.1 6.9 %collective-permute-start.9 = (bf16[264,128]{1,0:T(8,128)(2,1)S(1)}, bf16[264,128]{1,0:T(8,128)(2,1)S(1)}, u32[]{:S(2)}, u32[]{:S(2)}) collective-permute-start(bf16[264,128]{1,0:T(8,128)(2,1)S(1)} %get-tuple-element.77), channel_id=1, source_target_pairs={{0,16},{4,20},{8,24},{12,28},{16,0},{20,4},{24,8},{28,12},{1,17},{... | collective-permute-start | bytes 202760 | tf_op jit(solution)/shard_map/ppermute | solution.py:834
  59.0 1.3 %collective-permute-start.10 = (bf16[264,128]{1,0:T(8,128)(2,1)S(1)}, bf16[264,128]{1,0:T(8,128)(2,1)S(1)}, u32[]{:S(2)}, u32[]{:S(2)}) collective-permute-start(bf16[264,128]{1,0:T(8,128)(2,1)S(1)} %collective-permute-done.9.late), channel_id=1, source_target_pairs={{0,1},{1,0},{2,3},{3,2},{4,5},{5,4},{6,7},{7,6},{8,9},{9,8},{10,11... | collective-permute-start | bytes 202760 | tf_op jit(solution)/shard_map/ppermute | solution.py:845
  61.5 4.9 %collective-permute-start.12 = (bf16[32,1280]{1,0:T(8,128)(2,1)S(1)}, bf16[32,1280]{1,0:T(8,128)(2,1)S(1)}, u32[]{:S(2)}, u32[]{:S(2)}) collective-permute-start(bf16[32,1280]{1,0:T(8,128)(2,1)S(1)} %shard_map.270), channel_id=1, source_target_pairs={{0,2},{1,3},{2,0},{3,1},{4,6},{5,7},{6,4},{7,5},{8,10},{9,11},{10,... | collective-permute-start | bytes 245768 | tf_op jit(solution)/shard_map/ppermute | solution.py:889
